TPU v7x, 512 devices: a whole 4x8x8 slice. The times are simulated.
512 devices in a mesh: ep: 32 (over z, x), tp: 16 (over y, core).
Axes of the slice: x: 4, y: 8, z: 8, core: 2. Of those that a mesh axis runs over, the one named last changes fastest.
Arguments:
- mix_rows: bfloat16 [8192, 2048], P('ep'), may hold values from -6 to 6
- mix_gain: bfloat16 [2048], replicated, may hold values from 0.099609375 to 1.8984375
- w_query: bfloat16 [1024, 2048], P('tp'), may hold values from -0.125 to 0.125
- w_key: bfloat16 [1024, 2048], P('tp'), may hold values from -0.125 to 0.125
- w_value: bfloat16 [1024, 2048], P('tp'), may hold values from -0.125 to 0.125
- key_offset: float32 [16, 8192], P('tp'), may hold values from -11 to 0
- w_out: bfloat16 [1024, 2048], P('tp'), may hold values from -0.1875 to 0.1875
- out_gain: bfloat16 [2048], replicated, may hold values from 0.099609375 to 1.8984375
- exp_rows: bfloat16 [3072, 2048], P('ep', 'tp'), may hold values from -100 to 100
- exp_gain: bfloat16 [2048], P('tp'), may hold values from 0.099609375 to 1.8984375
- routes: int32 [3072, 4], P('ep'), may hold values from 0 to 31, all different within a row; in each aligned block of 96 rows (0 to 95, 96 to 191, ...) at most 16 rows name the same one
- route_weight: float32 [3072, 4], P('ep'), may hold values from 0.05 to 1
- w_gate: bfloat16 [32, 2048, 2048], P('ep', None, 'tp'), may hold values from -0.5 to 0.5
- w_up: bfloat16 [32, 2048, 2048], P('ep', None, 'tp'), may hold values from -0.5 to 0.5
- w_down: bfloat16 [32, 2048, 2048], P('ep', 'tp'), may hold values from -0.1875 to 0.1875
Outputs:
- mix_out: bfloat16 [8192, 2048], P('ep')
- exp_out: bfloat16 [3072, 2048], P('ep', 'tp')
Inputs may be any that keep to these rules, and one draw needn't show every extreme that they name: `routes`: each row names 4 different experts. Within the rows of one device (aligned blocks of 96 rows) no expert is named by more than 16 rows, and in some blocks one expert is named by exactly 16 rows.
All inputs are finite; a program needn't handle non-finite values.
Results may differ from a plain program's by a relative error of at most 0.019.
Values may be sent and summed in bfloat16 or wider, within the bound.
No kernel may reach another device: no remote copies, remote signals or barrier semaphores. Data moves between devices by JAX's collectives and lax.ppermute only.
A program may use at most 128 MiB of HBM per device.

v0:
```python
import math

import jax
import jax.numpy as jnp
from jax import lax
from jax.sharding import Mesh
from jax.sharding import PartitionSpec as P

EP = ("ep_0", "ep_1")
TP = ("tp_0", "tp_1")


EPSILON = 1e-06
CLAMP_LIMIT = 7.0
SILU_SHARPNESS = 1.702


def gathered_by_axis(value, axes, dim):
    out = value
    for number in range(len(axes) - 1, -1, -1):
        out = lax.all_gather(out, axes[number], axis=dim, tiled=True)
    return out


def split_up(value, dim, devices):
    dims = value.shape
    tiles = value.reshape(*dims[:dim], devices, dims[dim] // devices, *dims[dim + 1 :])
    return jnp.moveaxis(tiles, dim, 0)


def sent_and_summed(value, axis, dim):
    devices = lax.axis_size(axis)
    tiles = lax.all_to_all(split_up(value, dim, devices), axis, 0, 0, tiled=True)
    return jnp.sum(tiles.astype(jnp.float32), axis=0)


def from_everyone(value, axis):
    copies = jnp.broadcast_to(value, (lax.axis_size(axis), *value.shape))
    return lax.all_to_all(copies, axis, split_axis=0, concat_axis=0, tiled=True)


def of_everyone(value, axis):
    return from_everyone(value, axis).sum(axis=0)


def gather_turned(arrays, axis, dims):
    turned = [jnp.moveaxis(a, dim, 0) for a, dim in zip(arrays, dims)]
    widths = [t[0].size for t in turned]
    both = jnp.concatenate([t.reshape(-1, w) for t, w in zip(turned, widths)], axis=1)
    out = lax.all_gather(both, axis, axis=0, tiled=True)
    tiles = jnp.split(out, [sum(widths[:k]) for k in range(1, len(widths))], axis=1)
    return tuple(
        (
            jnp.moveaxis(b.reshape(-1, *t.shape[1:]), 0, dim)
            for b, t, dim in zip(tiles, turned, dims)
        )
    )


def summed_rows_2(value, chips, core, dim):
    sizes = (lax.axis_size(chips), lax.axis_size(core))
    tiles = split_up(value, dim, sizes[0] * sizes[1])
    inside = tiles.shape[1:]
    tiles = tiles.reshape(*sizes, *inside).swapaxes(0, 1).reshape(-1, *inside)
    tiles = lax.psum_scatter(tiles, core, scatter_dimension=0, tiled=True)
    return lax.psum_scatter(tiles, chips, scatter_dimension=0, tiled=True)[0]


def normalize(numbers, gain):
    factor = lax.rsqrt(jnp.mean(numbers * numbers, axis=-1, keepdims=True) + EPSILON)
    return numbers * factor * gain.astype(jnp.float32)


def project(normed, weight):
    product = lax.dot_general(
        normed, weight, (((1,), (1,)), ((), ())), preferred_element_type=jnp.float32
    )
    return product.astype(jnp.bfloat16)


def gated_units(gate_pre, up_pre):
    gate_part = jnp.minimum(gate_pre, CLAMP_LIMIT)
    up_part = jnp.clip(up_pre, -CLAMP_LIMIT, CLAMP_LIMIT)
    return (up_part + 1.0) * (gate_part * jax.nn.sigmoid(SILU_SHARPNESS * gate_part))


def stick_terms(queries, block_pairs, offset_values, query_index, key_index):
    heads_here = queries.shape[1]
    head_size = queries.shape[2]
    width = heads_here * head_size
    key_rows = block_pairs[:, :width].reshape(-1, heads_here, head_size)
    value_rows = block_pairs[:, width:].reshape(-1, heads_here, head_size)
    scores = jnp.einsum(
        "thd,shd->hts", queries, key_rows, preferred_element_type=jnp.float32
    ) / math.sqrt(head_size)
    scores = scores + offset_values[:, None, :]
    visible = (key_index[None, :] < query_index[:, None])[None]
    keep_log = jnp.where(visible, jax.nn.log_sigmoid(-scores), 0.0)
    later_sum = lax.cumsum(keep_log, axis=2, reverse=True) - keep_log
    exponent = jax.nn.log_sigmoid(scores) + later_sum
    weights = jnp.where(visible, jnp.exp(exponent), 0.0).astype(jnp.bfloat16)
    attended = jnp.einsum("hts,shd->thd", weights, value_rows, preferred_element_type=jnp.float32)
    return (attended, jnp.sum(keep_log, axis=2))


def on_device(
    mix_rows,
    mix_gain,
    w_query,
    w_key,
    w_value,
    key_offset,
    w_out,
    out_gain,
    exp_rows,
    exp_gain,
    routes,
    route_weight,
    w_gate,
    w_up,
    w_down,
):
    row_count = mix_rows.shape[0]
    heads_here = key_offset.shape[0]
    head_size = w_query.shape[0] // heads_here
    normed = normalize(mix_rows.astype(jnp.float32), mix_gain).astype(jnp.bfloat16)
    queries = project(normed, w_query).reshape(row_count, heads_here, head_size)
    own_pairs = jnp.concatenate([project(normed, w_key), project(normed, w_value)], axis=1)
    own_start = lax.axis_index(EP) * row_count
    query_index = own_start + jnp.arange(row_count, dtype=jnp.int32)
    every_pair = gathered_by_axis(own_pairs, EP, 0)
    key_index = jnp.arange(every_pair.shape[0], dtype=jnp.int32)
    attended, _ = stick_terms(queries, every_pair, key_offset, query_index, key_index)
    attended = attended.reshape(row_count, heads_here * head_size).astype(jnp.bfloat16)
    tp_count = lax.axis_size(TP)
    model_width = w_out.shape[1]
    column_count = model_width // tp_count
    columns = w_out
    share = sent_and_summed(
        lax.dot_general(
            columns, attended, (((0,), (1,)), ((), ())), preferred_element_type=jnp.float32
        ).astype(jnp.bfloat16),
        TP,
        0,
    )
    row_sums = of_everyone(jnp.sum(share * share, axis=0), TP)
    factor = lax.rsqrt(row_sums / model_width + EPSILON)
    gain_share = lax.dynamic_slice_in_dim(
        out_gain, lax.axis_index(TP) * column_count, column_count, 0
    ).astype(jnp.float32)
    own_columns = (share.T * factor[:, None] * gain_share[None, :]).astype(jnp.bfloat16)
    mix_out = lax.all_gather(own_columns, TP, axis=1, tiled=True)
    token_count, top_count = routes.shape
    ep_count = lax.axis_size(EP)
    experts = w_gate.shape[0] * ep_count
    capacity = 4 * token_count * top_count // (3 * experts)
    route_list = routes.reshape(-1)
    matches = (route_list[:, None] == jnp.arange(experts, dtype=jnp.int32)[None, :]).astype(
        jnp.int32
    )
    earlier = jnp.cumsum(matches, axis=0) - matches
    slot_index = route_list * capacity + jnp.sum(earlier * matches, axis=1)
    token_of = jnp.arange(route_list.shape[0], dtype=jnp.int32) // top_count + 1
    owners = jnp.zeros((experts * capacity,), jnp.int32).at[slot_index].set(token_of)
    whole_rows, whole_gain = gather_turned((exp_rows, exp_gain), TP, (1, 0))
    normed_exp = normalize(whole_rows.astype(jnp.float32), whole_gain).astype(jnp.bfloat16)
    outgoing = jnp.where(
        owners[:, None] > 0, normed_exp[jnp.maximum(owners - 1, 0)], jnp.zeros((), jnp.bfloat16)
    )
    arrived = lax.all_to_all(outgoing, EP, split_axis=0, concat_axis=0, tiled=True)
    gate_pre = jnp.dot(arrived, w_gate[0], preferred_element_type=jnp.float32)
    up_pre = jnp.dot(arrived, w_up[0], preferred_element_type=jnp.float32)
    hidden = gated_units(gate_pre, up_pre).astype(jnp.bfloat16)
    columns = w_down[0]
    expert_out = (
        summed_rows_2(
            lax.dot_general(
                columns, hidden, (((0,), (1,)), ((), ())), preferred_element_type=jnp.float32
            ).astype(jnp.bfloat16),
            "tp_0",
            "tp_1",
            0,
        )
        .astype(jnp.float32)
        .astype(jnp.bfloat16)
    )
    returned = lax.all_to_all(expert_out, EP, split_axis=1, concat_axis=1, tiled=True)
    picked = (
        jnp.take(returned, slot_index, axis=1)
        .astype(jnp.float32)
        .reshape(-1, token_count, top_count)
    )
    combined = jnp.sum(picked * route_weight[None], axis=2)
    exp_out = combined.T.astype(jnp.bfloat16)
    return (mix_out, exp_out)


def solution(mesh):
    torus = Mesh(mesh.devices.reshape(8, 4, 8, 2), ("ep_0", "ep_1", "tp_0", "tp_1"))
    in_specs = (
        P(EP, None),
        P(),
        P(TP, None),
        P(TP, None),
        P(TP, None),
        P(TP, None),
        P(TP, None),
        P(),
        P(EP, TP),
        P(TP),
        P(EP, None),
        P(EP, None),
        P(EP, None, TP),
        P(EP, None, TP),
        P(EP, TP, None),
    )
    out_specs = (P(EP, None), P(EP, TP))
    return jax.shard_map(
        on_device, mesh=torus, in_specs=in_specs, out_specs=out_specs, check_vma=False
    )
```

profile of v0, /device:TPU:1, one launch (start us, length us, event | category | flops | bytes accessed | tf_op | source)
XLA Modules:
  0.0 288.2 jit_solution(9969811278149230020)
XLA Ops:
  13.9 11.3 %all_gather.12 = bf16[1024,128]{0,1:T(8,128)(2,1)} all-gather(bf16[256,128]{0,1:T(8,128)(2,1)S(1)} %pad_maximum_fusion), channel_id=1, replica_groups=mesh['ep_0'=8,'ep_1'=4,'tp_0'=8,'tp_1'=2] {'ep_1'}, dimensions={0}, use_global_device_ids=true | all-gather | bytes 327680 | tf_op jit(solution)/shard_map/all_gather | solution.py:21
  28.4 2.9 %scatter_custom_fusion = s32[512]{0:T(512)S(1)} fusion(s32[384]{0:T(512)S(1)} %fusion.55, s32[384]{0:T(512)S(1)} %fusion.51, s32[]{:T(128)} %constant.94.clone.1), kind=kCustom, calls=%fused_computation.97 | custom fusion | bytes 2052 | tf_op jit(solution)/shard_map/scatter | solution.py:164
  32.1 23.8 %all_gather.15 = bf16[2048,97]{0,1:T(8,128)(2,1)S(1)} all-gather(bf16[128,97]{0,1:T(8,128)(2,1)S(1)} %pad_maximum_fusion.1), channel_id=1, replica_groups=mesh['ep_0'=8,'ep_1'=4,'tp_0'=8,'tp_1'=2] {'tp_0','tp_1'}, dimensions={0}, use_global_device_ids=true | all-gather | bytes 422144 | tf_op jit(solution)/shard_map/all_gather | solution.py:50
  56.3 2.5 gather_fusion
  60.3 10.9 %all-to-all-start.2 = ((bf16[32,16,2048]{2,1,0:T(8,128)(2,1)}), bf16[32,16,2048]{2,1,0:T(8,128)(2,1)S(1)}, u32[]{:S(2)}, u32[]{:S(2)}) async-start(bf16[32,16,2048]{2,1,0:T(8,128)(2,1)} %broadcast_select_fusion), calls=%async_computation.2 | async-start | bytes 4194304 | tf_op jit(solution)/shard_map/all_to_all | solution.py:170
  72.2 7.1 %fusion = f32[256,8192]{1,0:T(8,128)} fusion(f32[8192]{0:T(1024)S(1)} %bitcast.114, bf16[64,2048]{1,0:T(8,128)(2,1)S(1)} %copy-done.5, bf16[8192,128]{0,1:T(8,128)(2,1)} %all-gather.3.cloned.1.call-done, bf16[256,2048]{1,0:T(8,128)(2,1)} %param.15, f32[2048]{0:T(1024)S(1)} %convert_element_type.101, f32[256]{0:T(256)S(1)} %add_rsqrt_fusion.1), kind=kOutput, calls=%fused_computation.6 | convolution fusion | flops 341852160 | bytes 10789888 | tf_op jit(solution)/shard_map/thd,shd->hts/dot_general | solution.py:93
  79.3 7.4 %fusion.9 = f32[32,8,64,128]{3,1,2,0:T(8,128)S(1)} fusion(f32[256,8192]{1,0:T(8,128)} %fusion, s32[256]{0:T(256)S(1)} %iota_add_fusion), kind=kLoop, calls=%fused_computation.17 | loop fusion | flops 18874368 | bytes 16778240
  86.7 4.8 %copy.93 = f32[32,8,64,128]{3,2,1,0:T(8,128)} copy(f32[32,8,64,128]{3,1,2,0:T(8,128)S(1)} %fusion.9) | data formatting | bytes 16777216
  91.6 9.3 %copy.76 = f32[1,256,64,128]{1,2,3,0:T(8,128)} copy(f32[1,256,64,128]{3,2,1,0:T(8,128)} %bitcast.105) | data formatting | bytes 16777216 | tf_op jit(solution)/shard_map/reshape
  100.9 20.8 %all-to-all-done.2 = bf16[32,16,2048]{2,1,0:T(8,128)(2,1)S(1)} async-done(((bf16[32,16,2048]{2,1,0:T(8,128)(2,1)}), bf16[32,16,2048]{2,1,0:T(8,128)(2,1)S(1)}, u32[]{:S(2)}, u32[]{:S(2)}) %all-to-all-start.2) | async-done | bytes 2097184 | tf_op jit(solution)/shard_map/all_to_all | solution.py:170
  122.4 4.7 %fusion.12 = bf16[2048,512]{0,1:T(8,128)(2,1)} fusion(bf16[512,2048]{1,0:T(8,128)(2,1)S(1)} %bitcast.107, bf16[1,128,2048]{2,1,0:T(8,128)(2,1)S(1)} %copy-done, bf16[1,2048,128]{2,1,0:T(8,128)(2,1)} %param.28, f32[512,128]{1,0:T(8,128)S(1)} %convolution_minimum_fusion), kind=kOutput, calls=%fused_computation.20 | convolution fusion | flops 538509312 | bytes 5505024 | tf_op jit(solution)/shard_map/dot_general | solution.py:177
  127.1 3.2 %reshape_reshape.3 = bf16[8,2,128,512]{2,1,0,3:T(2,128)(2,1)S(1)} reshape(bf16[2048,512]{0,1:T(8,128)(2,1)} %fusion.12) | data formatting | bytes 4194304 | tf_op jit(solution)/shard_map/reshape;reshape | solution.py:64
  130.3 4.8 %copy.87 = bf16[8,2,128,512]{3,2,0,1:T(8,128)(2,1)} copy(bf16[8,2,128,512]{2,1,0,3:T(2,128)(2,1)S(1)} %reshape_reshape.3) | data formatting | bytes 4194304 | tf_op jit(solution)/shard_map/reshape;reshape | solution.py:64
  135.2 24.3 %fusion.67 = f32[1,256,64,128]{1,2,3,0:T(8,128)} fusion(f32[1,256,64,128]{1,2,3,0:T(8,128)} %copy.76), kind=kOutput, calls=%fused_computation.110 | output fusion | flops 266338304 | bytes 16777216 | tf_op jit(solution)/shard_map/reduce-window
  159.5 9.0 %copy.77 = f32[1,256,64,128]{3,2,1,0:T(8,128)} copy(f32[1,256,64,128]{1,2,3,0:T(8,128)} %fusion.67) | data formatting | bytes 16777216 | tf_op jit(solution)/shard_map/reduce-window
  170.0 2.3 broadcast.140
  173.4 18.7 %fusion.23 = bf16[256,64]{0,1:T(8,128)(2,1)S(1)} fusion(f32[32,8,64,128]{3,2,1,0:T(8,128)S(1)} %bitcast.110, f32[32,8,64,128]{3,2,1,0:T(8,128)S(1)} %bitcast.109, f32[256,8192]{1,0:T(8,128)} %fusion, s32[256]{0:T(256)S(1)} %iota_add_fusion, bf16[8192,128]{0,1:T(8,128)(2,1)S(1)} %copy-done.3), kind=kOutput, calls=%fused_computation.39 | convolution fusion | flops 314589184 | bytes 26248192 | tf_op jit(solution)/shard_map/hts,shd->thd/dot_general | solution.py:102
  193.9 6.2 %all-to-all-start = ((bf16[16,128,256]{1,2,0:T(8,128)(2,1)}), bf16[16,128,256]{1,2,0:T(8,128)(2,1)S(1)}, u32[]{:S(2)}, u32[]{:S(2)}) async-start(bf16[16,128,256]{1,2,0:T(8,128)(2,1)} %bitcast.102), calls=%async_computation | async-start | bytes 2097152 | tf_op jit(solution)/shard_map/all_to_all | solution.py:33
  200.6 29.8 %all-to-all-done = bf16[16,128,256]{1,2,0:T(8,128)(2,1)S(1)} async-done(((bf16[16,128,256]{1,2,0:T(8,128)(2,1)}), bf16[16,128,256]{1,2,0:T(8,128)(2,1)S(1)}, u32[]{:S(2)}, u32[]{:S(2)}) %all-to-all-start) | async-done | bytes 1048608 | tf_op jit(solution)/shard_map/all_to_all | solution.py:33
  231.3 4.8 %all-to-all-start.1 = ((f32[16,1,256]{2,1,0:T(1,128)}), f32[16,1,256]{2,1,0:T(1,128)S(1)}, u32[]{:S(2)}, u32[]{:S(2)}) async-start(f32[16,1,256]{2,1,0:T(1,128)} %broadcast_in_dim.31), calls=%async_computation.1 | async-start | bytes 32768 | tf_op jit(solution)/shard_map/all_to_all | solution.py:39
  236.9 6.6 %all-to-all-done.1 = f32[16,1,256]{2,1,0:T(1,128)S(1)} async-done(((f32[16,1,256]{2,1,0:T(1,128)}), f32[16,1,256]{2,1,0:T(1,128)S(1)}, u32[]{:S(2)}, u32[]{:S(2)}) %all-to-all-start.1) | async-done | bytes 16416 | tf_op jit(solution)/shard_map/all_to_all | solution.py:39
  246.2 6.9 %all-to-all-start.3 = ((bf16[128,32,16]{0,2,1:T(8,128)(2,1)}), bf16[128,32,16]{0,2,1:T(8,128)(2,1)S(1)}, u32[]{:S(2)}, u32[]{:S(2)}) async-start(bf16[128,32,16]{0,2,1:T(8,128)(2,1)} %bitcast.21), calls=%async_computation.5 | async-start | bytes 262144 | tf_op jit(solution)/shard_map/all_to_all | solution.py:187
  253.4 22.5 %all-gather.5.cloned.1.call-done = bf16[256,2048]{1,0:T(8,128)(2,1)} async-done(((bf16[256,128]{1,0:T(8,128)(2,1)}), bf16[256,2048]{1,0:T(8,128)(2,1)}) %all-gather.5.cloned.1.call-update) | async-done | bytes 1048592 | tf_op jit(solution)/shard_map/all_gather | solution.py:152
  278.3 2.3 copy.112
  (85 shorter events, 25.3 us)
Async XLA Ops:
  8.0 114.4 %copy-start = (bf16[1,128,2048]{2,1,0:T(8,128)(2,1)S(1)}, bf16[1,128,2048]{2,1,0:T(8,128)(2,1)}, u32[]{:S(2)}) copy-start(bf16[1,128,2048]{2,1,0:T(8,128)(2,1)} %param.29) | copy-start | bytes 1572868
  8.0 64.2 %all-gather.3.cloned.1.call-start = ((), (), s32[]{:S(2)}) async-start(), calls=%async_computation.6 | async-start | bytes 2359296 | tf_op jit(solution)/shard_map/all_gather | solution.py:21
  58.8 13.5 %copy-start.5 = (bf16[64,2048]{1,0:T(8,128)(2,1)S(1)}, bf16[64,2048]{1,0:T(8,128)(2,1)}, u32[]{:S(2)}) copy-start(bf16[64,2048]{1,0:T(8,128)(2,1)} %param.17) | copy-start | bytes 786436
  58.8 13.5 %copy-start.7 = (f32[1,8192]{1,0:T(1,128)S(1)}, f32[1,8192]{1,0:T(1,128)}, u32[]{:S(2)}) copy-start(f32[1,8192]{1,0:T(1,128)} %param.20) | copy-start | bytes 98308
  60.3 61.3 %all-to-all-start.2 = ((bf16[32,16,2048]{2,1,0:T(8,128)(2,1)}), bf16[32,16,2048]{2,1,0:T(8,128)(2,1)S(1)}, u32[]{:S(2)}, u32[]{:S(2)}) async-start(bf16[32,16,2048]{2,1,0:T(8,128)(2,1)} %broadcast_select_fusion), calls=%async_computation.2 | async-start | bytes 4194304 | tf_op jit(solution)/shard_map/all_to_all | solution.py:170
  71.2 128.9 %reduce-scatter.3.cloned.1.call-start = ((), (), s32[]{:S(2)}) async-start(), calls=%async_computation.8 | async-start | bytes 3145728 | tf_op jit(solution)/shard_map/reduce_scatter | solution.py:65
  91.6 30.0 %copy-start.4 = (bf16[1,2048,128]{2,1,0:T(8,128)(2,1)S(1)}, bf16[1,2048,128]{2,1,0:T(8,128)(2,1)}, u32[]{:S(2)}) copy-start(bf16[1,2048,128]{2,1,0:T(8,128)(2,1)} %param.27) | copy-start | bytes 1572868
  159.5 12.9 %copy-start.3 = (bf16[8192,128]{0,1:T(8,128)(2,1)S(1)}, bf16[8192,128]{0,1:T(8,128)(2,1)}, u32[]{:S(2)}) copy-start(bf16[8192,128]{0,1:T(8,128)(2,1)} %all-gather.3.cloned.1.call-done) | copy-start | bytes 6291460
  170.0 3.4 %copy-start.2 = (f32[1,256,64,128]{3,2,1,0:T(8,128)S(1)}, f32[1,256,64,128]{3,2,1,0:T(8,128)}, u32[]{:S(2)}) copy-start(f32[1,256,64,128]{3,2,1,0:T(8,128)} %copy.77) | copy-start | bytes 25165828
  173.4 18.7 %copy-start.6 = (bf16[64,2048]{1,0:T(8,128)(2,1)S(1)}, bf16[64,2048]{1,0:T(8,128)(2,1)}, u32[]{:S(2)}) copy-start(bf16[64,2048]{1,0:T(8,128)(2,1)} %param.21) | copy-start | bytes 786436
  173.4 107.2 %copy-start.1 = (bf16[1,128,2048]{2,1,0:T(8,128)(2,1)S(1)}, bf16[1,128,2048]{2,1,0:T(8,128)(2,1)}, u32[]{:S(2)}) copy-start(bf16[1,128,2048]{2,1,0:T(8,128)(2,1)} %param.29) | copy-start | bytes 1572868
  192.1 61.0 %copy-start.8 = (s32[96,4]{0,1:T(4,128)S(1)}, s32[96,4]{0,1:T(4,128)}, u32[]{:S(2)}) copy-start(s32[96,4]{0,1:T(4,128)} %param.25) | copy-start | bytes 4612
  192.1 61.1 %copy-start.9 = (f32[96,4]{0,1:T(4,128)S(1)}, f32[96,4]{0,1:T(4,128)}, u32[]{:S(2)}) copy-start(f32[96,4]{0,1:T(4,128)} %param.26) | copy-start | bytes 4612
  193.9 36.5 %all-to-all-start = ((bf16[16,128,256]{1,2,0:T(8,128)(2,1)}), bf16[16,128,256]{1,2,0:T(8,128)(2,1)S(1)}, u32[]{:S(2)}, u32[]{:S(2)}) async-start(bf16[16,128,256]{1,2,0:T(8,128)(2,1)} %bitcast.102), calls=%async_computation | async-start | bytes 2097152 | tf_op jit(solution)/shard_map/all_to_all | solution.py:33
  200.0 44.5 %reduce-scatter.5.cloned.1.call-start = ((), (), s32[]{:S(2)}) async-start(), calls=%async_computation.9 | async-start | bytes 1179648 | tf_op jit(solution)/shard_map/reduce_scatter | solution.py:66
  231.3 12.2 %all-to-all-start.1 = ((f32[16,1,256]{2,1,0:T(1,128)}), f32[16,1,256]{2,1,0:T(1,128)S(1)}, u32[]{:S(2)}, u32[]{:S(2)}) async-start(f32[16,1,256]{2,1,0:T(1,128)} %broadcast_in_dim.31), calls=%async_computation.1 | async-start | bytes 32768 | tf_op jit(solution)/shard_map/all_to_all | solution.py:39
  236.1 39.8 %all-gather.5.cloned.1.call-start = ((), (), s32[]{:S(2)}) async-start(), calls=%async_computation.7 | async-start | bytes 1114112 | tf_op jit(solution)/shard_map/all_gather | solution.py:152
  246.2 29.8 %all-to-all-start.3 = ((bf16[128,32,16]{0,2,1:T(8,128)(2,1)}), bf16[128,32,16]{0,2,1:T(8,128)(2,1)S(1)}, u32[]{:S(2)}, u32[]{:S(2)}) async-start(bf16[128,32,16]{0,2,1:T(8,128)(2,1)} %bitcast.21), calls=%async_computation.5 | async-start | bytes 262144 | tf_op jit(solution)/shard_map/all_to_all | solution.py:187
Sparse Core Ops, SparseCore 0:
  25.3 46.8 all-gather.2
  244.4 31.4 all-gather.4
Sparse Core Ops, SparseCore 1:
  135.2 15.2 reduce-scatter.2
  203.3 40.2 reduce-scatter.4
where the time goes:
time: 294 us; the launch traced here: 288 us
  waiting for transfers between devices  81 us (28%)
  local copies, waits for them, and re-layouts  50.1 us (17%)
  other arithmetic  41.7 us (14%)
  matrix products  35.2 us (12%)
  blocking collectives  35 us (12%)
  starting transfers between devices  29.2 us (10%)
  between operations  16 us (5%)
    all_to_all x1, waiting for transfers between devices, sent_and_summed(): lax.all_to_all(split_up(value, dim, devices), axis, 0, 0, tiled=True)  29.8 us
    another operation x4, other arithmetic  25.8 us
    all_gather x1, blocking collectives, gather_turned(): out = lax.all_gather(both, axis, axis=0, tiled=True)  23.8 us
    all_gather x1, waiting for transfers between devices, on_device(): mix_out = lax.all_gather(own_columns, TP, axis=1, tiled=True)  22.5 us
    all_to_all x1, waiting for transfers between devices, on_device(): lax.all_to_all(outgoing, EP, split_axis=0, concat_axis=0, tiled=True)  20.8 us
    dot_general x1, matrix products, stick_terms(): jnp.einsum('hts,shd->thd', weights, value_rows, preferred_element_type=jn...  18.7 us
    another operation x6, local copies, waits for them, and re-layouts  12.5 us
    all_gather x1, blocking collectives, gathered_by_axis(): out = lax.all_gather(out, axes[number], axis=dim, tiled=True)  11.3 us
  transfers between devices with their start and end apart: 8, of which 5 were waited for; matrix products, arithmetic and copies ran while one was open for 35% of the time, Pallas kernels for 0%

commit v1 on v0

v1 whole, which is shorter than its diff:
```python
import math

import jax
import jax.numpy as jnp
from jax import lax
from jax.experimental import pallas as pl
from jax.experimental.pallas import tpu as pltpu
from jax.sharding import Mesh
from jax.sharding import PartitionSpec as P

EP = ("ep_0", "ep_1")
TP = ("tp_0", "tp_1")

EPSILON = 1e-06
CLAMP_LIMIT = 7.0
SILU_SHARPNESS = 1.702
LOG2E = 1.4426950408889634
PAD = 16
UNROLL = 4


def dot(a, b, dims=((1,), (0,)), precision=None):
    return lax.dot_general(
        a, b, (dims, ((), ())), precision=precision, preferred_element_type=jnp.float32
    )


def row_factor(total, width):
    return lax.rsqrt(total / width + EPSILON)


def prepare_kernel(
    routes, weight, rows, mix_rows, gain, w_query, w_key, w_value, queries, payload, table
):
    top, tokens = routes.shape
    slots = table.shape[0]
    across, _, _ = payload.shape
    positions = mix_rows.shape[0]
    along = slots // (across * PAD)
    capacity = PAD
    slot = lax.broadcasted_iota(jnp.int32, (slots, tokens), 0)
    expert_of = slot // capacity
    place_of = slot - expert_of * capacity
    named = jnp.zeros((slots, tokens), jnp.float32)
    scale = jnp.zeros((slots, tokens), jnp.float32)
    for k in range(top):
        here = routes[k : k + 1, :] == expert_of
        named = jnp.where(here, 1.0, named)
        scale = jnp.where(here, weight[k : k + 1, :], scale)
    earlier = lax.broadcasted_iota(jnp.int32, (tokens, tokens), 0) < lax.broadcasted_iota(
        jnp.int32, (tokens, tokens), 1
    )
    earlier = jnp.where(earlier, 1.0, 0.0).astype(jnp.bfloat16)
    place = dot(named.astype(jnp.bfloat16), earlier)
    mine = (named > 0.0) & (place == place_of.astype(jnp.float32))
    table[...] = jnp.where(mine, scale, 0.0)
    chosen = jnp.where(mine, 1.0, 0.0).astype(jnp.bfloat16)
    outgoing = dot(chosen, rows[...]).astype(payload.dtype)
    for x in range(across):
        for z in range(along):
            at = (z * across + x) * capacity
            to = positions + z * capacity
            payload[x, to : to + capacity, :] = outgoing[at : at + capacity]

    numbers = mix_rows[...].astype(jnp.float32)
    factor = row_factor(jnp.sum(numbers * numbers, axis=1, keepdims=True), numbers.shape[1])
    normed = (numbers * factor * gain[...][None].astype(jnp.float32)).astype(jnp.bfloat16)
    queries[...] = dot(normed, w_query[...], ((1,), (1,))).astype(jnp.bfloat16)
    keys = dot(normed, w_key[...], ((1,), (1,)))
    values = dot(normed, w_value[...], ((1,), (1,)))
    pairs = jnp.concatenate([keys, values], axis=1).astype(payload.dtype)
    for x in range(across):
        payload[x, :positions, :] = pairs


def columns_kernel(w_down, w_out, out):
    parts, _, width = out.shape
    hidden = w_down.shape[1]
    for k in range(parts):
        at = slice(k * width, (k + 1) * width)
        out[k, :hidden, :] = w_down[0, :, at]
        out[k, hidden:, :] = w_out[:, at]


def attend_kernel(own_ref, queries, pairs, offsets, out):
    own = own_ref[0]
    rows, head = queries.shape
    q = queries[...]
    visible = lax.broadcasted_iota(jnp.int32, (rows, rows), 1) < lax.broadcasted_iota(
        jnp.int32, (rows, rows), 0
    )
    after = jnp.where(visible, -1.0, 0.0).astype(jnp.bfloat16)

    def front(j, diagonal):
        pair = pairs[j]
        offset = offsets[:, pl.ds(pl.multiple_of(j * rows, rows), rows)]
        s = dot(q, pair[:, :head], ((1,), (1,)))
        s = s * (LOG2E / math.sqrt(head)) + offset * LOG2E
        soft = jnp.log2(1.0 + jnp.exp2(-jnp.abs(s)))
        take = jnp.minimum(s, 0.0) - soft
        cost = jnp.maximum(s, 0.0) + soft
        if diagonal:
            cost = jnp.where(visible, cost, 0.0)
        inside = dot(cost.astype(jnp.bfloat16), after)
        return take + inside, inside[:, :1] - cost[:, :1], pair[:, head:]

    def back(ahead, state, diagonal):
        later, acc = state
        exponent, total, values = ahead
        w = jnp.exp2(exponent + later)
        if diagonal:
            w = jnp.where(visible, w, 0.0)
        return later + total, acc + dot(w.astype(jnp.bfloat16), values)

    def group(j, count, state):
        ahead = [front(j - i, False) for i in range(count)]
        for one in ahead:
            state = back(one, state, False)
        return state

    state = (jnp.zeros((rows, 1), jnp.float32), jnp.zeros((rows, head), jnp.float32))
    state = back(front(own, True), state, True)
    rest = own % UNROLL
    state = lax.fori_loop(0, rest, lambda i, c: group(own - 1 - i, 1, c), state)
    state = lax.fori_loop(
        0, own // UNROLL, lambda i, c: group(own - 1 - rest - i * UNROLL, UNROLL, c), state
    )
    half = rows // 2
    acc = state[1].astype(out.dtype)
    out[...] = jnp.concatenate([acc[:half], acc[half:]], axis=1)


def mix_columns_kernel(attended, weights, out):
    parts, half, width = attended.shape
    head = width // 2
    skip = weights.shape[1] - head
    side = jnp.concatenate([weights[k, skip:, :] for k in range(parts)], axis=0)
    top = jnp.concatenate([attended[k][:, :head] for k in range(parts)], axis=1)
    low = jnp.concatenate([attended[k][:, head:] for k in range(parts)], axis=1)
    out[:half, :] = dot(top, side).astype(out.dtype)
    out[half:, :] = dot(low, side).astype(out.dtype)


def mix_norm_kernel(core_ref, mine, theirs, gain, out):
    core = core_ref[0]
    groups, rows, width = mine.shape
    total = jnp.zeros((rows, width), jnp.float32)
    for k in range(groups):
        for side in (mine, theirs):
            numbers = side[k].astype(jnp.float32)
            total = total + numbers * numbers
    factor = row_factor(jnp.sum(total, axis=1, keepdims=True), 2 * groups * width)
    scale = gain[...].astype(jnp.float32)[None]
    first = core == 0
    for k in range(groups):
        pair = (mine[k].astype(jnp.float32), theirs[k].astype(jnp.float32))
        for which in range(2):
            at = slice((2 * k + which) * width, (2 * k + which + 1) * width)
            numbers = jnp.where(first, pair[which], pair[1 - which])
            out[:, at] = (numbers * factor * scale[:, at]).astype(out.dtype)


def expert_kernel(core_ref, mine, theirs, w_gate, w_up, out, normed):
    core = core_ref[0]
    groups, padded, width = mine.shape
    rows = padded - PAD
    total = jnp.zeros((rows, width), jnp.float32)
    for k in range(groups):
        for side in (mine, theirs):
            numbers = side[k, :rows, :].astype(jnp.float32)
            total = total + numbers * numbers
    factor = row_factor(jnp.sum(total, axis=1, keepdims=True), 2 * groups * width)
    for k in range(groups):
        for side, which in ((mine, core), (theirs, 1 - core)):
            at = pl.ds(pl.multiple_of((2 * k + which) * width, width), width)
            gain = side[k, rows : rows + 1, :].astype(jnp.float32)
            numbers = side[k, :rows, :].astype(jnp.float32) * factor * gain
            normed[:, at] = numbers.astype(jnp.bfloat16)
    gate = jnp.minimum(dot(normed[...], w_gate[0]), CLAMP_LIMIT)
    up = jnp.clip(dot(normed[...], w_up[0]), -CLAMP_LIMIT, CLAMP_LIMIT)
    hidden = (up + 1.0) * (gate * jax.nn.sigmoid(SILU_SHARPNESS * gate))
    out[...] = hidden.astype(out.dtype)


def down_kernel(hidden, weights, out):
    parts, _, width = hidden.shape
    total = jnp.zeros(out.shape, jnp.float32)
    for k in range(0, parts, 2):
        both = jnp.concatenate([hidden[k], hidden[k + 1]], axis=1)
        side = jnp.concatenate([weights[k, :width, :], weights[k + 1, :width, :]], axis=0)
        total = total + dot(both, side)
    out[...] = total.astype(out.dtype)


def combine_kernel(table, returned, out):
    scale = table[...]
    rows = returned[...]
    total = jnp.zeros(out.shape, jnp.float32)
    for _ in range(3):
        part = scale.astype(jnp.bfloat16)
        total = total + dot(part, rows, ((0,), (0,)))
        scale = scale - part.astype(jnp.float32)
    out[...] = total.astype(out.dtype)


def call(body, outs, *args, scalars=0, **kwargs):
    spaces = [pltpu.SMEM] * scalars + [pltpu.VMEM] * (len(args) - scalars)
    specs = [pl.BlockSpec(memory_space=space) for space in spaces]
    return pl.pallas_call(body, out_shape=outs, in_specs=specs, **kwargs)(*args)


def stacked(value, axis):
    copies = jnp.broadcast_to(value, (lax.axis_size(axis), *value.shape))
    return exchanged(copies, axis)


def exchanged(value, axis):
    return lax.all_to_all(value, axis, 0, 0, tiled=True)


def from_partner(value):
    return lax.ppermute(value, "tp_1", [(0, 1), (1, 0)])


def on_device(
    mix_rows,
    mix_gain,
    w_query,
    w_key,
    w_value,
    key_offset,
    w_out,
    out_gain,
    exp_rows,
    exp_gain,
    routes,
    route_weight,
    w_gate,
    w_up,
    w_down,
):
    bf16 = jnp.bfloat16
    shape = jax.ShapeDtypeStruct
    ep_count = lax.axis_size(EP)
    tp_count = lax.axis_size(TP)
    tokens, top = routes.shape
    part = exp_rows.shape[1]
    experts = ep_count * w_gate.shape[0]
    capacity = 4 * tokens * top // (3 * experts)
    slots = experts * capacity
    rows = mix_rows.shape[0]
    head = w_query.shape[0]
    model = mix_rows.shape[1]
    own = lax.axis_index(EP).astype(jnp.int32)[None]
    core = lax.axis_index("tp_1").astype(jnp.int32)[None]

    across = lax.axis_size("ep_1")
    height = rows + slots // across
    queries, payload, table = call(
        prepare_kernel,
        (
            shape((rows, head), bf16),
            shape((across, height, part), bf16),
            shape((slots, tokens), jnp.float32),
        ),
        routes.T,
        route_weight.T,
        exp_rows,
        mix_rows,
        mix_gain,
        w_query,
        w_key,
        w_value,
    )
    payload = exchanged(payload, "ep_1")
    pairs = payload[:, :rows]
    every_pair = lax.all_gather(pairs, "ep_0", axis=0, tiled=True)
    outgoing = payload[:, rows:].reshape(across, -1, capacity, part).swapaxes(0, 1)
    arrived = exchanged(outgoing, "ep_0").reshape(slots, part)
    gain_rows = jnp.broadcast_to(exp_gain[None], (PAD, part))
    mine = stacked(jnp.concatenate([arrived, gain_rows], axis=0), "tp_0")

    columns = call(
        columns_kernel,
        shape((tp_count, w_down.shape[1] + head, model // tp_count), bf16),
        w_down,
        w_out,
    )
    columns = exchanged(columns, TP)

    hidden = call(
        expert_kernel,
        shape((slots, w_gate.shape[2]), bf16),
        core,
        mine,
        from_partner(mine),
        w_gate,
        w_up,
        scalars=1,
        scratch_shapes=[pltpu.VMEM((slots, model), bf16)],
    )
    every_hidden = lax.all_gather(hidden, TP, axis=0)
    expert_out = call(down_kernel, shape((slots, part), bf16), every_hidden, columns)
    returned = exchanged(expert_out, EP)
    exp_out = call(combine_kernel, shape((tokens, part), bf16), table, returned)

    attended = call(
        attend_kernel,
        shape((rows // 2, 2 * head), bf16),
        own,
        queries,
        every_pair,
        key_offset,
        scalars=1,
    )
    every_head = lax.all_gather(attended, TP, axis=0)
    own_columns = call(
        mix_columns_kernel, shape((rows, model // tp_count), bf16), every_head, columns
    )
    mine = stacked(own_columns, "tp_0")
    mix_out = call(
        mix_norm_kernel,
        shape((rows, model), bf16),
        core,
        mine,
        from_partner(mine),
        out_gain,
        scalars=1,
    )
    return (mix_out, exp_out)


def solution(mesh):
    torus = Mesh(mesh.devices.reshape(8, 4, 8, 2), ("ep_0", "ep_1", "tp_0", "tp_1"))
    in_specs = (
        P(EP, None),
        P(),
        P(TP, None),
        P(TP, None),
        P(TP, None),
        P(TP, None),
        P(TP, None),
        P(),
        P(EP, TP),
        P(TP),
        P(EP, None),
        P(EP, None),
        P(EP, None, TP),
        P(EP, None, TP),
        P(EP, TP, None),
    )
    out_specs = (P(EP, None), P(EP, TP))

    def step(*args):
        return on_device(*args)

    step = jax.shard_map(
        step, mesh=torus, in_specs=in_specs, out_specs=out_specs, check_vma=False
    )
    return step
```

time: 294 us -> 192 us (0.65); the launches traced: 288 us -> 191 us
  blocking collectives: 35 us -> 122 us
  waiting for transfers between devices: 81 us -> 8.7 us
  local copies, waits for them, and re-layouts: 50.1 us -> 5.11 us
  other arithmetic: 41.7 us -> 0.01 us
  matrix products: 35.2 us -> 0 us
  Pallas kernels: 0 us -> 23.8 us
  starting transfers between devices: 29.2 us -> 17.5 us
    all_to_all x0 -> x4, blocking collectives: none -> 83.6 us  [exchanged(): return lax.all_to_all(value, axis, 0, 0, tiled=True)]
    all_to_all x4 -> x2, waiting for transfers between devices: 57.2 us -> 6.33 us  [exchanged(): return lax.all_to_all(value, axis, 0, 0, tiled=True)]
    dot_general x7 -> x0, matrix products: 35.2 us -> none  [the longest x1 18.7 us: stick_terms(): jnp.einsum('hts,shd->thd', weights, value_rows, preferred_element_type=jn...]
    another operation x4 -> x0, other arithmetic: 25.8 us -> none
    pallas_call x0 -> x8, Pallas kernels: none -> 23.8 us  [call(): return pl.pallas_call(body, out_shape=outs, in_specs=specs, **kwargs)(*args)]
    all_gather x2, waiting for transfers between devices: 23.3 us -> 0.03 us  [the longest x1 0.02 us: on_device(): every_hidden = lax.all_gather(hidden, TP, axis=0)]
    all_to_all x4 -> x2, starting transfers between devices: 28.8 us -> 7.62 us  [exchanged(): return lax.all_to_all(value, axis, 0, 0, tiled=True)]
    another operation x8 -> x0, local copies, waits for them, and re-layouts: 20.5 us -> none
  transfers between devices with their start and end apart: 8 -> 6, of which waited for: 5 -> 2; matrix products, arithmetic and copies ran while one was open for 35% -> 1% of each run, Pallas kernels for 0% -> 10%
where the time goes in v1:
time: 192 us; the launch traced here: 191 us
  blocking collectives  122 us (64%)
  Pallas kernels  23.8 us (12%)
  starting transfers between devices  17.5 us (9%)
  between operations  14.1 us (7%)
  waiting for transfers between devices  8.7 us (5%)
  local copies, waits for them, and re-layouts  5.11 us (3%)
    all_to_all x4, blocking collectives, exchanged(): return lax.all_to_all(value, axis, 0, 0, tiled=True)  83.6 us
    all_gather x1, blocking collectives, on_device(): every_head = lax.all_gather(attended, TP, axis=0)  38.6 us
    pallas_call x8, Pallas kernels, call(): return pl.pallas_call(body, out_shape=outs, in_specs=specs, **kwargs)(*args)  23.8 us
    ppermute x2, starting transfers between devices, from_partner(): return lax.ppermute(value, 'tp_1', [(0, 1), (1, 0)])  9.76 us
    all_to_all x2, starting transfers between devices, exchanged(): return lax.all_to_all(value, axis, 0, 0, tiled=True)  7.62 us
    all_to_all x2, waiting for transfers between devices, exchanged(): return lax.all_to_all(value, axis, 0, 0, tiled=True)  6.33 us
  transfers between devices with their start and end apart: 6, of which 2 were waited for; matrix products, arithmetic and copies ran while one was open for 1% of the time, Pallas kernels for 10%

profile of v1, /device:TPU:1, one launch (start us, length us, event | category | flops | bytes accessed | tf_op | source)
XLA Modules:
  0.0 191.5 jit_solution(499175432547218237)
XLA Ops:
  7.2 3.8 %shard_map.158 = (bf16[256,64]{1,0:T(8,128)(2,1)}, bf16[4,384,128]{2,1,0:T(8,128)(2,1)}, f32[512,96]{1,0:T(8,128)}) custom-call(s32[4,96]{1,0:T(4,128)} %bitcast.20, f32[4,96]{1,0:T(4,128)} %bitcast.21, bf16[96,128]{1,0:T(8,128)(2,1)} %rows.1, bf16[256,2048]{1,0:T(8,128)(2,1)} %mix_rows.1, bf16[2048]{0:T(1024)(128)(2,1)} %gain.2, bf16[64,2048]{1,0:T(8,128)(2,1)} %w_query.1, ...), custom_call_target="tpu_custom_call" | custom-call | tf_op jit(solution)/shard_map/pallas_call | solution.py:209
  11.0 11.2 %all_to_all.36 = bf16[4,384,128]{2,1,0:T(8,128)(2,1)S(1)} all-to-all(bf16[4,384,128]{2,1,0:T(8,128)(2,1)} %get-tuple-element.6), channel_id=1, replica_groups=mesh['ep_0'=8,'ep_1'=4,'tp_0'=8,'tp_1'=2] {'ep_1'}, dimensions={0} | all-to-all | bytes 786432 | tf_op jit(solution)/shard_map/all_to_all | solution.py:218
  22.2 0.7 slice.8
  23.0 18.8 %all_to_all.37 = bf16[8,4,16,128]{3,2,1,0:T(8,128)(2,1)S(1)} all-to-all(bf16[8,4,16,128]{3,2,1,0:T(8,128)(2,1)S(1)} %bitcast.19), channel_id=1, replica_groups=mesh['ep_0'=8,'ep_1'=4,'tp_0'=8,'tp_1'=2] {'ep_0'}, dimensions={0} | all-to-all | bytes 262144 | tf_op jit(solution)/shard_map/all_to_all | solution.py:218
  42.0 31.6 %all_to_all.38.mine = bf16[8,528,128]{2,1,0:T(8,128)(2,1)S(1)} all-to-all(bf16[8,528,128]{2,1,0:T(8,128)(2,1)S(1)} %broadcast_in_dim.22), channel_id=1, replica_groups=mesh['ep_0'=8,'ep_1'=4,'tp_0'=8,'tp_1'=2] {'tp_0'}, dimensions={0} | all-to-all | bytes 2162688 | tf_op jit(solution)/shard_map/all_to_all | solution.py:218
  73.6 7.3 %collective-permute-start.1 = (bf16[8,528,128]{2,1,0:T(8,128)(2,1)S(1)}, bf16[8,528,128]{2,1,0:T(8,128)(2,1)S(1)}, u32[]{:S(2)}, u32[]{:S(2)}) collective-permute-start(bf16[8,528,128]{2,1,0:T(8,128)(2,1)S(1)} %all_to_all.38.mine), channel_id=1, source_target_pairs={{0,1},{1,0},{2,3},{3,2},{4,5},{5,4},{6,7},{7,6},{8,9},{9,8},{10,11... | collective-permute-start | bytes 3244040 | tf_op jit(solution)/shard_map/ppermute | solution.py:222
  80.9 2.3 %collective-permute-done.1.theirs = bf16[8,528,128]{2,1,0:T(8,128)(2,1)S(1)} collective-permute-done((bf16[8,528,128]{2,1,0:T(8,128)(2,1)S(1)}, bf16[8,528,128]{2,1,0:T(8,128)(2,1)S(1)}, u32[]{:S(2)}, u32[]{:S(2)}) %collective-permute-start.1) | collective-permute-done | bytes 1081376 | tf_op jit(solution)/shard_map/ppermute | solution.py:222
  83.2 1.0 copy-done.3
  84.2 5.2 %shard_map.163 = bf16[512,128]{1,0:T(8,128)(2,1)} custom-call(s32[1]{0:T(128)} %bitcast.core_ref, bf16[8,528,128]{2,1,0:T(8,128)(2,1)} %copy-done.1, bf16[8,528,128]{2,1,0:T(8,128)(2,1)} %copy-done.3, bf16[1,2048,128]{2,1,0:T(8,128)(2,1)} %w_gate.1, bf16[1,2048,128]{2,1,0:T(8,128)(2,1)} %w_up.1), custom_call_target="tpu_custom_call" | custom-call | tf_op jit(solution)/shard_map/pallas_call | solution.py:209
  89.4 2.1 %shard_map.160 = bf16[16,192,128]{2,1,0:T(8,128)(2,1)} custom-call(bf16[1,128,2048]{2,1,0:T(8,128)(2,1)} %w_down.1, bf16[64,2048]{1,0:T(8,128)(2,1)} %w_out.1), custom_call_target="tpu_custom_call" | custom-call | tf_op jit(solution)/shard_map/pallas_call | solution.py:209
  91.5 3.8 %all-to-all-start.1 = ((bf16[16,192,128]{2,1,0:T(8,128)(2,1)}), bf16[16,192,128]{2,1,0:T(8,128)(2,1)S(1)}, u32[]{:S(2)}, u32[]{:S(2)}) async-start(bf16[16,192,128]{2,1,0:T(8,128)(2,1)} %shard_map.160), calls=%async_computation.1 | async-start | bytes 1572864 | tf_op jit(solution)/shard_map/all_to_all | solution.py:218
  95.3 2.8 %shard_map.159 = bf16[128,128]{1,0:T(8,128)(2,1)} custom-call(s32[1]{0:T(128)} %bitcast.1.own_ref, bf16[256,64]{1,0:T(8,128)(2,1)} %get-tuple-element.5.queries, bf16[32,256,128]{2,1,0:T(8,128)(2,1)} %all-gather.5.cloned.1.call-done.pairs, f32[1,8192]{1,0:T(1,128)} %offsets.1), custom_call_target="tpu_custom_call" | custom-call | tf_op jit(solution)/shard_map/pallas_call | solution.py:209
  98.1 38.6 %all-gather = bf16[2048,128]{1,0:T(8,128)(2,1)} all-gather(bf16[128,128]{1,0:T(8,128)(2,1)} %shard_map.159), channel_id=2, replica_groups=mesh['ep_0'=8,'ep_1'=4,'tp_0'=8,'tp_1'=2] {'tp_0','tp_1'}, dimensions={0}, use_global_device_ids=true | all-gather | bytes 557056 | tf_op jit(solution)/shard_map/all_gather | solution.py:316
  136.8 0.9 copy-done
  137.6 2.3 %shard_map.161 = bf16[256,128]{1,0:T(8,128)(2,1)} custom-call(bf16[16,128,128]{2,1,0:T(8,128)(2,1)} %bitcast.14, bf16[16,192,128]{2,1,0:T(8,128)(2,1)} %copy-done), custom_call_target="tpu_custom_call" | custom-call | tf_op jit(solution)/shard_map/pallas_call | solution.py:209
  139.9 0.9 broadcast_in_dim.20
  140.8 21.9 %all_to_all.39.mine = bf16[8,256,128]{2,1,0:T(8,128)(2,1)S(1)} all-to-all(bf16[8,256,128]{2,1,0:T(8,128)(2,1)S(1)} %broadcast_in_dim.20), channel_id=1, replica_groups=mesh['ep_0'=8,'ep_1'=4,'tp_0'=8,'tp_1'=2] {'tp_0'}, dimensions={0} | all-to-all | bytes 1048576 | tf_op jit(solution)/shard_map/all_to_all | solution.py:218
  162.7 2.5 %collective-permute-start = (bf16[8,256,128]{2,1,0:T(8,128)(2,1)S(1)}, bf16[8,256,128]{2,1,0:T(8,128)(2,1)S(1)}, u32[]{:S(2)}, u32[]{:S(2)}) collective-permute-start(bf16[8,256,128]{2,1,0:T(8,128)(2,1)S(1)} %all_to_all.39.mine), channel_id=1, source_target_pairs={{0,1},{1,0},{2,3},{3,2},{4,5},{5,4},{6,7},{7,6},{8,9},{9,8},{10,11... | collective-permute-start | bytes 1572872 | tf_op jit(solution)/shard_map/ppermute | solution.py:222
  165.2 3.1 %shard_map.164 = bf16[512,128]{1,0:T(8,128)(2,1)} custom-call(bf16[16,512,128]{2,1,0:T(8,128)(2,1)} %bitcast.13, bf16[16,192,128]{2,1,0:T(8,128)(2,1)} %copy-done), custom_call_target="tpu_custom_call" | custom-call | tf_op jit(solution)/shard_map/pallas_call | solution.py:209
  168.4 3.8 %all-to-all-start.5 = ((bf16[32,16,128]{2,1,0:T(8,128)(2,1)}), bf16[32,16,128]{2,1,0:T(8,128)(2,1)S(1)}, u32[]{:S(2)}, u32[]{:S(2)}) async-start(bf16[32,16,128]{2,1,0:T(8,128)(2,1)} %bitcast.16), calls=%async_computation.5 | async-start | bytes 262144 | tf_op jit(solution)/shard_map/all_to_all | solution.py:218
  172.2 0.8 copy-done.4
  173.0 2.7 %shard_map.162 = bf16[256,2048]{1,0:T(8,128)(2,1)} custom-call(s32[1]{0:T(128)} %bitcast.core_ref, bf16[8,256,128]{2,1,0:T(8,128)(2,1)} %copy-done.2, bf16[8,256,128]{2,1,0:T(8,128)(2,1)} %copy-done.4, bf16[2048]{0:T(1024)(128)(2,1)} %gain.3), custom_call_target="tpu_custom_call" | custom-call | tf_op jit(solution)/shard_map/pallas_call | solution.py:209
  175.8 6.3 %all-to-all-done.5 = bf16[32,16,128]{2,1,0:T(8,128)(2,1)S(1)} async-done(((bf16[32,16,128]{2,1,0:T(8,128)(2,1)}), bf16[32,16,128]{2,1,0:T(8,128)(2,1)S(1)}, u32[]{:S(2)}, u32[]{:S(2)}) %all-to-all-start.5) | async-done | bytes 131104 | tf_op jit(solution)/shard_map/all_to_all | solution.py:218
  182.7 1.9 shard_map.165
  (24 shorter events, 1.0 us)
Async XLA Ops:
  7.2 88.2 %all-gather.5.cloned.1.call-start = ((), (), s32[]{:S(2)}) async-start(), calls=%async_computation.6 | async-start | bytes 2359296 | tf_op jit(solution)/shard_map/all_gather | solution.py:277
  11.0 30.9 %copy-start.6 = (bf16[128]{0:T(256)(128)(2,1)S(1)}, bf16[128]{0:T(256)(128)(2,1)}, u32[]{:S(2)}) copy-start(bf16[128]{0:T(256)(128)(2,1)} %param.24) | copy-start | bytes 772
  22.9 142.3 %all-gather.7.cloned.1.call-start = ((), (), s32[]{:S(2)}) async-start(), calls=%async_computation.7 | async-start | bytes 2228224 | tf_op jit(solution)/shard_map/all_gather | solution.py:302
  73.6 9.6 %copy-start.1 = (bf16[8,528,128]{2,1,0:T(8,128)(2,1)}, bf16[8,528,128]{2,1,0:T(8,128)(2,1)S(1)}, u32[]{:S(2)}) copy-start(bf16[8,528,128]{2,1,0:T(8,128)(2,1)S(1)} %all_to_all.38.mine) | copy-start | bytes 3244036
  73.6 9.6 %collective-permute-start.1 = (bf16[8,528,128]{2,1,0:T(8,128)(2,1)S(1)}, bf16[8,528,128]{2,1,0:T(8,128)(2,1)S(1)}, u32[]{:S(2)}, u32[]{:S(2)}) collective-permute-start(bf16[8,528,128]{2,1,0:T(8,128)(2,1)S(1)} %all_to_all.38.mine), channel_id=1, source_target_pairs={{0,1},{1,0},{2,3},{3,2},{4,5},{5,4},{6,7},{7,6},{8,9},{9,8},{10,11... | collective-permute-start | bytes 3244040 | tf_op jit(solution)/shard_map/ppermute | solution.py:222
  83.2 1.0 copy-start.3
  91.5 45.2 %all-to-all-start.1 = ((bf16[16,192,128]{2,1,0:T(8,128)(2,1)}), bf16[16,192,128]{2,1,0:T(8,128)(2,1)S(1)}, u32[]{:S(2)}, u32[]{:S(2)}) async-start(bf16[16,192,128]{2,1,0:T(8,128)(2,1)} %shard_map.160), calls=%async_computation.1 | async-start | bytes 1572864 | tf_op jit(solution)/shard_map/all_to_all | solution.py:218
  136.7 0.9 copy-start
  162.7 5.7 %copy-start.2 = (bf16[8,256,128]{2,1,0:T(8,128)(2,1)}, bf16[8,256,128]{2,1,0:T(8,128)(2,1)S(1)}, u32[]{:S(2)}) copy-start(bf16[8,256,128]{2,1,0:T(8,128)(2,1)S(1)} %all_to_all.39.mine) | copy-start | bytes 1572868
  162.7 9.5 %collective-permute-start = (bf16[8,256,128]{2,1,0:T(8,128)(2,1)S(1)}, bf16[8,256,128]{2,1,0:T(8,128)(2,1)S(1)}, u32[]{:S(2)}, u32[]{:S(2)}) collective-permute-start(bf16[8,256,128]{2,1,0:T(8,128)(2,1)S(1)} %all_to_all.39.mine), channel_id=1, source_target_pairs={{0,1},{1,0},{2,3},{3,2},{4,5},{5,4},{6,7},{7,6},{8,9},{9,8},{10,11... | collective-permute-start | bytes 1572872 | tf_op jit(solution)/shard_map/ppermute | solution.py:222
  168.4 13.7 %all-to-all-start.5 = ((bf16[32,16,128]{2,1,0:T(8,128)(2,1)}), bf16[32,16,128]{2,1,0:T(8,128)(2,1)S(1)}, u32[]{:S(2)}, u32[]{:S(2)}) async-start(bf16[32,16,128]{2,1,0:T(8,128)(2,1)} %bitcast.16), calls=%async_computation.5 | async-start | bytes 262144 | tf_op jit(solution)/shard_map/all_to_all | solution.py:218
  172.2 0.8 copy-start.4
  182.1 0.7 copy-start.5
Sparse Core Ops, SparseCore 0:
  23.0 44.7 all-gather.4
  89.5 40.5 all-gather.6

commit v2 on v1

--- a/solution.py
+++ b/solution.py
@@ -16,7 +16,6 @@
 SILU_SHARPNESS = 1.702
 LOG2E = 1.4426950408889634
 PAD = 16
-UNROLL = 4
 
 
 def dot(a, b, dims=((1,), (0,)), precision=None):
@@ -65,7 +64,9 @@
     numbers = mix_rows[...].astype(jnp.float32)
     factor = row_factor(jnp.sum(numbers * numbers, axis=1, keepdims=True), numbers.shape[1])
     normed = (numbers * factor * gain[...][None].astype(jnp.float32)).astype(jnp.bfloat16)
-    queries[...] = dot(normed, w_query[...], ((1,), (1,))).astype(jnp.bfloat16)
+    half = positions // 2
+    asked = dot(normed, w_query[...], ((1,), (1,))).astype(jnp.bfloat16)
+    queries[...] = jnp.concatenate([asked[:half], asked[half:]], axis=1)
     keys = dot(normed, w_key[...], ((1,), (1,)))
     values = dot(normed, w_value[...], ((1,), (1,)))
     pairs = jnp.concatenate([keys, values], axis=1).astype(payload.dtype)
@@ -82,20 +83,42 @@
         out[k, hidden:, :] = w_out[:, at]
 
 
-def attend_kernel(own_ref, queries, pairs, offsets, out):
-    own = own_ref[0]
-    rows, head = queries.shape
-    q = queries[...]
+def relay_kernel(payload, queries, out):
+    across = payload.shape[0]
+    along = out.shape[0]
+    half = queries.shape[0]
+    positions = 2 * half
+    own = queries[...]
+    for z in range(along):
+        at = slice(positions + z * PAD, positions + (z + 1) * PAD)
+        for x in range(across):
+            out[z, x * PAD : (x + 1) * PAD, :] = payload[x, at, :]
+        out[z, across * PAD :, :] = own
+
+
+def identity(size):
+    row = lax.broadcasted_iota(jnp.int32, (size, size), 0)
+    return jnp.where(row == lax.broadcasted_iota(jnp.int32, (size, size), 1), 1.0, 0.0)
+
+
+def attend_kernel(where_ref, payload, asked, offsets, out):
+    z, x = where_ref[0], where_ref[1]
+    across = payload.shape[0]
+    along = asked.shape[0]
+    half = asked.shape[1] - across * PAD
+    rows = 2 * half
+    head = asked.shape[2] // 2
     visible = lax.broadcasted_iota(jnp.int32, (rows, rows), 1) < lax.broadcasted_iota(
         jnp.int32, (rows, rows), 0
     )
     after = jnp.where(visible, -1.0, 0.0).astype(jnp.bfloat16)
-
-    def front(j, diagonal):
-        pair = pairs[j]
-        offset = offsets[:, pl.ds(pl.multiple_of(j * rows, rows), rows)]
+    turn = identity(rows).astype(jnp.bfloat16)
+
+    def front(q, j, diagonal):
+        pair = payload[j, :rows, :]
+        at = pl.multiple_of((z * across + j) * rows, rows)
         s = dot(q, pair[:, :head], ((1,), (1,)))
-        s = s * (LOG2E / math.sqrt(head)) + offset * LOG2E
+        s = s * (LOG2E / math.sqrt(head)) + offsets[:, pl.ds(at, rows)] * LOG2E
         soft = jnp.log2(1.0 + jnp.exp2(-jnp.abs(s)))
         take = jnp.minimum(s, 0.0) - soft
         cost = jnp.maximum(s, 0.0) + soft
@@ -112,22 +135,61 @@
             w = jnp.where(visible, w, 0.0)
         return later + total, acc + dot(w.astype(jnp.bfloat16), values)
 
-    def group(j, count, state):
-        ahead = [front(j - i, False) for i in range(count)]
+    def asked_by(block):
+        both = asked[block, across * PAD :, :]
+        return jnp.concatenate([both[:, :head], both[:, head:]], axis=0)
+
+    def send(block, state):
+        later, acc = state
+        acc = acc.astype(out.dtype)
+        out[block, :half, :] = jnp.concatenate([acc[:half], acc[half:]], axis=1)
+        high = later.astype(jnp.bfloat16)
+        low = (later - high.astype(jnp.float32)).astype(jnp.bfloat16)
+        wide = (rows, PAD // 2)
+        parts = [jnp.broadcast_to(high, wide), jnp.broadcast_to(low, wide)]
+        parts = dot(jnp.concatenate(parts, axis=1), turn, ((0,), (0,))).astype(out.dtype)
+        out[block, half : half + PAD, :] = parts[:, :half]
+        out[block, half + PAD :, :] = parts[:, half:]
+
+    start = (jnp.zeros((rows, 1), jnp.float32), jnp.zeros((rows, head), jnp.float32))
+
+    def nothing(block, carry):
+        out[block] = jnp.zeros(out.shape[1:], out.dtype)
+        return carry
+
+    def everything(block, carry):
+        q = asked_by(block)
+        state = start
+        ahead = [front(q, across - 1 - i, False) for i in range(across)]
         for one in ahead:
             state = back(one, state, False)
-        return state
-
-    state = (jnp.zeros((rows, 1), jnp.float32), jnp.zeros((rows, head), jnp.float32))
-    state = back(front(own, True), state, True)
-    rest = own % UNROLL
-    state = lax.fori_loop(0, rest, lambda i, c: group(own - 1 - i, 1, c), state)
-    state = lax.fori_loop(
-        0, own // UNROLL, lambda i, c: group(own - 1 - rest - i * UNROLL, UNROLL, c), state
-    )
-    half = rows // 2
-    acc = state[1].astype(out.dtype)
-    out[...] = jnp.concatenate([acc[:half], acc[half:]], axis=1)
+        send(block, state)
+        return carry
+
+    lax.fori_loop(0, z, nothing, 0)
+    q = asked_by(z)
+    state = back(front(q, x, True), start, True)
+    state = lax.fori_loop(0, x, lambda i, c: back(front(q, x - 1 - i, False), c, False), state)
+    send(z, state)
+    lax.fori_loop(z + 1, along, everything, 0)
+
+
+def gather_kernel(partial, out):
+    along, _, width = partial.shape
+    half, head = width, width // 2
+    rows = 2 * half
+    turn = identity(rows).astype(jnp.bfloat16)
+    later = jnp.zeros((rows, 1), jnp.float32)
+    total = jnp.zeros((rows, head), jnp.float32)
+    for g in range(along - 1, -1, -1):
+        both = partial[g, :half, :].astype(jnp.float32)
+        both = jnp.concatenate([both[:, :head], both[:, head:]], axis=0)
+        total = total + jnp.exp2(later) * both
+        parts = [partial[g, half : half + PAD, :], partial[g, half + PAD :, :]]
+        parts = dot(turn, jnp.concatenate(parts, axis=1), ((1,), (1,)))
+        later = later + (parts[:, :1] + parts[:, PAD // 2 : PAD // 2 + 1])
+    total = total.astype(out.dtype)
+    out[...] = jnp.concatenate([total[:half], total[half:]], axis=1)
 
 
 def mix_columns_kernel(attended, weights, out):
@@ -137,8 +199,11 @@
     side = jnp.concatenate([weights[k, skip:, :] for k in range(parts)], axis=0)
     top = jnp.concatenate([attended[k][:, :head] for k in range(parts)], axis=1)
     low = jnp.concatenate([attended[k][:, head:] for k in range(parts)], axis=1)
-    out[:half, :] = dot(top, side).astype(out.dtype)
-    out[half:, :] = dot(low, side).astype(out.dtype)
+    top = dot(top, side).astype(out.dtype)
+    low = dot(low, side).astype(out.dtype)
+    for copy in range(out.shape[0]):
+        out[copy, :half, :] = top
+        out[copy, half:, :] = low
 
 
 def mix_norm_kernel(core_ref, mine, theirs, gain, out):
@@ -160,26 +225,24 @@
             out[:, at] = (numbers * factor * scale[:, at]).astype(out.dtype)
 
 
-def expert_kernel(core_ref, mine, theirs, w_gate, w_up, out, normed):
-    core = core_ref[0]
-    groups, padded, width = mine.shape
+def expert_kernel(arrived, w_gate, w_up, out, scaled, both):
+    parts, padded, width = arrived.shape
     rows = padded - PAD
+    hidden = w_gate.shape[2]
+    both[:, :hidden] = w_gate[0]
+    both[:, hidden:] = w_up[0]
     total = jnp.zeros((rows, width), jnp.float32)
-    for k in range(groups):
-        for side in (mine, theirs):
-            numbers = side[k, :rows, :].astype(jnp.float32)
-            total = total + numbers * numbers
-    factor = row_factor(jnp.sum(total, axis=1, keepdims=True), 2 * groups * width)
-    for k in range(groups):
-        for side, which in ((mine, core), (theirs, 1 - core)):
-            at = pl.ds(pl.multiple_of((2 * k + which) * width, width), width)
-            gain = side[k, rows : rows + 1, :].astype(jnp.float32)
-            numbers = side[k, :rows, :].astype(jnp.float32) * factor * gain
-            normed[:, at] = numbers.astype(jnp.bfloat16)
-    gate = jnp.minimum(dot(normed[...], w_gate[0]), CLAMP_LIMIT)
-    up = jnp.clip(dot(normed[...], w_up[0]), -CLAMP_LIMIT, CLAMP_LIMIT)
-    hidden = (up + 1.0) * (gate * jax.nn.sigmoid(SILU_SHARPNESS * gate))
-    out[...] = hidden.astype(out.dtype)
+    for k in range(parts):
+        numbers = arrived[k, :rows, :].astype(jnp.float32)
+        total = total + numbers * numbers
+        gain = arrived[k, rows : rows + 1, :].astype(jnp.float32)
+        scaled[:, k * width : (k + 1) * width] = (numbers * gain).astype(jnp.bfloat16)
+    factor = row_factor(jnp.sum(total, axis=1, keepdims=True), parts * width)
+    pre = dot(scaled[...], both[...]) * factor
+    gate = jnp.minimum(pre[:, :hidden], CLAMP_LIMIT)
+    up = jnp.clip(pre[:, hidden:], -CLAMP_LIMIT, CLAMP_LIMIT)
+    units = (up + 1.0) * (gate * jax.nn.sigmoid(SILU_SHARPNESS * gate))
+    out[...] = units.astype(out.dtype)
 
 
 def down_kernel(hidden, weights, out):
@@ -207,11 +270,6 @@
     spaces = [pltpu.SMEM] * scalars + [pltpu.VMEM] * (len(args) - scalars)
     specs = [pl.BlockSpec(memory_space=space) for space in spaces]
     return pl.pallas_call(body, out_shape=outs, in_specs=specs, **kwargs)(*args)
-
-
-def stacked(value, axis):
-    copies = jnp.broadcast_to(value, (lax.axis_size(axis), *value.shape))
-    return exchanged(copies, axis)
 
 
 def exchanged(value, axis):
@@ -251,16 +309,17 @@
     rows = mix_rows.shape[0]
     head = w_query.shape[0]
     model = mix_rows.shape[1]
-    own = lax.axis_index(EP).astype(jnp.int32)[None]
+    own = jnp.stack([lax.axis_index("ep_0"), lax.axis_index("ep_1")]).astype(jnp.int32)
     core = lax.axis_index("tp_1").astype(jnp.int32)[None]
 
     across = lax.axis_size("ep_1")
-    height = rows + slots // across
+    along = lax.axis_size("ep_0")
+    half = rows // 2
     queries, payload, table = call(
         prepare_kernel,
         (
-            shape((rows, head), bf16),
-            shape((across, height, part), bf16),
+            shape((half, 2 * head), bf16),
+            shape((across, rows + along * capacity, part), bf16),
             shape((slots, tokens), jnp.float32),
         ),
         routes.T,
@@ -273,12 +332,14 @@
         w_value,
     )
     payload = exchanged(payload, "ep_1")
-    pairs = payload[:, :rows]
-    every_pair = lax.all_gather(pairs, "ep_0", axis=0, tiled=True)
-    outgoing = payload[:, rows:].reshape(across, -1, capacity, part).swapaxes(0, 1)
-    arrived = exchanged(outgoing, "ep_0").reshape(slots, part)
+    asked = call(
+        relay_kernel, shape((along, across * capacity + half, part), bf16), payload, queries
+    )
+    asked = exchanged(asked, "ep_0")
+    arrived = asked[:, : across * capacity].reshape(slots, part)
     gain_rows = jnp.broadcast_to(exp_gain[None], (PAD, part))
-    mine = stacked(jnp.concatenate([arrived, gain_rows], axis=0), "tp_0")
+    every_row = jnp.concatenate([arrived, gain_rows], axis=0)
+    every_row = lax.all_gather(every_row, TP, axis=0)
 
     columns = call(
         columns_kernel,
@@ -288,36 +349,43 @@
     )
     columns = exchanged(columns, TP)
 
+    partial = call(
+        attend_kernel,
+        shape((along, half + 2 * PAD, 2 * head), bf16),
+        own,
+        payload,
+        asked,
+        key_offset,
+        scalars=1,
+    )
+    partial = exchanged(partial, "ep_0")
+    attended = call(gather_kernel, shape((half, 2 * head), bf16), partial)
+
+    units = w_gate.shape[2]
     hidden = call(
         expert_kernel,
-        shape((slots, w_gate.shape[2]), bf16),
-        core,
-        mine,
-        from_partner(mine),
+        shape((slots, units), bf16),
+        every_row,
         w_gate,
         w_up,
-        scalars=1,
-        scratch_shapes=[pltpu.VMEM((slots, model), bf16)],
+        scratch_shapes=[
+            pltpu.VMEM((slots, model), bf16),
+            pltpu.VMEM((model, 2 * units), bf16),
+        ],
     )
     every_hidden = lax.all_gather(hidden, TP, axis=0)
     expert_out = call(down_kernel, shape((slots, part), bf16), every_hidden, columns)
     returned = exchanged(expert_out, EP)
     exp_out = call(combine_kernel, shape((tokens, part), bf16), table, returned)
 
-    attended = call(
-        attend_kernel,
-        shape((rows // 2, 2 * head), bf16),
-        own,
-        queries,
-        every_pair,
-        key_offset,
-        scalars=1,
-    )
     every_head = lax.all_gather(attended, TP, axis=0)
     own_columns = call(
-        mix_columns_kernel, shape((rows, model // tp_count), bf16), every_head, columns
-    )
-    mine = stacked(own_columns, "tp_0")
+        mix_columns_kernel,
+        shape((tp_count // 2, rows, model // tp_count), bf16),
+        every_head,
+        columns,
+    )
+    mine = exchanged(own_columns, "tp_0")
     mix_out = call(
         mix_norm_kernel,
         shape((rows, model), bf16),

time: 192 us -> 218 us (1.14)
  waiting for transfers between devices: 8.7 us -> 57.7 us
  blocking collectives: 122 us -> 89.8 us
  Pallas kernels: 23.8 us -> 33.7 us
  local copies, waits for them, and re-layouts: 5.11 us -> 2.33 us
    all_gather x1, waiting for transfers between devices: 0.01 us -> 39.7 us  [on_device(): every_row = lax.all_gather(every_row, TP, axis=0)]
    all_to_all x4 -> x3, blocking collectives: 83.6 us -> 57.3 us  [exchanged(): return lax.all_to_all(value, axis, 0, 0, tiled=True)]
    all_to_all x2 -> x3, waiting for transfers between devices: 6.33 us -> 17.9 us  [exchanged(): return lax.all_to_all(value, axis, 0, 0, tiled=True)]
    pallas_call x8 -> x10, Pallas kernels: 23.8 us -> 33.7 us  [call(): return pl.pallas_call(body, out_shape=outs, in_specs=specs, **kwargs)(*args)]
    all_to_all x2 -> x3, starting transfers between devices: 7.62 us -> 15.5 us  [exchanged(): return lax.all_to_all(value, axis, 0, 0, tiled=True)]
    ppermute x2 -> x1, starting transfers between devices: 9.76 us -> 2.49 us  [from_partner(): return lax.ppermute(value, 'tp_1', [(0, 1), (1, 0)])]
    all_gather x1, blocking collectives: 38.6 us -> 32.5 us  [on_device(): every_head = lax.all_gather(attended, TP, axis=0)]
    ppermute x2 -> x1, waiting for transfers between devices: 2.31 us -> 0.01 us  [from_partner(): return lax.ppermute(value, 'tp_1', [(0, 1), (1, 0)])]
  transfers between devices with their start and end apart: 6 -> 6, of which waited for: 2 -> 3; matrix products, arithmetic and copies ran while one was open for 1% -> 0% of each run, Pallas kernels for 10% -> 10%
where the time goes in v2:
time: 218 us; the launch traced here: 217 us
  blocking collectives  89.8 us (41%)
  waiting for transfers between devices  57.7 us (26%)
  Pallas kernels  33.7 us (15%)
  starting transfers between devices  18 us (8%)
  between operations  14.1 us (6%)
  local copies, waits for them, and re-layouts  2.33 us (1%)
    all_to_all x3, blocking collectives, exchanged(): return lax.all_to_all(value, axis, 0, 0, tiled=True)  57.3 us
    all_gather x1, waiting for transfers between devices, on_device(): every_row = lax.all_gather(every_row, TP, axis=0)  39.7 us
    pallas_call x10, Pallas kernels, call(): return pl.pallas_call(body, out_shape=outs, in_specs=specs, **kwargs)(*args)  33.7 us
    all_gather x1, blocking collectives, on_device(): every_head = lax.all_gather(attended, TP, axis=0)  32.5 us
    all_to_all x3, waiting for transfers between devices, exchanged(): return lax.all_to_all(value, axis, 0, 0, tiled=True)  17.9 us
    all_to_all x3, starting transfers between devices, exchanged(): return lax.all_to_all(value, axis, 0, 0, tiled=True)  15.5 us
  transfers between devices with their start and end apart: 6, of which 3 were waited for; matrix products, arithmetic and copies ran while one was open for 0% of the time, Pallas kernels for 10%

profile of v2, /device:TPU:1, one launch (start us, length us, event | category | flops | bytes accessed | tf_op | source)
XLA Modules:
  0.0 217.0 jit_solution(274636692821717020)
XLA Ops:
  7.2 3.8 %shard_map.158 = (bf16[128,128]{1,0:T(8,128)(2,1)}, bf16[4,384,128]{2,1,0:T(8,128)(2,1)}, f32[512,96]{1,0:T(8,128)}) custom-call(s32[4,96]{1,0:T(4,128)} %bitcast.17, f32[4,96]{1,0:T(4,128)} %bitcast.18, bf16[96,128]{1,0:T(8,128)(2,1)} %rows.1, bf16[256,2048]{1,0:T(8,128)(2,1)} %mix_rows.1, bf16[2048]{0:T(1024)(128)(2,1)} %gain.2, bf16[64,2048]{1,0:T(8,128)(2,1)} %w_query.1, ...), custom_call_target="tpu_custom_call" | custom-call | tf_op jit(solution)/shard_map/pallas_call | solution.py:272
  11.0 11.2 %all_to_all.36.payload = bf16[4,384,128]{2,1,0:T(8,128)(2,1)} all-to-all(bf16[4,384,128]{2,1,0:T(8,128)(2,1)} %get-tuple-element.5), channel_id=1, replica_groups=mesh['ep_0'=8,'ep_1'=4,'tp_0'=8,'tp_1'=2] {'ep_1'}, dimensions={0} | all-to-all | bytes 786432 | tf_op jit(solution)/shard_map/all_to_all | solution.py:276
  22.1 1.8 shard_map.159
  23.9 22.8 %all_to_all.37.asked = bf16[8,192,128]{2,1,0:T(8,128)(2,1)S(1)} all-to-all(bf16[8,192,128]{2,1,0:T(8,128)(2,1)} %shard_map.159), channel_id=1, replica_groups=mesh['ep_0'=8,'ep_1'=4,'tp_0'=8,'tp_1'=2] {'ep_0'}, dimensions={0} | all-to-all | bytes 786432 | tf_op jit(solution)/shard_map/all_to_all | solution.py:276
  46.7 0.7 pad_maximum_fusion
  47.6 39.7 %all-gather.6.cloned.1.call-done = bf16[8448,128]{1,0:T(8,128)(2,1)} async-done(((bf16[528,128]{1,0:T(8,128)(2,1)}), bf16[8448,128]{1,0:T(8,128)(2,1)}) %all-gather.6.cloned.1.call-update) | async-done | bytes 2162704 | tf_op jit(solution)/shard_map/all_gather | solution.py:342
  87.3 3.8 %shard_map.165 = bf16[512,128]{1,0:T(8,128)(2,1)} custom-call(bf16[16,528,128]{2,1,0:T(8,128)(2,1)} %bitcast.11, bf16[1,2048,128]{2,1,0:T(8,128)(2,1)} %w_gate.1, bf16[1,2048,128]{2,1,0:T(8,128)(2,1)} %w_up.1), custom_call_target="tpu_custom_call" | custom-call | tf_op jit(solution)/shard_map/pallas_call | solution.py:272
  91.7 9.6 %shard_map.160 = bf16[8,160,128]{2,1,0:T(8,128)(2,1)} custom-call(s32[2]{0:T(128)} %pad_add_fusion.where_ref, bf16[4,384,128]{2,1,0:T(8,128)(2,1)} %all_to_all.36.payload, bf16[8,192,128]{2,1,0:T(8,128)(2,1)} %copy-done.1, f32[1,8192]{1,0:T(1,128)} %offsets.1), custom_call_target="tpu_custom_call" | custom-call | tf_op jit(solution)/shard_map/pallas_call | solution.py:272
  101.3 3.4 %all-to-all-start.2 = ((bf16[8,160,128]{2,1,0:T(8,128)(2,1)}), bf16[8,160,128]{2,1,0:T(8,128)(2,1)S(1)}, u32[]{:S(2)}, u32[]{:S(2)}) async-start(bf16[8,160,128]{2,1,0:T(8,128)(2,1)} %shard_map.160), calls=%async_computation.2 | async-start | bytes 655360 | tf_op jit(solution)/shard_map/all_to_all | solution.py:276
  104.8 2.1 shard_map.162
  106.9 11.5 %all-to-all-done.2.partial = bf16[8,160,128]{2,1,0:T(8,128)(2,1)S(1)} async-done(((bf16[8,160,128]{2,1,0:T(8,128)(2,1)}), bf16[8,160,128]{2,1,0:T(8,128)(2,1)S(1)}, u32[]{:S(2)}, u32[]{:S(2)}) %all-to-all-start.2) | async-done | bytes 327712 | tf_op jit(solution)/shard_map/all_to_all | solution.py:276
  118.4 5.0 %all-to-all-start.3 = ((bf16[16,192,128]{2,1,0:T(8,128)(2,1)}), bf16[16,192,128]{2,1,0:T(8,128)(2,1)S(1)}, u32[]{:S(2)}, u32[]{:S(2)}) async-start(bf16[16,192,128]{2,1,0:T(8,128)(2,1)} %shard_map.162), calls=%async_computation.3 | async-start | bytes 1572864 | tf_op jit(solution)/shard_map/all_to_all | solution.py:276
  123.5 2.4 %shard_map.161 = bf16[128,128]{1,0:T(8,128)(2,1)} custom-call(bf16[8,160,128]{2,1,0:T(8,128)(2,1)} %copy-done.3), custom_call_target="tpu_custom_call" | custom-call | tf_op jit(solution)/shard_map/pallas_call | solution.py:272
  125.9 32.5 %all-gather = bf16[2048,128]{1,0:T(8,128)(2,1)} all-gather(bf16[128,128]{1,0:T(8,128)(2,1)} %shard_map.161), channel_id=2, replica_groups=mesh['ep_0'=8,'ep_1'=4,'tp_0'=8,'tp_1'=2] {'tp_0','tp_1'}, dimensions={0}, use_global_device_ids=true | all-gather | bytes 557056 | tf_op jit(solution)/shard_map/all_gather | solution.py:381
  158.4 0.9 copy-done
  159.3 2.4 %shard_map.163 = bf16[8,256,128]{2,1,0:T(8,128)(2,1)} custom-call(bf16[16,128,128]{2,1,0:T(8,128)(2,1)} %bitcast.12, bf16[16,192,128]{2,1,0:T(8,128)(2,1)} %copy-done), custom_call_target="tpu_custom_call" | custom-call | tf_op jit(solution)/shard_map/pallas_call | solution.py:272
  161.7 23.3 %all_to_all.38.mine = bf16[8,256,128]{2,1,0:T(8,128)(2,1)S(1)} all-to-all(bf16[8,256,128]{2,1,0:T(8,128)(2,1)} %shard_map.163), channel_id=1, replica_groups=mesh['ep_0'=8,'ep_1'=4,'tp_0'=8,'tp_1'=2] {'tp_0'}, dimensions={0} | all-to-all | bytes 1048576 | tf_op jit(solution)/shard_map/all_to_all | solution.py:276
  185.1 2.5 %collective-permute-start = (bf16[8,256,128]{2,1,0:T(8,128)(2,1)S(1)}, bf16[8,256,128]{2,1,0:T(8,128)(2,1)S(1)}, u32[]{:S(2)}, u32[]{:S(2)}) collective-permute-start(bf16[8,256,128]{2,1,0:T(8,128)(2,1)S(1)} %all_to_all.38.mine), channel_id=1, source_target_pairs={{0,1},{1,0},{2,3},{3,2},{4,5},{5,4},{6,7},{7,6},{8,9},{9,8},{10,11... | collective-permute-start | bytes 1572872 | tf_op jit(solution)/shard_map/ppermute | solution.py:280
  187.6 3.1 %shard_map.166 = bf16[512,128]{1,0:T(8,128)(2,1)} custom-call(bf16[16,512,128]{2,1,0:T(8,128)(2,1)} %bitcast.13, bf16[16,192,128]{2,1,0:T(8,128)(2,1)} %copy-done), custom_call_target="tpu_custom_call" | custom-call | tf_op jit(solution)/shard_map/pallas_call | solution.py:272
  190.7 7.0 %all-to-all-start.5 = ((bf16[32,16,128]{2,1,0:T(8,128)(2,1)}), bf16[32,16,128]{2,1,0:T(8,128)(2,1)S(1)}, u32[]{:S(2)}, u32[]{:S(2)}) async-start(bf16[32,16,128]{2,1,0:T(8,128)(2,1)} %bitcast.15), calls=%async_computation.5 | async-start | bytes 262144 | tf_op jit(solution)/shard_map/all_to_all | solution.py:276
  197.8 0.8 copy-done.4
  198.5 2.7 %shard_map.164 = bf16[256,2048]{1,0:T(8,128)(2,1)} custom-call(s32[1]{0:T(128)} %bitcast.core_ref, bf16[8,256,128]{2,1,0:T(8,128)(2,1)} %copy-done.2, bf16[8,256,128]{2,1,0:T(8,128)(2,1)} %copy-done.4, bf16[2048]{0:T(1024)(128)(2,1)} %gain.3), custom_call_target="tpu_custom_call" | custom-call | tf_op jit(solution)/shard_map/pallas_call | solution.py:272
  201.3 6.4 %all-to-all-done.5 = bf16[32,16,128]{2,1,0:T(8,128)(2,1)S(1)} async-done(((bf16[32,16,128]{2,1,0:T(8,128)(2,1)}), bf16[32,16,128]{2,1,0:T(8,128)(2,1)S(1)}, u32[]{:S(2)}, u32[]{:S(2)}) %all-to-all-start.5) | async-done | bytes 131104 | tf_op jit(solution)/shard_map/all_to_all | solution.py:276
  208.3 1.9 shard_map.167
  (22 shorter events, 1.4 us)
Async XLA Ops:
  7.2 80.1 %all-gather.6.cloned.1.call-start = ((), (), s32[]{:S(2)}) async-start(), calls=%async_computation.6 | async-start | bytes 2297856 | tf_op jit(solution)/shard_map/all_gather | solution.py:342
  7.2 39.5 %copy-start.6 = (bf16[128]{0:T(256)(128)(2,1)S(1)}, bf16[128]{0:T(256)(128)(2,1)}, u32[]{:S(2)}) copy-start(bf16[128]{0:T(256)(128)(2,1)} %param.24) | copy-start | bytes 772
  46.7 45.0 %copy-start.1 = (bf16[8,192,128]{2,1,0:T(8,128)(2,1)}, bf16[8,192,128]{2,1,0:T(8,128)(2,1)S(1)}, u32[]{:S(2)}) copy-start(bf16[8,192,128]{2,1,0:T(8,128)(2,1)S(1)} %all_to_all.37.asked) | copy-start | bytes 1179652
  47.5 140.1 %all-gather.8.cloned.1.call-start = ((), (), s32[]{:S(2)}) async-start(), calls=%async_computation.7 | async-start | bytes 2228224 | tf_op jit(solution)/shard_map/all_gather | solution.py:376
  101.3 17.1 %all-to-all-start.2 = ((bf16[8,160,128]{2,1,0:T(8,128)(2,1)}), bf16[8,160,128]{2,1,0:T(8,128)(2,1)S(1)}, u32[]{:S(2)}, u32[]{:S(2)}) async-start(bf16[8,160,128]{2,1,0:T(8,128)(2,1)} %shard_map.160), calls=%async_computation.2 | async-start | bytes 655360 | tf_op jit(solution)/shard_map/all_to_all | solution.py:276
  118.4 5.0 %copy-start.3 = (bf16[8,160,128]{2,1,0:T(8,128)(2,1)}, bf16[8,160,128]{2,1,0:T(8,128)(2,1)S(1)}, u32[]{:S(2)}) copy-start(bf16[8,160,128]{2,1,0:T(8,128)(2,1)S(1)} %all-to-all-done.2.partial) | copy-start | bytes 983044
  118.4 40.0 %all-to-all-start.3 = ((bf16[16,192,128]{2,1,0:T(8,128)(2,1)}), bf16[16,192,128]{2,1,0:T(8,128)(2,1)S(1)}, u32[]{:S(2)}, u32[]{:S(2)}) async-start(bf16[16,192,128]{2,1,0:T(8,128)(2,1)} %shard_map.162), calls=%async_computation.3 | async-start | bytes 1572864 | tf_op jit(solution)/shard_map/all_to_all | solution.py:276
  158.4 0.9 copy-start
  185.1 12.7 %copy-start.2 = (bf16[8,256,128]{2,1,0:T(8,128)(2,1)}, bf16[8,256,128]{2,1,0:T(8,128)(2,1)S(1)}, u32[]{:S(2)}) copy-start(bf16[8,256,128]{2,1,0:T(8,128)(2,1)S(1)} %all_to_all.38.mine) | copy-start | bytes 1572868
  185.1 12.7 %collective-permute-start = (bf16[8,256,128]{2,1,0:T(8,128)(2,1)S(1)}, bf16[8,256,128]{2,1,0:T(8,128)(2,1)S(1)}, u32[]{:S(2)}, u32[]{:S(2)}) collective-permute-start(bf16[8,256,128]{2,1,0:T(8,128)(2,1)S(1)} %all_to_all.38.mine), channel_id=1, source_target_pairs={{0,1},{1,0},{2,3},{3,2},{4,5},{5,4},{6,7},{7,6},{8,9},{9,8},{10,11... | collective-permute-start | bytes 1572872 | tf_op jit(solution)/shard_map/ppermute | solution.py:280
  190.7 16.9 %all-to-all-start.5 = ((bf16[32,16,128]{2,1,0:T(8,128)(2,1)}), bf16[32,16,128]{2,1,0:T(8,128)(2,1)S(1)}, u32[]{:S(2)}, u32[]{:S(2)}) async-start(bf16[32,16,128]{2,1,0:T(8,128)(2,1)} %bitcast.15), calls=%async_computation.5 | async-start | bytes 262144 | tf_op jit(solution)/shard_map/all_to_all | solution.py:276
  197.7 0.8 copy-start.4
  207.7 0.6 copy-start.5
Sparse Core Ops, SparseCore 0:
  47.6 39.6 all-gather.5
  91.3 43.2 all-gather.7

commit v3 on v2

--- a/solution.py
+++ b/solution.py
@@ -29,17 +29,13 @@
 
 
 def prepare_kernel(
-    routes, weight, rows, mix_rows, gain, w_query, w_key, w_value, queries, payload, table
+    routes, weight, rows, mix_rows, gain, w_query, w_key, w_value, asked, pairs, outgoing, table
 ):
     top, tokens = routes.shape
     slots = table.shape[0]
-    across, _, _ = payload.shape
-    positions = mix_rows.shape[0]
-    along = slots // (across * PAD)
-    capacity = PAD
     slot = lax.broadcasted_iota(jnp.int32, (slots, tokens), 0)
-    expert_of = slot // capacity
-    place_of = slot - expert_of * capacity
+    expert_of = slot // PAD
+    place_of = slot - expert_of * PAD
     named = jnp.zeros((slots, tokens), jnp.float32)
     scale = jnp.zeros((slots, tokens), jnp.float32)
     for k in range(top):
@@ -54,24 +50,19 @@
     mine = (named > 0.0) & (place == place_of.astype(jnp.float32))
     table[...] = jnp.where(mine, scale, 0.0)
     chosen = jnp.where(mine, 1.0, 0.0).astype(jnp.bfloat16)
-    outgoing = dot(chosen, rows[...]).astype(payload.dtype)
-    for x in range(across):
-        for z in range(along):
-            at = (z * across + x) * capacity
-            to = positions + z * capacity
-            payload[x, to : to + capacity, :] = outgoing[at : at + capacity]
+    outgoing[...] = dot(chosen, rows[...]).astype(outgoing.dtype)
 
     numbers = mix_rows[...].astype(jnp.float32)
     factor = row_factor(jnp.sum(numbers * numbers, axis=1, keepdims=True), numbers.shape[1])
     normed = (numbers * factor * gain[...][None].astype(jnp.float32)).astype(jnp.bfloat16)
-    half = positions // 2
-    asked = dot(normed, w_query[...], ((1,), (1,))).astype(jnp.bfloat16)
-    queries[...] = jnp.concatenate([asked[:half], asked[half:]], axis=1)
+    queries = dot(normed, w_query[...], ((1,), (1,))).astype(asked.dtype)
+    half = queries.shape[0] // 2
+    queries = jnp.concatenate([queries[:half], queries[half:]], axis=1)
+    for copy in range(asked.shape[0]):
+        asked[copy] = queries
     keys = dot(normed, w_key[...], ((1,), (1,)))
     values = dot(normed, w_value[...], ((1,), (1,)))
-    pairs = jnp.concatenate([keys, values], axis=1).astype(payload.dtype)
-    for x in range(across):
-        payload[x, :positions, :] = pairs
+    pairs[...] = jnp.concatenate([keys, values], axis=1).astype(pairs.dtype)
 
 
 def columns_kernel(w_down, w_out, out):
@@ -83,29 +74,15 @@
         out[k, hidden:, :] = w_out[:, at]
 
 
-def relay_kernel(payload, queries, out):
-    across = payload.shape[0]
-    along = out.shape[0]
-    half = queries.shape[0]
-    positions = 2 * half
-    own = queries[...]
-    for z in range(along):
-        at = slice(positions + z * PAD, positions + (z + 1) * PAD)
-        for x in range(across):
-            out[z, x * PAD : (x + 1) * PAD, :] = payload[x, at, :]
-        out[z, across * PAD :, :] = own
-
-
 def identity(size):
     row = lax.broadcasted_iota(jnp.int32, (size, size), 0)
     return jnp.where(row == lax.broadcasted_iota(jnp.int32, (size, size), 1), 1.0, 0.0)
 
 
-def attend_kernel(where_ref, payload, asked, offsets, out):
+def attend_kernel(where_ref, pairs, asked, offsets, out):
     z, x = where_ref[0], where_ref[1]
-    across = payload.shape[0]
-    along = asked.shape[0]
-    half = asked.shape[1] - across * PAD
+    across = pairs.shape[0]
+    along, half = asked.shape[:2]
     rows = 2 * half
     head = asked.shape[2] // 2
     visible = lax.broadcasted_iota(jnp.int32, (rows, rows), 1) < lax.broadcasted_iota(
@@ -115,7 +92,7 @@
     turn = identity(rows).astype(jnp.bfloat16)
 
     def front(q, j, diagonal):
-        pair = payload[j, :rows, :]
+        pair = pairs[j]
         at = pl.multiple_of((z * across + j) * rows, rows)
         s = dot(q, pair[:, :head], ((1,), (1,)))
         s = s * (LOG2E / math.sqrt(head)) + offsets[:, pl.ds(at, rows)] * LOG2E
@@ -136,7 +113,7 @@
         return later + total, acc + dot(w.astype(jnp.bfloat16), values)
 
     def asked_by(block):
-        both = asked[block, across * PAD :, :]
+        both = asked[block]
         return jnp.concatenate([both[:, :head], both[:, head:]], axis=0)
 
     def send(block, state):
@@ -312,14 +289,14 @@
     own = jnp.stack([lax.axis_index("ep_0"), lax.axis_index("ep_1")]).astype(jnp.int32)
     core = lax.axis_index("tp_1").astype(jnp.int32)[None]
 
-    across = lax.axis_size("ep_1")
     along = lax.axis_size("ep_0")
     half = rows // 2
-    queries, payload, table = call(
+    asked, pairs, outgoing, table = call(
         prepare_kernel,
         (
-            shape((half, 2 * head), bf16),
-            shape((across, rows + along * capacity, part), bf16),
+            shape((along, half, 2 * head), bf16),
+            shape((rows, 2 * head), bf16),
+            shape((slots, part), bf16),
             shape((slots, tokens), jnp.float32),
         ),
         routes.T,
@@ -331,12 +308,9 @@
         w_key,
         w_value,
     )
-    payload = exchanged(payload, "ep_1")
-    asked = call(
-        relay_kernel, shape((along, across * capacity + half, part), bf16), payload, queries
-    )
+    arrived = exchanged(outgoing, EP)
+    near_pairs = lax.all_gather(pairs, "ep_1", axis=0)
     asked = exchanged(asked, "ep_0")
-    arrived = asked[:, : across * capacity].reshape(slots, part)
     gain_rows = jnp.broadcast_to(exp_gain[None], (PAD, part))
     every_row = jnp.concatenate([arrived, gain_rows], axis=0)
     every_row = lax.all_gather(every_row, TP, axis=0)
@@ -353,7 +327,7 @@
         attend_kernel,
         shape((along, half + 2 * PAD, 2 * head), bf16),
         own,
-        payload,
+        near_pairs,
         asked,
         key_offset,
         scalars=1,

time: 218 us -> 222 us (1.018)
  starting transfers between devices: 18 us -> 27.5 us
  waiting for transfers between devices: 57.7 us -> 53 us
    all_gather x0 -> x1, blocking collectives: none -> 11 us  [on_device(): near_pairs = lax.all_gather(pairs, 'ep_1', axis=0)]
    all_to_all x3 -> x2, blocking collectives: 57.3 us -> 46.5 us  [exchanged(): return lax.all_to_all(value, axis, 0, 0, tiled=True)]
    all_to_all x3 -> x4, starting transfers between devices: 15.5 us -> 24.9 us  [exchanged(): return lax.all_to_all(value, axis, 0, 0, tiled=True)]
    all_to_all x3 -> x4, waiting for transfers between devices: 17.9 us -> 14.3 us  [exchanged(): return lax.all_to_all(value, axis, 0, 0, tiled=True)]
    pallas_call x10 -> x9, Pallas kernels: 33.7 us -> 31.7 us  [call(): return pl.pallas_call(body, out_shape=outs, in_specs=specs, **kwargs)(*args)]
  transfers between devices with their start and end apart: 6 -> 7, of which waited for: 3 -> 4; matrix products, arithmetic and copies ran while one was open for 0% -> 0% of each run, Pallas kernels for 10% -> 10%
where the time goes in v3:
time: 222 us; the launch traced here: 221 us
  blocking collectives  89.3 us (40%)
  waiting for transfers between devices  53 us (24%)
  Pallas kernels  31.7 us (14%)
  starting transfers between devices  27.5 us (12%)
  between operations  14.1 us (6%)
  local copies, waits for them, and re-layouts  3.69 us (2%)
    all_to_all x2, blocking collectives, exchanged(): return lax.all_to_all(value, axis, 0, 0, tiled=True)  46.5 us
    all_gather x1, waiting for transfers between devices, on_device(): every_row = lax.all_gather(every_row, TP, axis=0)  38.6 us
    all_gather x1, blocking collectives, on_device(): every_head = lax.all_gather(attended, TP, axis=0)  31.8 us
    pallas_call x9, Pallas kernels, call(): return pl.pallas_call(body, out_shape=outs, in_specs=specs, **kwargs)(*args)  31.7 us
    all_to_all x4, starting transfers between devices, exchanged(): return lax.all_to_all(value, axis, 0, 0, tiled=True)  24.9 us
    all_to_all x4, waiting for transfers between devices, exchanged(): return lax.all_to_all(value, axis, 0, 0, tiled=True)  14.3 us
    all_gather x1, blocking collectives, on_device(): near_pairs = lax.all_gather(pairs, 'ep_1', axis=0)  11 us
  transfers between devices with their start and end apart: 7, of which 4 were waited for; matrix products, arithmetic and copies ran while one was open for 0% of the time, Pallas kernels for 10%

profile of v3, /device:TPU:1, one launch (start us, length us, event | category | flops | bytes accessed | tf_op | source)
XLA Modules:
  0.0 220.6 jit_solution(8520018268449068983)
XLA Ops:
  7.2 3.7 %shard_map.158 = (bf16[8,128,128]{2,1,0:T(8,128)(2,1)}, bf16[256,128]{1,0:T(8,128)(2,1)}, bf16[512,128]{1,0:T(8,128)(2,1)}, f32[512,96]{1,0:T(8,128)}) custom-call(s32[4,96]{1,0:T(4,128)} %bitcast.21, f32[4,96]{1,0:T(4,128)} %bitcast.22, bf16[96,128]{1,0:T(8,128)(2,1)} %rows.1, bf16[256,2048]{1,0:T(8,128)(2,1)} %mix_rows.1, bf16[2048]{0:T(1024)(128)(2,1)} %gain.2, ...), custom_call_target="tpu_custom_call" | custom-call | tf_op jit(solution)/shard_map/pallas_call | solution.py:249
  10.9 23.0 %all_to_all.43 = bf16[32,16,128]{2,1,0:T(8,128)(2,1)S(1)} all-to-all(bf16[32,16,128]{2,1,0:T(8,128)(2,1)} %bitcast.20), channel_id=1, replica_groups=mesh['ep_0'=8,'ep_1'=4,'tp_0'=8,'tp_1'=2] {'ep_0','ep_1'}, dimensions={0} | all-to-all | bytes 262144 | tf_op jit(solution)/shard_map/all_to_all | solution.py:253
  35.3 38.6 %all-gather.7.cloned.1.call-done = bf16[8448,128]{1,0:T(8,128)(2,1)} async-done(((bf16[528,128]{1,0:T(8,128)(2,1)}), bf16[8448,128]{1,0:T(8,128)(2,1)}) %all-gather.7.cloned.1.call-update) | async-done | bytes 2162704 | tf_op jit(solution)/shard_map/all_gather | solution.py:316
  73.9 3.8 %shard_map.164 = bf16[512,128]{1,0:T(8,128)(2,1)} custom-call(bf16[16,528,128]{2,1,0:T(8,128)(2,1)} %bitcast.13, bf16[1,2048,128]{2,1,0:T(8,128)(2,1)} %w_gate.1, bf16[1,2048,128]{2,1,0:T(8,128)(2,1)} %w_up.1), custom_call_target="tpu_custom_call" | custom-call | tf_op jit(solution)/shard_map/pallas_call | solution.py:249
  77.8 7.1 %all-to-all-start = ((bf16[8,128,128]{2,1,0:T(8,128)(2,1)}), bf16[8,128,128]{2,1,0:T(8,128)(2,1)S(1)}, u32[]{:S(2)}, u32[]{:S(2)}) async-start(bf16[8,128,128]{2,1,0:T(8,128)(2,1)} %get-tuple-element.7), calls=%async_computation | async-start | bytes 524288 | tf_op jit(solution)/shard_map/all_to_all | solution.py:253
  84.9 11.0 %all-gather = bf16[1024,128]{1,0:T(8,128)(2,1)} all-gather(bf16[256,128]{1,0:T(8,128)(2,1)S(1)} %copy-done.6), channel_id=2, replica_groups=mesh['ep_0'=8,'ep_1'=4,'tp_0'=8,'tp_1'=2] {'ep_1'}, dimensions={0}, use_global_device_ids=true | all-gather | bytes 327680 | tf_op jit(solution)/shard_map/all_gather | solution.py:312
  96.6 0.7 copy-done.3
  97.3 9.5 %shard_map.159 = bf16[8,160,128]{2,1,0:T(8,128)(2,1)} custom-call(s32[2]{0:T(128)} %pad_add_fusion.where_ref, bf16[4,256,128]{2,1,0:T(8,128)(2,1)} %bitcast.16, bf16[8,128,128]{2,1,0:T(8,128)(2,1)} %copy-done.3, f32[1,8192]{1,0:T(1,128)} %offsets.1), custom_call_target="tpu_custom_call" | custom-call | tf_op jit(solution)/shard_map/pallas_call | solution.py:249
  106.7 3.4 %all-to-all-start.1 = ((bf16[8,160,128]{2,1,0:T(8,128)(2,1)}), bf16[8,160,128]{2,1,0:T(8,128)(2,1)S(1)}, u32[]{:S(2)}, u32[]{:S(2)}) async-start(bf16[8,160,128]{2,1,0:T(8,128)(2,1)} %shard_map.159), calls=%async_computation.1 | async-start | bytes 655360 | tf_op jit(solution)/shard_map/all_to_all | solution.py:253
  110.2 2.1 shard_map.161
  112.3 7.9 %all-to-all-done.1.partial = bf16[8,160,128]{2,1,0:T(8,128)(2,1)S(1)} async-done(((bf16[8,160,128]{2,1,0:T(8,128)(2,1)}), bf16[8,160,128]{2,1,0:T(8,128)(2,1)S(1)}, u32[]{:S(2)}, u32[]{:S(2)}) %all-to-all-start.1) | async-done | bytes 327712 | tf_op jit(solution)/shard_map/all_to_all | solution.py:253
  120.2 8.7 %all-to-all-start.2 = ((bf16[16,192,128]{2,1,0:T(8,128)(2,1)}), bf16[16,192,128]{2,1,0:T(8,128)(2,1)S(1)}, u32[]{:S(2)}, u32[]{:S(2)}) async-start(bf16[16,192,128]{2,1,0:T(8,128)(2,1)} %shard_map.161), calls=%async_computation.2 | async-start | bytes 1572864 | tf_op jit(solution)/shard_map/all_to_all | solution.py:253
  128.9 2.4 %shard_map.160 = bf16[128,128]{1,0:T(8,128)(2,1)} custom-call(bf16[8,160,128]{2,1,0:T(8,128)(2,1)} %copy-done.2), custom_call_target="tpu_custom_call" | custom-call | tf_op jit(solution)/shard_map/pallas_call | solution.py:249
  131.3 31.8 %all-gather.1 = bf16[2048,128]{1,0:T(8,128)(2,1)} all-gather(bf16[128,128]{1,0:T(8,128)(2,1)} %shard_map.160), channel_id=3, replica_groups=mesh['ep_0'=8,'ep_1'=4,'tp_0'=8,'tp_1'=2] {'tp_0','tp_1'}, dimensions={0}, use_global_device_ids=true | all-gather | bytes 557056 | tf_op jit(solution)/shard_map/all_gather | solution.py:355
  163.1 0.9 copy-done
  164.0 2.4 %shard_map.162 = bf16[8,256,128]{2,1,0:T(8,128)(2,1)} custom-call(bf16[16,128,128]{2,1,0:T(8,128)(2,1)} %bitcast.14, bf16[16,192,128]{2,1,0:T(8,128)(2,1)} %copy-done), custom_call_target="tpu_custom_call" | custom-call | tf_op jit(solution)/shard_map/pallas_call | solution.py:249
  166.5 23.5 %all_to_all.44.mine = bf16[8,256,128]{2,1,0:T(8,128)(2,1)S(1)} all-to-all(bf16[8,256,128]{2,1,0:T(8,128)(2,1)} %shard_map.162), channel_id=1, replica_groups=mesh['ep_0'=8,'ep_1'=4,'tp_0'=8,'tp_1'=2] {'tp_0'}, dimensions={0} | all-to-all | bytes 1048576 | tf_op jit(solution)/shard_map/all_to_all | solution.py:253
  190.0 2.5 %collective-permute-start = (bf16[8,256,128]{2,1,0:T(8,128)(2,1)S(1)}, bf16[8,256,128]{2,1,0:T(8,128)(2,1)S(1)}, u32[]{:S(2)}, u32[]{:S(2)}) collective-permute-start(bf16[8,256,128]{2,1,0:T(8,128)(2,1)S(1)} %all_to_all.44.mine), channel_id=1, source_target_pairs={{0,1},{1,0},{2,3},{3,2},{4,5},{5,4},{6,7},{7,6},{8,9},{9,8},{10,11... | collective-permute-start | bytes 1572872 | tf_op jit(solution)/shard_map/ppermute | solution.py:257
  192.5 3.1 %shard_map.165 = bf16[512,128]{1,0:T(8,128)(2,1)} custom-call(bf16[16,512,128]{2,1,0:T(8,128)(2,1)} %bitcast.15, bf16[16,192,128]{2,1,0:T(8,128)(2,1)} %copy-done), custom_call_target="tpu_custom_call" | custom-call | tf_op jit(solution)/shard_map/pallas_call | solution.py:249
  195.6 5.7 %all-to-all-start.5 = ((bf16[32,16,128]{2,1,0:T(8,128)(2,1)}), bf16[32,16,128]{2,1,0:T(8,128)(2,1)S(1)}, u32[]{:S(2)}, u32[]{:S(2)}) async-start(bf16[32,16,128]{2,1,0:T(8,128)(2,1)} %bitcast.18), calls=%async_computation.5 | async-start | bytes 262144 | tf_op jit(solution)/shard_map/all_to_all | solution.py:253
  201.4 0.8 copy-done.4
  202.1 2.7 %shard_map.163 = bf16[256,2048]{1,0:T(8,128)(2,1)} custom-call(s32[1]{0:T(128)} %bitcast.core_ref, bf16[8,256,128]{2,1,0:T(8,128)(2,1)} %copy-done.1, bf16[8,256,128]{2,1,0:T(8,128)(2,1)} %copy-done.4, bf16[2048]{0:T(1024)(128)(2,1)} %gain.3), custom_call_target="tpu_custom_call" | custom-call | tf_op jit(solution)/shard_map/pallas_call | solution.py:249
  204.9 6.4 %all-to-all-done.5 = bf16[32,16,128]{2,1,0:T(8,128)(2,1)S(1)} async-done(((bf16[32,16,128]{2,1,0:T(8,128)(2,1)}), bf16[32,16,128]{2,1,0:T(8,128)(2,1)S(1)}, u32[]{:S(2)}, u32[]{:S(2)}) %all-to-all-start.5) | async-done | bytes 131104 | tf_op jit(solution)/shard_map/all_to_all | solution.py:253
  211.9 1.9 shard_map.166
  (22 shorter events, 2.9 us)
Async XLA Ops:
  7.2 66.7 %all-gather.7.cloned.1.call-start = ((), (), s32[]{:S(2)}) async-start(), calls=%async_computation.6 | async-start | bytes 2297856 | tf_op jit(solution)/shard_map/all_gather | solution.py:316
  34.6 50.3 %copy-start.6 = (bf16[256,128]{1,0:T(8,128)(2,1)S(1)}, bf16[256,128]{1,0:T(8,128)(2,1)}, u32[]{:S(2)}) copy-start(bf16[256,128]{1,0:T(8,128)(2,1)} %get-tuple-element.6) | copy-start | bytes 196612
  35.3 157.2 %all-gather.9.cloned.1.call-start = ((), (), s32[]{:S(2)}) async-start(), calls=%async_computation.7 | async-start | bytes 2228224 | tf_op jit(solution)/shard_map/all_gather | solution.py:350
  77.8 18.8 %all-to-all-start = ((bf16[8,128,128]{2,1,0:T(8,128)(2,1)}), bf16[8,128,128]{2,1,0:T(8,128)(2,1)S(1)}, u32[]{:S(2)}, u32[]{:S(2)}) async-start(bf16[8,128,128]{2,1,0:T(8,128)(2,1)} %get-tuple-element.7), calls=%async_computation | async-start | bytes 524288 | tf_op jit(solution)/shard_map/all_to_all | solution.py:253
  96.6 0.7 copy-start.3
  106.7 13.5 %all-to-all-start.1 = ((bf16[8,160,128]{2,1,0:T(8,128)(2,1)}), bf16[8,160,128]{2,1,0:T(8,128)(2,1)S(1)}, u32[]{:S(2)}, u32[]{:S(2)}) async-start(bf16[8,160,128]{2,1,0:T(8,128)(2,1)} %shard_map.159), calls=%async_computation.1 | async-start | bytes 655360 | tf_op jit(solution)/shard_map/all_to_all | solution.py:253
  120.2 8.7 %copy-start.2 = (bf16[8,160,128]{2,1,0:T(8,128)(2,1)}, bf16[8,160,128]{2,1,0:T(8,128)(2,1)S(1)}, u32[]{:S(2)}) copy-start(bf16[8,160,128]{2,1,0:T(8,128)(2,1)S(1)} %all-to-all-done.1.partial) | copy-start | bytes 983044
  120.2 42.9 %all-to-all-start.2 = ((bf16[16,192,128]{2,1,0:T(8,128)(2,1)}), bf16[16,192,128]{2,1,0:T(8,128)(2,1)S(1)}, u32[]{:S(2)}, u32[]{:S(2)}) async-start(bf16[16,192,128]{2,1,0:T(8,128)(2,1)} %shard_map.161), calls=%async_computation.2 | async-start | bytes 1572864 | tf_op jit(solution)/shard_map/all_to_all | solution.py:253
  163.1 0.9 copy-start
  190.0 11.4 %copy-start.1 = (bf16[8,256,128]{2,1,0:T(8,128)(2,1)}, bf16[8,256,128]{2,1,0:T(8,128)(2,1)S(1)}, u32[]{:S(2)}) copy-start(bf16[8,256,128]{2,1,0:T(8,128)(2,1)S(1)} %all_to_all.44.mine) | copy-start | bytes 1572868
  190.0 11.4 %collective-permute-start = (bf16[8,256,128]{2,1,0:T(8,128)(2,1)S(1)}, bf16[8,256,128]{2,1,0:T(8,128)(2,1)S(1)}, u32[]{:S(2)}, u32[]{:S(2)}) collective-permute-start(bf16[8,256,128]{2,1,0:T(8,128)(2,1)S(1)} %all_to_all.44.mine), channel_id=1, source_target_pairs={{0,1},{1,0},{2,3},{3,2},{4,5},{5,4},{6,7},{7,6},{8,9},{9,8},{10,11... | collective-permute-start | bytes 1572872 | tf_op jit(solution)/shard_map/ppermute | solution.py:257
  195.6 15.6 %all-to-all-start.5 = ((bf16[32,16,128]{2,1,0:T(8,128)(2,1)}), bf16[32,16,128]{2,1,0:T(8,128)(2,1)S(1)}, u32[]{:S(2)}, u32[]{:S(2)}) async-start(bf16[32,16,128]{2,1,0:T(8,128)(2,1)} %bitcast.18), calls=%async_computation.5 | async-start | bytes 262144 | tf_op jit(solution)/shard_map/all_to_all | solution.py:253
  201.3 0.8 copy-start.4
  211.2 0.6 copy-start.5
Sparse Core Ops, SparseCore 0:
  35.4 38.4 all-gather.6
  77.9 40.8 all-gather.8

commit v4 on v2

--- a/solution.py
+++ b/solution.py
@@ -74,13 +74,12 @@
         payload[x, :positions, :] = pairs
 
 
-def columns_kernel(w_down, w_out, out):
+def columns_kernel(w_down, w_out, down, out):
     parts, _, width = out.shape
-    hidden = w_down.shape[1]
     for k in range(parts):
         at = slice(k * width, (k + 1) * width)
-        out[k, :hidden, :] = w_down[0, :, at]
-        out[k, hidden:, :] = w_out[:, at]
+        down[k] = w_down[0, :, at]
+        out[k] = w_out[:, at]
 
 
 def relay_kernel(payload, queries, out):
@@ -195,8 +194,7 @@
 def mix_columns_kernel(attended, weights, out):
     parts, half, width = attended.shape
     head = width // 2
-    skip = weights.shape[1] - head
-    side = jnp.concatenate([weights[k, skip:, :] for k in range(parts)], axis=0)
+    side = jnp.concatenate([weights[k] for k in range(parts)], axis=0)
     top = jnp.concatenate([attended[k][:, :head] for k in range(parts)], axis=1)
     low = jnp.concatenate([attended[k][:, head:] for k in range(parts)], axis=1)
     top = dot(top, side).astype(out.dtype)
@@ -341,13 +339,15 @@
     every_row = jnp.concatenate([arrived, gain_rows], axis=0)
     every_row = lax.all_gather(every_row, TP, axis=0)
 
-    columns = call(
+    columns = (tp_count, w_out.shape[0], model // tp_count)
+    down_columns, out_columns = call(
         columns_kernel,
-        shape((tp_count, w_down.shape[1] + head, model // tp_count), bf16),
+        (shape((tp_count, w_down.shape[1], columns[2]), bf16), shape(columns, bf16)),
         w_down,
         w_out,
     )
-    columns = exchanged(columns, TP)
+    out_columns = exchanged(out_columns, TP)
+    down_columns = exchanged(down_columns, TP)
 
     partial = call(
         attend_kernel,
@@ -374,7 +374,7 @@
         ],
     )
     every_hidden = lax.all_gather(hidden, TP, axis=0)
-    expert_out = call(down_kernel, shape((slots, part), bf16), every_hidden, columns)
+    expert_out = call(down_kernel, shape((slots, part), bf16), every_hidden, down_columns)
     returned = exchanged(expert_out, EP)
     exp_out = call(combine_kernel, shape((tokens, part), bf16), table, returned)
 
@@ -383,7 +383,7 @@
         mix_columns_kernel,
         shape((tp_count // 2, rows, model // tp_count), bf16),
         every_head,
-        columns,
+        out_columns,
     )
     mine = exchanged(own_columns, "tp_0")
     mix_out = call(

time: 218 us -> 226 us (1.037)
  waiting for transfers between devices: 57.7 us -> 73.3 us
  blocking collectives: 89.8 us -> 78.5 us
  starting transfers between devices: 18 us -> 21.3 us
    all_to_all x3 -> x4, waiting for transfers between devices: 17.9 us -> 33.5 us  [exchanged(): return lax.all_to_all(value, axis, 0, 0, tiled=True)]
    all_gather x1, blocking collectives: 32.5 us -> 21 us  [on_device(): every_head = lax.all_gather(attended, TP, axis=0)]
    all_to_all x3 -> x4, starting transfers between devices: 15.5 us -> 19.1 us  [exchanged(): return lax.all_to_all(value, axis, 0, 0, tiled=True)]
  transfers between devices with their start and end apart: 6 -> 7, of which waited for: 3 -> 4; matrix products, arithmetic and copies ran while one was open for 0% -> 0% of each run, Pallas kernels for 10% -> 10%
where the time goes in v4:
time: 226 us; the launch traced here: 225 us
  blocking collectives  78.5 us (35%)
  waiting for transfers between devices  73.3 us (32%)
  Pallas kernels  33.4 us (15%)
  starting transfers between devices  21.3 us (9%)
  between operations  14.1 us (6%)
  local copies, waits for them, and re-layouts  2.94 us (1%)
    all_to_all x3, blocking collectives, exchanged(): return lax.all_to_all(value, axis, 0, 0, tiled=True)  57.5 us
    all_gather x1, waiting for transfers between devices, on_device(): every_row = lax.all_gather(every_row, TP, axis=0)  39.7 us
    all_to_all x4, waiting for transfers between devices, exchanged(): return lax.all_to_all(value, axis, 0, 0, tiled=True)  33.5 us
    pallas_call x10, Pallas kernels, call(): return pl.pallas_call(body, out_shape=outs, in_specs=specs, **kwargs)(*args)  33.4 us
    all_gather x1, blocking collectives, on_device(): every_head = lax.all_gather(attended, TP, axis=0)  21 us
    all_to_all x4, starting transfers between devices, exchanged(): return lax.all_to_all(value, axis, 0, 0, tiled=True)  19.1 us
  transfers between devices with their start and end apart: 7, of which 4 were waited for; matrix products, arithmetic and copies ran while one was open for 0% of the time, Pallas kernels for 10%

profile of v4, /device:TPU:1, one launch (start us, length us, event | category | flops | bytes accessed | tf_op | source)
XLA Modules:
  0.0 225.1 jit_solution(1618708079142969309)
XLA Ops:
  7.2 3.8 %shard_map.158 = (bf16[128,128]{1,0:T(8,128)(2,1)}, bf16[4,384,128]{2,1,0:T(8,128)(2,1)}, f32[512,96]{1,0:T(8,128)}) custom-call(s32[4,96]{1,0:T(4,128)} %bitcast.17, f32[4,96]{1,0:T(4,128)} %bitcast.18, bf16[96,128]{1,0:T(8,128)(2,1)} %rows.1, bf16[256,2048]{1,0:T(8,128)(2,1)} %mix_rows.1, bf16[2048]{0:T(1024)(128)(2,1)} %gain.2, bf16[64,2048]{1,0:T(8,128)(2,1)} %w_query.1, ...), custom_call_target="tpu_custom_call" | custom-call | tf_op jit(solution)/shard_map/pallas_call | solution.py:270
  11.0 11.2 %all_to_all.41.payload = bf16[4,384,128]{2,1,0:T(8,128)(2,1)} all-to-all(bf16[4,384,128]{2,1,0:T(8,128)(2,1)} %get-tuple-element.7), channel_id=1, replica_groups=mesh['ep_0'=8,'ep_1'=4,'tp_0'=8,'tp_1'=2] {'ep_1'}, dimensions={0} | all-to-all | bytes 786432 | tf_op jit(solution)/shard_map/all_to_all | solution.py:274
  22.2 1.8 shard_map.159
  23.9 22.8 %all_to_all.42.asked = bf16[8,192,128]{2,1,0:T(8,128)(2,1)S(1)} all-to-all(bf16[8,192,128]{2,1,0:T(8,128)(2,1)} %shard_map.159), channel_id=1, replica_groups=mesh['ep_0'=8,'ep_1'=4,'tp_0'=8,'tp_1'=2] {'ep_0'}, dimensions={0} | all-to-all | bytes 786432 | tf_op jit(solution)/shard_map/all_to_all | solution.py:274
  47.6 39.7 %all-gather.6.cloned.1.call-done = bf16[8448,128]{1,0:T(8,128)(2,1)} async-done(((bf16[528,128]{1,0:T(8,128)(2,1)}), bf16[8448,128]{1,0:T(8,128)(2,1)}) %all-gather.6.cloned.1.call-update) | async-done | bytes 2162704 | tf_op jit(solution)/shard_map/all_gather | solution.py:340
  87.3 3.8 %shard_map.165 = bf16[512,128]{1,0:T(8,128)(2,1)} custom-call(bf16[16,528,128]{2,1,0:T(8,128)(2,1)} %bitcast.11, bf16[1,2048,128]{2,1,0:T(8,128)(2,1)} %w_gate.1, bf16[1,2048,128]{2,1,0:T(8,128)(2,1)} %w_up.1), custom_call_target="tpu_custom_call" | custom-call | tf_op jit(solution)/shard_map/pallas_call | solution.py:270
  91.8 9.6 %shard_map.160 = bf16[8,160,128]{2,1,0:T(8,128)(2,1)} custom-call(s32[2]{0:T(128)} %pad_add_fusion.where_ref, bf16[4,384,128]{2,1,0:T(8,128)(2,1)} %all_to_all.41.payload, bf16[8,192,128]{2,1,0:T(8,128)(2,1)} %copy-done, f32[1,8192]{1,0:T(1,128)} %offsets.1), custom_call_target="tpu_custom_call" | custom-call | tf_op jit(solution)/shard_map/pallas_call | solution.py:270
  101.4 3.4 %all-to-all-start.2 = ((bf16[8,160,128]{2,1,0:T(8,128)(2,1)}), bf16[8,160,128]{2,1,0:T(8,128)(2,1)S(1)}, u32[]{:S(2)}, u32[]{:S(2)}) async-start(bf16[8,160,128]{2,1,0:T(8,128)(2,1)} %shard_map.160), calls=%async_computation.2 | async-start | bytes 655360 | tf_op jit(solution)/shard_map/all_to_all | solution.py:274
  104.9 2.1 shard_map.162
  107.0 11.5 %all-to-all-done.2.partial = bf16[8,160,128]{2,1,0:T(8,128)(2,1)S(1)} async-done(((bf16[8,160,128]{2,1,0:T(8,128)(2,1)}), bf16[8,160,128]{2,1,0:T(8,128)(2,1)S(1)}, u32[]{:S(2)}, u32[]{:S(2)}) %all-to-all-start.2) | async-done | bytes 327712 | tf_op jit(solution)/shard_map/all_to_all | solution.py:274
  118.5 5.0 %all-to-all-start.3 = ((bf16[16,64,128]{2,1,0:T(8,128)(2,1)}), bf16[16,64,128]{2,1,0:T(8,128)(2,1)S(1)}, u32[]{:S(2)}, u32[]{:S(2)}) async-start(bf16[16,64,128]{2,1,0:T(8,128)(2,1)} %get-tuple-element.9), calls=%async_computation.3 | async-start | bytes 524288 | tf_op jit(solution)/shard_map/all_to_all | solution.py:274
  123.6 2.4 %shard_map.161 = bf16[128,128]{1,0:T(8,128)(2,1)} custom-call(bf16[8,160,128]{2,1,0:T(8,128)(2,1)} %copy-done.3), custom_call_target="tpu_custom_call" | custom-call | tf_op jit(solution)/shard_map/pallas_call | solution.py:270
  126.0 21.0 %all-gather = bf16[2048,128]{1,0:T(8,128)(2,1)} all-gather(bf16[128,128]{1,0:T(8,128)(2,1)} %shard_map.161), channel_id=2, replica_groups=mesh['ep_0'=8,'ep_1'=4,'tp_0'=8,'tp_1'=2] {'tp_0','tp_1'}, dimensions={0}, use_global_device_ids=true | all-gather | bytes 557056 | tf_op jit(solution)/shard_map/all_gather | solution.py:381
  147.7 2.3 %shard_map.163 = bf16[8,256,128]{2,1,0:T(8,128)(2,1)} custom-call(bf16[16,128,128]{2,1,0:T(8,128)(2,1)} %bitcast.13, bf16[16,64,128]{2,1,0:T(8,128)(2,1)} %copy-done.4), custom_call_target="tpu_custom_call" | custom-call | tf_op jit(solution)/shard_map/pallas_call | solution.py:270
  150.0 23.5 %all_to_all.43.mine = bf16[8,256,128]{2,1,0:T(8,128)(2,1)S(1)} all-to-all(bf16[8,256,128]{2,1,0:T(8,128)(2,1)} %shard_map.163), channel_id=1, replica_groups=mesh['ep_0'=8,'ep_1'=4,'tp_0'=8,'tp_1'=2] {'tp_0'}, dimensions={0} | all-to-all | bytes 1048576 | tf_op jit(solution)/shard_map/all_to_all | solution.py:274
  173.5 4.0 %all-to-all-start.5 = ((bf16[16,128,128]{2,1,0:T(8,128)(2,1)}), bf16[16,128,128]{2,1,0:T(8,128)(2,1)S(1)}, u32[]{:S(2)}, u32[]{:S(2)}) async-start(bf16[16,128,128]{2,1,0:T(8,128)(2,1)} %get-tuple-element.11), calls=%async_computation.5 | async-start | bytes 1048576 | tf_op jit(solution)/shard_map/all_to_all | solution.py:274
  177.5 2.1 collective-permute-start
  179.6 15.2 %all-to-all-done.5.weights = bf16[16,128,128]{2,1,0:T(8,128)(2,1)S(1)} async-done(((bf16[16,128,128]{2,1,0:T(8,128)(2,1)}), bf16[16,128,128]{2,1,0:T(8,128)(2,1)S(1)}, u32[]{:S(2)}, u32[]{:S(2)}) %all-to-all-start.5) | async-done | bytes 524320 | tf_op jit(solution)/shard_map/all_to_all | solution.py:274
  194.8 0.8 copy-done.2
  195.6 3.0 %shard_map.166 = bf16[512,128]{1,0:T(8,128)(2,1)} custom-call(bf16[16,512,128]{2,1,0:T(8,128)(2,1)} %bitcast.12, bf16[16,128,128]{2,1,0:T(8,128)(2,1)} %copy-done.2), custom_call_target="tpu_custom_call" | custom-call | tf_op jit(solution)/shard_map/pallas_call | solution.py:270
  198.7 6.7 %all-to-all-start.6 = ((bf16[32,16,128]{2,1,0:T(8,128)(2,1)}), bf16[32,16,128]{2,1,0:T(8,128)(2,1)S(1)}, u32[]{:S(2)}, u32[]{:S(2)}) async-start(bf16[32,16,128]{2,1,0:T(8,128)(2,1)} %bitcast.16), calls=%async_computation.6 | async-start | bytes 262144 | tf_op jit(solution)/shard_map/all_to_all | solution.py:274
  206.2 2.7 %shard_map.164 = bf16[256,2048]{1,0:T(8,128)(2,1)} custom-call(s32[1]{0:T(128)} %bitcast.core_ref, bf16[8,256,128]{2,1,0:T(8,128)(2,1)} %copy-done.1, bf16[8,256,128]{2,1,0:T(8,128)(2,1)} %copy-done.5, bf16[2048]{0:T(1024)(128)(2,1)} %gain.3), custom_call_target="tpu_custom_call" | custom-call | tf_op jit(solution)/shard_map/pallas_call | solution.py:270
  208.9 6.8 %all-to-all-done.6 = bf16[32,16,128]{2,1,0:T(8,128)(2,1)S(1)} async-done(((bf16[32,16,128]{2,1,0:T(8,128)(2,1)}), bf16[32,16,128]{2,1,0:T(8,128)(2,1)S(1)}, u32[]{:S(2)}, u32[]{:S(2)}) %all-to-all-start.6) | async-done | bytes 131104 | tf_op jit(solution)/shard_map/all_to_all | solution.py:274
  216.4 1.9 shard_map.167
  (26 shorter events, 3.7 us)
Async XLA Ops:
  7.2 80.1 %all-gather.6.cloned.1.call-start = ((), (), s32[]{:S(2)}) async-start(), calls=%async_computation.7 | async-start | bytes 2297856 | tf_op jit(solution)/shard_map/all_gather | solution.py:340
  7.2 39.5 %copy-start.7 = (bf16[128]{0:T(256)(128)(2,1)S(1)}, bf16[128]{0:T(256)(128)(2,1)}, u32[]{:S(2)}) copy-start(bf16[128]{0:T(256)(128)(2,1)} %param.24) | copy-start | bytes 772
  46.7 45.1 %copy-start = (bf16[8,192,128]{2,1,0:T(8,128)(2,1)}, bf16[8,192,128]{2,1,0:T(8,128)(2,1)S(1)}, u32[]{:S(2)}) copy-start(bf16[8,192,128]{2,1,0:T(8,128)(2,1)S(1)} %all_to_all.42.asked) | copy-start | bytes 1179652
  47.5 147.3 %all-gather.8.cloned.1.call-start = ((), (), s32[]{:S(2)}) async-start(), calls=%async_computation.8 | async-start | bytes 2228224 | tf_op jit(solution)/shard_map/all_gather | solution.py:376
  101.4 17.1 %all-to-all-start.2 = ((bf16[8,160,128]{2,1,0:T(8,128)(2,1)}), bf16[8,160,128]{2,1,0:T(8,128)(2,1)S(1)}, u32[]{:S(2)}, u32[]{:S(2)}) async-start(bf16[8,160,128]{2,1,0:T(8,128)(2,1)} %shard_map.160), calls=%async_computation.2 | async-start | bytes 655360 | tf_op jit(solution)/shard_map/all_to_all | solution.py:274
  118.5 5.0 %copy-start.3 = (bf16[8,160,128]{2,1,0:T(8,128)(2,1)}, bf16[8,160,128]{2,1,0:T(8,128)(2,1)S(1)}, u32[]{:S(2)}) copy-start(bf16[8,160,128]{2,1,0:T(8,128)(2,1)S(1)} %all-to-all-done.2.partial) | copy-start | bytes 983044
  118.5 28.5 %all-to-all-start.3 = ((bf16[16,64,128]{2,1,0:T(8,128)(2,1)}), bf16[16,64,128]{2,1,0:T(8,128)(2,1)S(1)}, u32[]{:S(2)}, u32[]{:S(2)}) async-start(bf16[16,64,128]{2,1,0:T(8,128)(2,1)} %get-tuple-element.9), calls=%async_computation.3 | async-start | bytes 524288 | tf_op jit(solution)/shard_map/all_to_all | solution.py:274
  147.1 0.7 copy-start.4
  173.5 31.9 %copy-start.1 = (bf16[8,256,128]{2,1,0:T(8,128)(2,1)}, bf16[8,256,128]{2,1,0:T(8,128)(2,1)S(1)}, u32[]{:S(2)}) copy-start(bf16[8,256,128]{2,1,0:T(8,128)(2,1)S(1)} %all_to_all.43.mine) | copy-start | bytes 1572868
  173.5 21.3 %all-to-all-start.5 = ((bf16[16,128,128]{2,1,0:T(8,128)(2,1)}), bf16[16,128,128]{2,1,0:T(8,128)(2,1)S(1)}, u32[]{:S(2)}, u32[]{:S(2)}) async-start(bf16[16,128,128]{2,1,0:T(8,128)(2,1)} %get-tuple-element.11), calls=%async_computation.5 | async-start | bytes 1048576 | tf_op jit(solution)/shard_map/all_to_all | solution.py:274
  177.5 27.9 %collective-permute-start = (bf16[8,256,128]{2,1,0:T(8,128)(2,1)S(1)}, bf16[8,256,128]{2,1,0:T(8,128)(2,1)S(1)}, u32[]{:S(2)}, u32[]{:S(2)}) collective-permute-start(bf16[8,256,128]{2,1,0:T(8,128)(2,1)S(1)} %all_to_all.43.mine), channel_id=1, source_target_pairs={{0,1},{1,0},{2,3},{3,2},{4,5},{5,4},{6,7},{7,6},{8,9},{9,8},{10,11... | collective-permute-start | bytes 1572872 | tf_op jit(solution)/shard_map/ppermute | solution.py:278
  194.8 0.8 copy-start.2
  198.7 17.1 %all-to-all-start.6 = ((bf16[32,16,128]{2,1,0:T(8,128)(2,1)}), bf16[32,16,128]{2,1,0:T(8,128)(2,1)S(1)}, u32[]{:S(2)}, u32[]{:S(2)}) async-start(bf16[32,16,128]{2,1,0:T(8,128)(2,1)} %bitcast.16), calls=%async_computation.6 | async-start | bytes 262144 | tf_op jit(solution)/shard_map/all_to_all | solution.py:274
  205.4 0.8 copy-start.5
  215.7 0.6 copy-start.6
Sparse Core Ops, SparseCore 0:
  47.6 39.6 all-gather.5
  91.3 42.4 all-gather.7

commit v5 on v2

--- a/solution.py
+++ b/solution.py
@@ -29,7 +29,18 @@
 
 
 def prepare_kernel(
-    routes, weight, rows, mix_rows, gain, w_query, w_key, w_value, queries, payload, table
+    routes,
+    weight,
+    rows,
+    mix_rows,
+    gain,
+    w_query,
+    w_key,
+    w_value,
+    queries,
+    payload,
+    table,
+    every,
 ):
     top, tokens = routes.shape
     slots = table.shape[0]
@@ -65,17 +76,27 @@
     factor = row_factor(jnp.sum(numbers * numbers, axis=1, keepdims=True), numbers.shape[1])
     normed = (numbers * factor * gain[...][None].astype(jnp.float32)).astype(jnp.bfloat16)
     half = positions // 2
-    asked = dot(normed, w_query[...], ((1,), (1,))).astype(jnp.bfloat16)
+    head = w_query.shape[0]
+    every[:head, :] = w_query[...]
+    every[head : 2 * head, :] = w_key[...]
+    every[2 * head :, :] = w_value[...]
+    both = dot(normed, every[...], ((1,), (1,))).astype(jnp.bfloat16)
+    asked = both[:, :head]
     queries[...] = jnp.concatenate([asked[:half], asked[half:]], axis=1)
-    keys = dot(normed, w_key[...], ((1,), (1,)))
-    values = dot(normed, w_value[...], ((1,), (1,)))
-    pairs = jnp.concatenate([keys, values], axis=1).astype(payload.dtype)
+    pairs = both[:, head:]
     for x in range(across):
         payload[x, :positions, :] = pairs
 
 
-def columns_kernel(w_down, w_out, out):
+def columns_kernel(w_down, w_out, table, out, turned):
     parts, _, width = out.shape
+    scale = table[...]
+    slots, _ = scale.shape
+    turn = identity(slots).astype(jnp.bfloat16)
+    for k in range(turned.shape[0]):
+        piece = scale.astype(jnp.bfloat16)
+        scale = scale - piece.astype(jnp.float32)
+        turned[k] = dot(piece, turn, ((0,), (0,))).astype(jnp.bfloat16)
     hidden = w_down.shape[1]
     for k in range(parts):
         at = slice(k * width, (k + 1) * width)
@@ -256,13 +277,8 @@
 
 
 def combine_kernel(table, returned, out):
-    scale = table[...]
     rows = returned[...]
-    total = jnp.zeros(out.shape, jnp.float32)
-    for _ in range(3):
-        part = scale.astype(jnp.bfloat16)
-        total = total + dot(part, rows, ((0,), (0,)))
-        scale = scale - part.astype(jnp.float32)
+    total = dot(table[0], rows) + dot(table[1], rows)
     out[...] = total.astype(out.dtype)
 
 
@@ -330,6 +346,7 @@
         w_query,
         w_key,
         w_value,
+        scratch_shapes=[pltpu.VMEM((3 * head, model), bf16)],
     )
     payload = exchanged(payload, "ep_1")
     asked = call(
@@ -341,11 +358,15 @@
     every_row = jnp.concatenate([arrived, gain_rows], axis=0)
     every_row = lax.all_gather(every_row, TP, axis=0)
 
-    columns = call(
+    columns, turned = call(
         columns_kernel,
-        shape((tp_count, w_down.shape[1] + head, model // tp_count), bf16),
+        (
+            shape((tp_count, w_down.shape[1] + head, model // tp_count), bf16),
+            shape((2, tokens, slots), bf16),
+        ),
         w_down,
         w_out,
+        table,
     )
     columns = exchanged(columns, TP)
 
@@ -376,7 +397,7 @@
     every_hidden = lax.all_gather(hidden, TP, axis=0)
     expert_out = call(down_kernel, shape((slots, part), bf16), every_hidden, columns)
     returned = exchanged(expert_out, EP)
-    exp_out = call(combine_kernel, shape((tokens, part), bf16), table, returned)
+    exp_out = call(combine_kernel, shape((tokens, part), bf16), turned, returned)
 
     every_head = lax.all_gather(attended, TP, axis=0)
     own_columns = call(

time: 218 us -> 217 us (level)
  transfers between devices with their start and end apart: 6 -> 6, of which waited for: 3 -> 3; matrix products, arithmetic and copies ran while one was open for 0% -> 0% of each run, Pallas kernels for 10% -> 11%
where the time goes in v5:
time: 217 us
  blocking collectives  89.8 us (41%)
  waiting for transfers between devices  57.3 us (26%)
  Pallas kernels  33.5 us (15%)
  starting transfers between devices  18 us (8%)
  between operations  14.1 us (6%)
  local copies, waits for them, and re-layouts  2.34 us (1%)
    all_to_all x3, blocking collectives, exchanged(): return lax.all_to_all(value, axis, 0, 0, tiled=True)  57.3 us
    all_gather x1, waiting for transfers between devices, on_device(): every_row = lax.all_gather(every_row, TP, axis=0)  39.7 us
    pallas_call x10, Pallas kernels, call(): return pl.pallas_call(body, out_shape=outs, in_specs=specs, **kwargs)(*args)  33.5 us
    all_gather x1, blocking collectives, on_device(): every_head = lax.all_gather(attended, TP, axis=0)  32.5 us
    all_to_all x3, waiting for transfers between devices, exchanged(): return lax.all_to_all(value, axis, 0, 0, tiled=True)  17.5 us
    all_to_all x3, starting transfers between devices, exchanged(): return lax.all_to_all(value, axis, 0, 0, tiled=True)  15.5 us
  transfers between devices with their start and end apart: 6, of which 3 were waited for; matrix products, arithmetic and copies ran while one was open for 0% of the time, Pallas kernels for 11%

profile of v5, /device:TPU:1, one launch (start us, length us, event | category | flops | bytes accessed | tf_op | source)
XLA Modules:
  0.0 216.5 jit_solution(12683699042477906313)
XLA Ops:
  7.2 3.3 %shard_map.158 = (bf16[128,128]{1,0:T(8,128)(2,1)}, bf16[4,384,128]{2,1,0:T(8,128)(2,1)}, f32[512,96]{1,0:T(8,128)}) custom-call(s32[4,96]{1,0:T(4,128)} %bitcast.17, f32[4,96]{1,0:T(4,128)} %bitcast.18, bf16[96,128]{1,0:T(8,128)(2,1)} %rows.1, bf16[256,2048]{1,0:T(8,128)(2,1)} %mix_rows.1, bf16[2048]{0:T(1024)(128)(2,1)} %gain.2, bf16[64,2048]{1,0:T(8,128)(2,1)} %w_query.1, ...), custom_call_target="tpu_custom_call" | custom-call | tf_op jit(solution)/shard_map/pallas_call | solution.py:288
  10.5 11.2 %all_to_all.36.payload = bf16[4,384,128]{2,1,0:T(8,128)(2,1)} all-to-all(bf16[4,384,128]{2,1,0:T(8,128)(2,1)} %get-tuple-element.7), channel_id=1, replica_groups=mesh['ep_0'=8,'ep_1'=4,'tp_0'=8,'tp_1'=2] {'ep_1'}, dimensions={0} | all-to-all | bytes 786432 | tf_op jit(solution)/shard_map/all_to_all | solution.py:292
  21.7 1.8 shard_map.159
  23.5 22.8 %all_to_all.37.asked = bf16[8,192,128]{2,1,0:T(8,128)(2,1)S(1)} all-to-all(bf16[8,192,128]{2,1,0:T(8,128)(2,1)} %shard_map.159), channel_id=1, replica_groups=mesh['ep_0'=8,'ep_1'=4,'tp_0'=8,'tp_1'=2] {'ep_0'}, dimensions={0} | all-to-all | bytes 786432 | tf_op jit(solution)/shard_map/all_to_all | solution.py:292
  46.3 0.7 pad_maximum_fusion
  47.1 39.7 %all-gather.6.cloned.1.call-done = bf16[8448,128]{1,0:T(8,128)(2,1)} async-done(((bf16[528,128]{1,0:T(8,128)(2,1)}), bf16[8448,128]{1,0:T(8,128)(2,1)}) %all-gather.6.cloned.1.call-update) | async-done | bytes 2162704 | tf_op jit(solution)/shard_map/all_gather | solution.py:359
  86.8 3.8 %shard_map.165 = bf16[512,128]{1,0:T(8,128)(2,1)} custom-call(bf16[16,528,128]{2,1,0:T(8,128)(2,1)} %bitcast.11, bf16[1,2048,128]{2,1,0:T(8,128)(2,1)} %w_gate.1, bf16[1,2048,128]{2,1,0:T(8,128)(2,1)} %w_up.1), custom_call_target="tpu_custom_call" | custom-call | tf_op jit(solution)/shard_map/pallas_call | solution.py:288
  91.3 9.6 %shard_map.160 = bf16[8,160,128]{2,1,0:T(8,128)(2,1)} custom-call(s32[2]{0:T(128)} %pad_add_fusion.where_ref, bf16[4,384,128]{2,1,0:T(8,128)(2,1)} %all_to_all.36.payload, bf16[8,192,128]{2,1,0:T(8,128)(2,1)} %copy-done.1, f32[1,8192]{1,0:T(1,128)} %offsets.1), custom_call_target="tpu_custom_call" | custom-call | tf_op jit(solution)/shard_map/pallas_call | solution.py:288
  100.9 3.4 %all-to-all-start.2 = ((bf16[8,160,128]{2,1,0:T(8,128)(2,1)}), bf16[8,160,128]{2,1,0:T(8,128)(2,1)S(1)}, u32[]{:S(2)}, u32[]{:S(2)}) async-start(bf16[8,160,128]{2,1,0:T(8,128)(2,1)} %shard_map.160), calls=%async_computation.2 | async-start | bytes 655360 | tf_op jit(solution)/shard_map/all_to_all | solution.py:292
  104.3 2.5 %shard_map.162 = (bf16[16,192,128]{2,1,0:T(8,128)(2,1)}, bf16[2,96,512]{2,1,0:T(8,128)(2,1)}) custom-call(bf16[1,128,2048]{2,1,0:T(8,128)(2,1)} %w_down.1, bf16[64,2048]{1,0:T(8,128)(2,1)} %w_out.1, f32[512,96]{1,0:T(8,128)} %get-tuple-element.9.table), custom_call_target="tpu_custom_call" | custom-call | tf_op jit(solution)/shard_map/pallas_call | solution.py:288
  106.9 11.2 %all-to-all-done.2.partial = bf16[8,160,128]{2,1,0:T(8,128)(2,1)S(1)} async-done(((bf16[8,160,128]{2,1,0:T(8,128)(2,1)}), bf16[8,160,128]{2,1,0:T(8,128)(2,1)S(1)}, u32[]{:S(2)}, u32[]{:S(2)}) %all-to-all-start.2) | async-done | bytes 327712 | tf_op jit(solution)/shard_map/all_to_all | solution.py:292
  118.0 5.0 %all-to-all-start.3 = ((bf16[16,192,128]{2,1,0:T(8,128)(2,1)}), bf16[16,192,128]{2,1,0:T(8,128)(2,1)S(1)}, u32[]{:S(2)}, u32[]{:S(2)}) async-start(bf16[16,192,128]{2,1,0:T(8,128)(2,1)} %get-tuple-element.10), calls=%async_computation.3 | async-start | bytes 1572864 | tf_op jit(solution)/shard_map/all_to_all | solution.py:292
  123.0 2.4 %shard_map.161 = bf16[128,128]{1,0:T(8,128)(2,1)} custom-call(bf16[8,160,128]{2,1,0:T(8,128)(2,1)} %copy-done.3), custom_call_target="tpu_custom_call" | custom-call | tf_op jit(solution)/shard_map/pallas_call | solution.py:288
  125.5 32.5 %all-gather = bf16[2048,128]{1,0:T(8,128)(2,1)} all-gather(bf16[128,128]{1,0:T(8,128)(2,1)} %shard_map.161), channel_id=2, replica_groups=mesh['ep_0'=8,'ep_1'=4,'tp_0'=8,'tp_1'=2] {'tp_0','tp_1'}, dimensions={0}, use_global_device_ids=true | all-gather | bytes 557056 | tf_op jit(solution)/shard_map/all_gather | solution.py:402
  158.0 0.9 copy-done
  158.9 2.4 %shard_map.163 = bf16[8,256,128]{2,1,0:T(8,128)(2,1)} custom-call(bf16[16,128,128]{2,1,0:T(8,128)(2,1)} %bitcast.12, bf16[16,192,128]{2,1,0:T(8,128)(2,1)} %copy-done), custom_call_target="tpu_custom_call" | custom-call | tf_op jit(solution)/shard_map/pallas_call | solution.py:288
  161.3 23.3 %all_to_all.38.mine = bf16[8,256,128]{2,1,0:T(8,128)(2,1)S(1)} all-to-all(bf16[8,256,128]{2,1,0:T(8,128)(2,1)} %shard_map.163), channel_id=1, replica_groups=mesh['ep_0'=8,'ep_1'=4,'tp_0'=8,'tp_1'=2] {'tp_0'}, dimensions={0} | all-to-all | bytes 1048576 | tf_op jit(solution)/shard_map/all_to_all | solution.py:292
  184.7 2.5 %collective-permute-start = (bf16[8,256,128]{2,1,0:T(8,128)(2,1)S(1)}, bf16[8,256,128]{2,1,0:T(8,128)(2,1)S(1)}, u32[]{:S(2)}, u32[]{:S(2)}) collective-permute-start(bf16[8,256,128]{2,1,0:T(8,128)(2,1)S(1)} %all_to_all.38.mine), channel_id=1, source_target_pairs={{0,1},{1,0},{2,3},{3,2},{4,5},{5,4},{6,7},{7,6},{8,9},{9,8},{10,11... | collective-permute-start | bytes 1572872 | tf_op jit(solution)/shard_map/ppermute | solution.py:296
  187.2 3.1 %shard_map.166 = bf16[512,128]{1,0:T(8,128)(2,1)} custom-call(bf16[16,512,128]{2,1,0:T(8,128)(2,1)} %bitcast.13, bf16[16,192,128]{2,1,0:T(8,128)(2,1)} %copy-done), custom_call_target="tpu_custom_call" | custom-call | tf_op jit(solution)/shard_map/pallas_call | solution.py:288
  190.3 7.0 %all-to-all-start.5 = ((bf16[32,16,128]{2,1,0:T(8,128)(2,1)}), bf16[32,16,128]{2,1,0:T(8,128)(2,1)S(1)}, u32[]{:S(2)}, u32[]{:S(2)}) async-start(bf16[32,16,128]{2,1,0:T(8,128)(2,1)} %bitcast.14), calls=%async_computation.5 | async-start | bytes 262144 | tf_op jit(solution)/shard_map/all_to_all | solution.py:292
  197.4 0.8 copy-done.4
  198.1 2.7 %shard_map.164 = bf16[256,2048]{1,0:T(8,128)(2,1)} custom-call(s32[1]{0:T(128)} %bitcast.core_ref, bf16[8,256,128]{2,1,0:T(8,128)(2,1)} %copy-done.2, bf16[8,256,128]{2,1,0:T(8,128)(2,1)} %copy-done.4, bf16[2048]{0:T(1024)(128)(2,1)} %gain.3), custom_call_target="tpu_custom_call" | custom-call | tf_op jit(solution)/shard_map/pallas_call | solution.py:288
  200.9 6.4 %all-to-all-done.5 = bf16[32,16,128]{2,1,0:T(8,128)(2,1)S(1)} async-done(((bf16[32,16,128]{2,1,0:T(8,128)(2,1)}), bf16[32,16,128]{2,1,0:T(8,128)(2,1)S(1)}, u32[]{:S(2)}, u32[]{:S(2)}) %all-to-all-start.5) | async-done | bytes 131104 | tf_op jit(solution)/shard_map/all_to_all | solution.py:292
  207.9 1.8 shard_map.167
  (22 shorter events, 1.5 us)
Async XLA Ops:
  7.2 79.7 %all-gather.6.cloned.1.call-start = ((), (), s32[]{:S(2)}) async-start(), calls=%async_computation.6 | async-start | bytes 2297856 | tf_op jit(solution)/shard_map/all_gather | solution.py:359
  7.2 39.1 %copy-start.6 = (bf16[128]{0:T(256)(128)(2,1)S(1)}, bf16[128]{0:T(256)(128)(2,1)}, u32[]{:S(2)}) copy-start(bf16[128]{0:T(256)(128)(2,1)} %param.24) | copy-start | bytes 772
  46.2 45.1 %copy-start.1 = (bf16[8,192,128]{2,1,0:T(8,128)(2,1)}, bf16[8,192,128]{2,1,0:T(8,128)(2,1)S(1)}, u32[]{:S(2)}) copy-start(bf16[8,192,128]{2,1,0:T(8,128)(2,1)S(1)} %all_to_all.37.asked) | copy-start | bytes 1179652
  47.1 140.1 %all-gather.8.cloned.1.call-start = ((), (), s32[]{:S(2)}) async-start(), calls=%async_computation.7 | async-start | bytes 2228224 | tf_op jit(solution)/shard_map/all_gather | solution.py:397
  100.9 17.1 %all-to-all-start.2 = ((bf16[8,160,128]{2,1,0:T(8,128)(2,1)}), bf16[8,160,128]{2,1,0:T(8,128)(2,1)S(1)}, u32[]{:S(2)}, u32[]{:S(2)}) async-start(bf16[8,160,128]{2,1,0:T(8,128)(2,1)} %shard_map.160), calls=%async_computation.2 | async-start | bytes 655360 | tf_op jit(solution)/shard_map/all_to_all | solution.py:292
  118.0 5.0 %copy-start.3 = (bf16[8,160,128]{2,1,0:T(8,128)(2,1)}, bf16[8,160,128]{2,1,0:T(8,128)(2,1)S(1)}, u32[]{:S(2)}) copy-start(bf16[8,160,128]{2,1,0:T(8,128)(2,1)S(1)} %all-to-all-done.2.partial) | copy-start | bytes 983044
  118.0 40.0 %all-to-all-start.3 = ((bf16[16,192,128]{2,1,0:T(8,128)(2,1)}), bf16[16,192,128]{2,1,0:T(8,128)(2,1)S(1)}, u32[]{:S(2)}, u32[]{:S(2)}) async-start(bf16[16,192,128]{2,1,0:T(8,128)(2,1)} %get-tuple-element.10), calls=%async_computation.3 | async-start | bytes 1572864 | tf_op jit(solution)/shard_map/all_to_all | solution.py:292
  158.0 0.9 copy-start
  184.6 12.7 %copy-start.2 = (bf16[8,256,128]{2,1,0:T(8,128)(2,1)}, bf16[8,256,128]{2,1,0:T(8,128)(2,1)S(1)}, u32[]{:S(2)}) copy-start(bf16[8,256,128]{2,1,0:T(8,128)(2,1)S(1)} %all_to_all.38.mine) | copy-start | bytes 1572868
  184.7 12.7 %collective-permute-start = (bf16[8,256,128]{2,1,0:T(8,128)(2,1)S(1)}, bf16[8,256,128]{2,1,0:T(8,128)(2,1)S(1)}, u32[]{:S(2)}, u32[]{:S(2)}) collective-permute-start(bf16[8,256,128]{2,1,0:T(8,128)(2,1)S(1)} %all_to_all.38.mine), channel_id=1, source_target_pairs={{0,1},{1,0},{2,3},{3,2},{4,5},{5,4},{6,7},{7,6},{8,9},{9,8},{10,11... | collective-permute-start | bytes 1572872 | tf_op jit(solution)/shard_map/ppermute | solution.py:296
  190.3 16.9 %all-to-all-start.5 = ((bf16[32,16,128]{2,1,0:T(8,128)(2,1)}), bf16[32,16,128]{2,1,0:T(8,128)(2,1)S(1)}, u32[]{:S(2)}, u32[]{:S(2)}) async-start(bf16[32,16,128]{2,1,0:T(8,128)(2,1)} %bitcast.14), calls=%async_computation.5 | async-start | bytes 262144 | tf_op jit(solution)/shard_map/all_to_all | solution.py:292
  197.3 0.8 copy-start.4
  207.2 0.6 copy-start.5
Sparse Core Ops, SparseCore 0:
  47.2 39.6 all-gather.5
  90.8 43.2 all-gather.7

commit v6 on v5

--- a/solution.py
+++ b/solution.py
@@ -122,8 +122,8 @@
     return jnp.where(row == lax.broadcasted_iota(jnp.int32, (size, size), 1), 1.0, 0.0)
 
 
-def attend_kernel(where_ref, payload, asked, offsets, out):
-    z, x = where_ref[0], where_ref[1]
+def attend_kernel(z_ref, x_ref, payload, asked, offsets, out):
+    z, x = z_ref[0], x_ref[0]
     across = payload.shape[0]
     along = asked.shape[0]
     half = asked.shape[1] - across * PAD
@@ -178,13 +178,14 @@
         out[block] = jnp.zeros(out.shape[1:], out.dtype)
         return carry
 
-    def everything(block, carry):
-        q = asked_by(block)
-        state = start
-        ahead = [front(q, across - 1 - i, False) for i in range(across)]
-        for one in ahead:
-            state = back(one, state, False)
-        send(block, state)
+    def everything(blocks, carry):
+        asked_now = [asked_by(block) for block in blocks]
+        ahead = [[front(q, across - 1 - i, False) for i in range(across)] for q in asked_now]
+        for block, terms in zip(blocks, ahead):
+            state = start
+            for one in terms:
+                state = back(one, state, False)
+            send(block, state)
         return carry
 
     lax.fori_loop(0, z, nothing, 0)
@@ -192,7 +193,11 @@
     state = back(front(q, x, True), start, True)
     state = lax.fori_loop(0, x, lambda i, c: back(front(q, x - 1 - i, False), c, False), state)
     send(z, state)
-    lax.fori_loop(z + 1, along, everything, 0)
+    rest = along - 1 - z
+    lax.fori_loop(0, rest % 2, lambda i, c: everything([along - 1], c), 0)
+    lax.fori_loop(
+        0, rest // 2, lambda i, c: everything([z + 1 + 2 * i, z + 2 + 2 * i], c), 0
+    )
 
 
 def gather_kernel(partial, out):
@@ -273,12 +278,6 @@
         both = jnp.concatenate([hidden[k], hidden[k + 1]], axis=1)
         side = jnp.concatenate([weights[k, :width, :], weights[k + 1, :width, :]], axis=0)
         total = total + dot(both, side)
-    out[...] = total.astype(out.dtype)
-
-
-def combine_kernel(table, returned, out):
-    rows = returned[...]
-    total = dot(table[0], rows) + dot(table[1], rows)
     out[...] = total.astype(out.dtype)
 
 
@@ -325,7 +324,6 @@
     rows = mix_rows.shape[0]
     head = w_query.shape[0]
     model = mix_rows.shape[1]
-    own = jnp.stack([lax.axis_index("ep_0"), lax.axis_index("ep_1")]).astype(jnp.int32)
     core = lax.axis_index("tp_1").astype(jnp.int32)[None]
 
     across = lax.axis_size("ep_1")
@@ -373,11 +371,12 @@
     partial = call(
         attend_kernel,
         shape((along, half + 2 * PAD, 2 * head), bf16),
-        own,
+        lax.axis_index("ep_0").astype(jnp.int32)[None],
+        lax.axis_index("ep_1").astype(jnp.int32)[None],
         payload,
         asked,
         key_offset,
-        scalars=1,
+        scalars=2,
     )
     partial = exchanged(partial, "ep_0")
     attended = call(gather_kernel, shape((half, 2 * head), bf16), partial)
@@ -397,7 +396,9 @@
     every_hidden = lax.all_gather(hidden, TP, axis=0)
     expert_out = call(down_kernel, shape((slots, part), bf16), every_hidden, columns)
     returned = exchanged(expert_out, EP)
-    exp_out = call(combine_kernel, shape((tokens, part), bf16), turned, returned)
+    returned = returned.reshape(slots, part)
+    combined = dot(turned.reshape(2 * tokens, slots), returned).reshape(2, tokens, part)
+    exp_out = (combined[0] + combined[1]).astype(bf16)
 
     every_head = lax.all_gather(attended, TP, axis=0)
     own_columns = call(

time: 217 us -> 215 us (level)
  Pallas kernels: 33.5 us -> 30.8 us
    pallas_call x10 -> x9, Pallas kernels: 33.5 us -> 30.8 us  [call(): return pl.pallas_call(body, out_shape=outs, in_specs=specs, **kwargs)(*args)]
  transfers between devices with their start and end apart: 6 -> 6, of which waited for: 3 -> 3; matrix products, arithmetic and copies ran while one was open for 0% -> 0% of each run, Pallas kernels for 11% -> 10%
where the time goes in v6:
time: 215 us
  blocking collectives  90 us (42%)
  waiting for transfers between devices  57.3 us (27%)
  Pallas kernels  30.8 us (14%)
  starting transfers between devices  19 us (9%)
  between operations  14.2 us (7%)
    all_to_all x3, blocking collectives, exchanged(): return lax.all_to_all(value, axis, 0, 0, tiled=True)  57.3 us
    all_gather x1, waiting for transfers between devices, on_device(): every_row = lax.all_gather(every_row, TP, axis=0)  39.7 us
    all_gather x1, blocking collectives, on_device(): every_head = lax.all_gather(attended, TP, axis=0)  32.7 us
    pallas_call x9, Pallas kernels, call(): return pl.pallas_call(body, out_shape=outs, in_specs=specs, **kwargs)(*args)  30.8 us
    all_to_all x3, waiting for transfers between devices, exchanged(): return lax.all_to_all(value, axis, 0, 0, tiled=True)  17.6 us
    all_to_all x3, starting transfers between devices, exchanged(): return lax.all_to_all(value, axis, 0, 0, tiled=True)  16.4 us
  transfers between devices with their start and end apart: 6, of which 3 were waited for; matrix products, arithmetic and copies ran while one was open for 0% of the time, Pallas kernels for 10%

profile of v6, /device:TPU:1, one launch (start us, length us, event | category | flops | bytes accessed | tf_op | source)
XLA Modules:
  0.0 214.5 jit_solution(831444806332527288)
XLA Ops:
  7.2 3.3 %shard_map.158 = (bf16[128,128]{1,0:T(8,128)(2,1)}, bf16[4,384,128]{2,1,0:T(8,128)(2,1)}, f32[512,96]{1,0:T(8,128)}) custom-call(s32[4,96]{1,0:T(4,128)} %bitcast.21, f32[4,96]{1,0:T(4,128)} %bitcast.22, bf16[96,128]{1,0:T(8,128)(2,1)} %rows.1, bf16[256,2048]{1,0:T(8,128)(2,1)} %mix_rows.1, bf16[2048]{0:T(1024)(128)(2,1)} %gain.2, bf16[64,2048]{1,0:T(8,128)(2,1)} %w_query.1, ...), custom_call_target="tpu_custom_call" | custom-call | tf_op jit(solution)/shard_map/pallas_call | solution.py:287
  10.5 11.2 %all_to_all.37.payload = bf16[4,384,128]{2,1,0:T(8,128)(2,1)} all-to-all(bf16[4,384,128]{2,1,0:T(8,128)(2,1)} %get-tuple-element.7), channel_id=1, replica_groups=mesh['ep_0'=8,'ep_1'=4,'tp_0'=8,'tp_1'=2] {'ep_1'}, dimensions={0} | all-to-all | bytes 786432 | tf_op jit(solution)/shard_map/all_to_all | solution.py:291
  21.7 1.8 shard_map.159
  23.5 22.8 %all_to_all.38.asked = bf16[8,192,128]{2,1,0:T(8,128)(2,1)S(1)} all-to-all(bf16[8,192,128]{2,1,0:T(8,128)(2,1)} %shard_map.159), channel_id=1, replica_groups=mesh['ep_0'=8,'ep_1'=4,'tp_0'=8,'tp_1'=2] {'ep_0'}, dimensions={0} | all-to-all | bytes 786432 | tf_op jit(solution)/shard_map/all_to_all | solution.py:291
  46.3 0.7 pad_maximum_fusion
  47.1 39.7 %all-gather.6.cloned.1.call-done = bf16[8448,128]{1,0:T(8,128)(2,1)} async-done(((bf16[528,128]{1,0:T(8,128)(2,1)}), bf16[8448,128]{1,0:T(8,128)(2,1)}) %all-gather.6.cloned.1.call-update) | async-done | bytes 2162704 | tf_op jit(solution)/shard_map/all_gather | solution.py:357
  86.8 3.8 %shard_map.165 = bf16[512,128]{1,0:T(8,128)(2,1)} custom-call(bf16[16,528,128]{2,1,0:T(8,128)(2,1)} %bitcast.14, bf16[1,2048,128]{2,1,0:T(8,128)(2,1)} %w_gate.1, bf16[1,2048,128]{2,1,0:T(8,128)(2,1)} %w_up.1), custom_call_target="tpu_custom_call" | custom-call | tf_op jit(solution)/shard_map/pallas_call | solution.py:287
  90.7 8.6 %shard_map.160 = bf16[8,160,128]{2,1,0:T(8,128)(2,1)} custom-call(s32[1]{0:T(128)} %bitcast.1.z_ref, s32[1]{0:T(128)} %bitcast.2.x_ref, bf16[4,384,128]{2,1,0:T(8,128)(2,1)} %all_to_all.37.payload, bf16[8,192,128]{2,1,0:T(8,128)(2,1)} %copy-done.1, f32[1,8192]{1,0:T(1,128)} %offsets.1), custom_call_target="tpu_custom_call" | custom-call | tf_op jit(solution)/shard_map/pallas_call | solution.py:287
  99.3 3.8 %all-to-all-start.2 = ((bf16[8,160,128]{2,1,0:T(8,128)(2,1)}), bf16[8,160,128]{2,1,0:T(8,128)(2,1)S(1)}, u32[]{:S(2)}, u32[]{:S(2)}) async-start(bf16[8,160,128]{2,1,0:T(8,128)(2,1)} %shard_map.160), calls=%async_computation.2 | async-start | bytes 655360 | tf_op jit(solution)/shard_map/all_to_all | solution.py:291
  103.1 2.5 %shard_map.162 = (bf16[16,192,128]{2,1,0:T(8,128)(2,1)}, bf16[2,96,512]{2,1,0:T(8,128)(2,1)}) custom-call(bf16[1,128,2048]{2,1,0:T(8,128)(2,1)} %w_down.1, bf16[64,2048]{1,0:T(8,128)(2,1)} %w_out.1, f32[512,96]{1,0:T(8,128)} %get-tuple-element.9.table), custom_call_target="tpu_custom_call" | custom-call | tf_op jit(solution)/shard_map/pallas_call | solution.py:287
  105.6 11.2 %all-to-all-done.2.partial = bf16[8,160,128]{2,1,0:T(8,128)(2,1)S(1)} async-done(((bf16[8,160,128]{2,1,0:T(8,128)(2,1)}), bf16[8,160,128]{2,1,0:T(8,128)(2,1)S(1)}, u32[]{:S(2)}, u32[]{:S(2)}) %all-to-all-start.2) | async-done | bytes 327712 | tf_op jit(solution)/shard_map/all_to_all | solution.py:291
  116.8 5.1 %all-to-all-start.3 = ((bf16[16,192,128]{2,1,0:T(8,128)(2,1)}), bf16[16,192,128]{2,1,0:T(8,128)(2,1)S(1)}, u32[]{:S(2)}, u32[]{:S(2)}) async-start(bf16[16,192,128]{2,1,0:T(8,128)(2,1)} %get-tuple-element.10), calls=%async_computation.3 | async-start | bytes 1572864 | tf_op jit(solution)/shard_map/all_to_all | solution.py:291
  121.9 2.4 %shard_map.161 = bf16[128,128]{1,0:T(8,128)(2,1)} custom-call(bf16[8,160,128]{2,1,0:T(8,128)(2,1)} %copy-done.3), custom_call_target="tpu_custom_call" | custom-call | tf_op jit(solution)/shard_map/pallas_call | solution.py:287
  124.3 32.7 %all-gather = bf16[2048,128]{1,0:T(8,128)(2,1)} all-gather(bf16[128,128]{1,0:T(8,128)(2,1)} %shard_map.161), channel_id=2, replica_groups=mesh['ep_0'=8,'ep_1'=4,'tp_0'=8,'tp_1'=2] {'tp_0','tp_1'}, dimensions={0}, use_global_device_ids=true | all-gather | bytes 557056 | tf_op jit(solution)/shard_map/all_gather | solution.py:403
  157.0 0.9 copy-done
  157.9 2.4 %shard_map.163 = bf16[8,256,128]{2,1,0:T(8,128)(2,1)} custom-call(bf16[16,128,128]{2,1,0:T(8,128)(2,1)} %bitcast.15, bf16[16,192,128]{2,1,0:T(8,128)(2,1)} %copy-done), custom_call_target="tpu_custom_call" | custom-call | tf_op jit(solution)/shard_map/pallas_call | solution.py:287
  160.3 23.3 %all_to_all.39.mine = bf16[8,256,128]{2,1,0:T(8,128)(2,1)S(1)} all-to-all(bf16[8,256,128]{2,1,0:T(8,128)(2,1)} %shard_map.163), channel_id=1, replica_groups=mesh['ep_0'=8,'ep_1'=4,'tp_0'=8,'tp_1'=2] {'tp_0'}, dimensions={0} | all-to-all | bytes 1048576 | tf_op jit(solution)/shard_map/all_to_all | solution.py:291
  183.7 2.5 %collective-permute-start = (bf16[8,256,128]{2,1,0:T(8,128)(2,1)S(1)}, bf16[8,256,128]{2,1,0:T(8,128)(2,1)S(1)}, u32[]{:S(2)}, u32[]{:S(2)}) collective-permute-start(bf16[8,256,128]{2,1,0:T(8,128)(2,1)S(1)} %all_to_all.39.mine), channel_id=1, source_target_pairs={{0,1},{1,0},{2,3},{3,2},{4,5},{5,4},{6,7},{7,6},{8,9},{9,8},{10,11... | collective-permute-start | bytes 1572872 | tf_op jit(solution)/shard_map/ppermute | solution.py:295
  186.2 3.2 %shard_map.166 = bf16[512,128]{1,0:T(8,128)(2,1)} custom-call(bf16[16,512,128]{2,1,0:T(8,128)(2,1)} %bitcast.16, bf16[16,192,128]{2,1,0:T(8,128)(2,1)} %copy-done), custom_call_target="tpu_custom_call" | custom-call | tf_op jit(solution)/shard_map/pallas_call | solution.py:287
  189.4 7.5 %all-to-all-start.5 = ((bf16[32,16,128]{2,1,0:T(8,128)(2,1)}), bf16[32,16,128]{2,1,0:T(8,128)(2,1)S(1)}, u32[]{:S(2)}, u32[]{:S(2)}) async-start(bf16[32,16,128]{2,1,0:T(8,128)(2,1)} %bitcast.17), calls=%async_computation.5 | async-start | bytes 262144 | tf_op jit(solution)/shard_map/all_to_all | solution.py:291
  197.0 0.8 copy-done.4
  197.8 2.7 %shard_map.164 = bf16[256,2048]{1,0:T(8,128)(2,1)} custom-call(s32[1]{0:T(128)} %bitcast.core_ref, bf16[8,256,128]{2,1,0:T(8,128)(2,1)} %copy-done.2, bf16[8,256,128]{2,1,0:T(8,128)(2,1)} %copy-done.4, bf16[2048]{0:T(1024)(128)(2,1)} %gain.3), custom_call_target="tpu_custom_call" | custom-call | tf_op jit(solution)/shard_map/pallas_call | solution.py:287
  200.5 6.4 %all-to-all-done.5 = bf16[32,16,128]{2,1,0:T(8,128)(2,1)S(1)} async-done(((bf16[32,16,128]{2,1,0:T(8,128)(2,1)}), bf16[32,16,128]{2,1,0:T(8,128)(2,1)S(1)}, u32[]{:S(2)}, u32[]{:S(2)}) %all-to-all-start.5) | async-done | bytes 131104 | tf_op jit(solution)/shard_map/all_to_all | solution.py:291
  207.1 0.6 fusion
  (22 shorter events, 0.4 us)
Async XLA Ops:
  7.2 79.7 %all-gather.6.cloned.1.call-start = ((), (), s32[]{:S(2)}) async-start(), calls=%async_computation.6 | async-start | bytes 2297856 | tf_op jit(solution)/shard_map/all_gather | solution.py:357
  7.2 39.1 %copy-start.6 = (bf16[128]{0:T(256)(128)(2,1)S(1)}, bf16[128]{0:T(256)(128)(2,1)}, u32[]{:S(2)}) copy-start(bf16[128]{0:T(256)(128)(2,1)} %param.24) | copy-start | bytes 772
  46.2 44.4 %copy-start.1 = (bf16[8,192,128]{2,1,0:T(8,128)(2,1)}, bf16[8,192,128]{2,1,0:T(8,128)(2,1)S(1)}, u32[]{:S(2)}) copy-start(bf16[8,192,128]{2,1,0:T(8,128)(2,1)S(1)} %all_to_all.38.asked) | copy-start | bytes 1179652
  47.1 139.1 %all-gather.8.cloned.1.call-start = ((), (), s32[]{:S(2)}) async-start(), calls=%async_computation.7 | async-start | bytes 2228224 | tf_op jit(solution)/shard_map/all_gather | solution.py:396
  99.3 17.5 %all-to-all-start.2 = ((bf16[8,160,128]{2,1,0:T(8,128)(2,1)}), bf16[8,160,128]{2,1,0:T(8,128)(2,1)S(1)}, u32[]{:S(2)}, u32[]{:S(2)}) async-start(bf16[8,160,128]{2,1,0:T(8,128)(2,1)} %shard_map.160), calls=%async_computation.2 | async-start | bytes 655360 | tf_op jit(solution)/shard_map/all_to_all | solution.py:291
  116.8 5.1 %copy-start.3 = (bf16[8,160,128]{2,1,0:T(8,128)(2,1)}, bf16[8,160,128]{2,1,0:T(8,128)(2,1)S(1)}, u32[]{:S(2)}) copy-start(bf16[8,160,128]{2,1,0:T(8,128)(2,1)S(1)} %all-to-all-done.2.partial) | copy-start | bytes 983044
  116.8 40.2 %all-to-all-start.3 = ((bf16[16,192,128]{2,1,0:T(8,128)(2,1)}), bf16[16,192,128]{2,1,0:T(8,128)(2,1)S(1)}, u32[]{:S(2)}, u32[]{:S(2)}) async-start(bf16[16,192,128]{2,1,0:T(8,128)(2,1)} %get-tuple-element.10), calls=%async_computation.3 | async-start | bytes 1572864 | tf_op jit(solution)/shard_map/all_to_all | solution.py:291
  157.0 0.9 copy-start
  183.7 13.3 %copy-start.2 = (bf16[8,256,128]{2,1,0:T(8,128)(2,1)}, bf16[8,256,128]{2,1,0:T(8,128)(2,1)S(1)}, u32[]{:S(2)}) copy-start(bf16[8,256,128]{2,1,0:T(8,128)(2,1)S(1)} %all_to_all.39.mine) | copy-start | bytes 1572868
  183.7 13.3 %collective-permute-start = (bf16[8,256,128]{2,1,0:T(8,128)(2,1)S(1)}, bf16[8,256,128]{2,1,0:T(8,128)(2,1)S(1)}, u32[]{:S(2)}, u32[]{:S(2)}) collective-permute-start(bf16[8,256,128]{2,1,0:T(8,128)(2,1)S(1)} %all_to_all.39.mine), channel_id=1, source_target_pairs={{0,1},{1,0},{2,3},{3,2},{4,5},{5,4},{6,7},{7,6},{8,9},{9,8},{10,11... | collective-permute-start | bytes 1572872 | tf_op jit(solution)/shard_map/ppermute | solution.py:295
  186.2 20.7 %copy-start.5 = (bf16[2,96,512]{2,1,0:T(8,128)(2,1)S(1)}, bf16[2,96,512]{2,1,0:T(8,128)(2,1)}, u32[]{:S(2)}) copy-start(bf16[2,96,512]{2,1,0:T(8,128)(2,1)} %get-tuple-element.11) | copy-start | bytes 589828
  189.4 17.5 %all-to-all-start.5 = ((bf16[32,16,128]{2,1,0:T(8,128)(2,1)}), bf16[32,16,128]{2,1,0:T(8,128)(2,1)S(1)}, u32[]{:S(2)}, u32[]{:S(2)}) async-start(bf16[32,16,128]{2,1,0:T(8,128)(2,1)} %bitcast.17), calls=%async_computation.5 | async-start | bytes 262144 | tf_op jit(solution)/shard_map/all_to_all | solution.py:291
  197.0 0.8 copy-start.4
Sparse Core Ops, SparseCore 0:
  47.2 39.6 all-gather.5
  90.8 45.6 all-gather.7

commit v7 on v6

--- a/solution.py
+++ b/solution.py
@@ -88,20 +88,22 @@
         payload[x, :positions, :] = pairs
 
 
-def columns_kernel(w_down, w_out, table, out, turned):
-    parts, _, width = out.shape
+def halves_kernel(core_ref, w_out, keep, give):
+    core = core_ref[0]
+    width = w_out.shape[1] // (2 * (keep.shape[1] // 128))
+    for k in range(keep.shape[1] // width):
+        for out, which in ((keep, core), (give, 1 - core)):
+            at = pl.ds(pl.multiple_of((2 * k + which) * width, width), width)
+            out[:, k * width : (k + 1) * width] = w_out[:, at]
+
+
+def turn_kernel(table, turned):
     scale = table[...]
-    slots, _ = scale.shape
-    turn = identity(slots).astype(jnp.bfloat16)
+    turn = identity(scale.shape[0]).astype(jnp.bfloat16)
     for k in range(turned.shape[0]):
         piece = scale.astype(jnp.bfloat16)
         scale = scale - piece.astype(jnp.float32)
         turned[k] = dot(piece, turn, ((0,), (0,))).astype(jnp.bfloat16)
-    hidden = w_down.shape[1]
-    for k in range(parts):
-        at = slice(k * width, (k + 1) * width)
-        out[k, :hidden, :] = w_down[0, :, at]
-        out[k, hidden:, :] = w_out[:, at]
 
 
 def relay_kernel(payload, queries, out):
@@ -218,40 +220,49 @@
     out[...] = jnp.concatenate([total[:half], total[half:]], axis=1)
 
 
-def mix_columns_kernel(attended, weights, out):
-    parts, half, width = attended.shape
+def product_kernel(mine, theirs, keep, given, out):
+    half, width = mine.shape
     head = width // 2
-    skip = weights.shape[1] - head
-    side = jnp.concatenate([weights[k, skip:, :] for k in range(parts)], axis=0)
-    top = jnp.concatenate([attended[k][:, :head] for k in range(parts)], axis=1)
-    low = jnp.concatenate([attended[k][:, head:] for k in range(parts)], axis=1)
+    top = jnp.concatenate([mine[:, :head], theirs[:, :head]], axis=1)
+    low = jnp.concatenate([mine[:, head:], theirs[:, head:]], axis=1)
+    side = jnp.concatenate([keep[...], given[...]], axis=0)
     top = dot(top, side).astype(out.dtype)
     low = dot(low, side).astype(out.dtype)
-    for copy in range(out.shape[0]):
-        out[copy, :half, :] = top
-        out[copy, half:, :] = low
-
-
-def mix_norm_kernel(core_ref, mine, theirs, gain, out):
+    size = out.shape[2]
+    for k in range(out.shape[0]):
+        out[k, :half, :] = top[:, k * size : (k + 1) * size]
+        out[k, half:, :] = low[:, k * size : (k + 1) * size]
+
+
+def total_kernel(parts, out):
+    total = parts[0].astype(jnp.float32)
+    for k in range(1, parts.shape[0]):
+        total = total + parts[k].astype(jnp.float32)
+    out[...] = total.astype(out.dtype)
+
+
+def pair_kernel(mine, theirs, out):
+    for k in range(out.shape[0]):
+        total = mine[k].astype(jnp.float32) + theirs[k].astype(jnp.float32)
+        out[k] = total.astype(out.dtype)
+
+
+def mix_norm_kernel(columns, gain, out):
+    parts, rows, width = columns.shape
+    total = jnp.zeros((rows, 1), jnp.float32)
+    for k in range(parts):
+        numbers = columns[k].astype(jnp.float32)
+        total = total + jnp.sum(numbers * numbers, axis=1, keepdims=True)
+    factor = row_factor(total, parts * width)
+    scale = gain[...].astype(jnp.float32)[None]
+    for k in range(parts):
+        at = slice(k * width, (k + 1) * width)
+        numbers = columns[k].astype(jnp.float32) * factor * scale[:, at]
+        out[:, at] = numbers.astype(out.dtype)
+
+
+def expert_kernel(core_ref, arrived, w_gate, w_up, w_down, keep, give, scaled, both):
     core = core_ref[0]
-    groups, rows, width = mine.shape
-    total = jnp.zeros((rows, width), jnp.float32)
-    for k in range(groups):
-        for side in (mine, theirs):
-            numbers = side[k].astype(jnp.float32)
-            total = total + numbers * numbers
-    factor = row_factor(jnp.sum(total, axis=1, keepdims=True), 2 * groups * width)
-    scale = gain[...].astype(jnp.float32)[None]
-    first = core == 0
-    for k in range(groups):
-        pair = (mine[k].astype(jnp.float32), theirs[k].astype(jnp.float32))
-        for which in range(2):
-            at = slice((2 * k + which) * width, (2 * k + which + 1) * width)
-            numbers = jnp.where(first, pair[which], pair[1 - which])
-            out[:, at] = (numbers * factor * scale[:, at]).astype(out.dtype)
-
-
-def expert_kernel(arrived, w_gate, w_up, out, scaled, both):
     parts, padded, width = arrived.shape
     rows = padded - PAD
     hidden = w_gate.shape[2]
@@ -268,17 +279,11 @@
     gate = jnp.minimum(pre[:, :hidden], CLAMP_LIMIT)
     up = jnp.clip(pre[:, hidden:], -CLAMP_LIMIT, CLAMP_LIMIT)
     units = (up + 1.0) * (gate * jax.nn.sigmoid(SILU_SHARPNESS * gate))
-    out[...] = units.astype(out.dtype)
-
-
-def down_kernel(hidden, weights, out):
-    parts, _, width = hidden.shape
-    total = jnp.zeros(out.shape, jnp.float32)
-    for k in range(0, parts, 2):
-        both = jnp.concatenate([hidden[k], hidden[k + 1]], axis=1)
-        side = jnp.concatenate([weights[k, :width, :], weights[k + 1, :width, :]], axis=0)
-        total = total + dot(both, side)
-    out[...] = total.astype(out.dtype)
+    units = units.astype(keep.dtype)
+    for k in range(keep.shape[0]):
+        for out, which in ((keep, core), (give, 1 - core)):
+            at = pl.ds(pl.multiple_of((2 * k + which) * width, width), width)
+            out[k] = dot(units, w_down[0, :, at]).astype(out.dtype)
 
 
 def call(body, outs, *args, scalars=0, **kwargs):
@@ -348,7 +353,10 @@
     )
     payload = exchanged(payload, "ep_1")
     asked = call(
-        relay_kernel, shape((along, across * capacity + half, part), bf16), payload, queries
+        relay_kernel,
+        shape((along, across * capacity + half, part), bf16),
+        payload,
+        queries,
     )
     asked = exchanged(asked, "ep_0")
     arrived = asked[:, : across * capacity].reshape(slots, part)
@@ -356,17 +364,17 @@
     every_row = jnp.concatenate([arrived, gain_rows], axis=0)
     every_row = lax.all_gather(every_row, TP, axis=0)
 
-    columns, turned = call(
-        columns_kernel,
-        (
-            shape((tp_count, w_down.shape[1] + head, model // tp_count), bf16),
-            shape((2, tokens, slots), bf16),
-        ),
-        w_down,
+    groups = tp_count // 2
+    size = model // tp_count
+    keep_out, give_out = call(
+        halves_kernel,
+        (shape((head, groups * size), bf16), shape((head, groups * size), bf16)),
+        core,
         w_out,
-        table,
-    )
-    columns = exchanged(columns, TP)
+        scalars=1,
+    )
+    given_out = from_partner(give_out)
+    turned = call(turn_kernel, shape((2, tokens, slots), bf16), table)
 
     partial = call(
         attend_kernel,
@@ -381,42 +389,42 @@
     partial = exchanged(partial, "ep_0")
     attended = call(gather_kernel, shape((half, 2 * head), bf16), partial)
 
+    products = call(
+        product_kernel,
+        shape((groups, rows, size), bf16),
+        attended,
+        from_partner(attended),
+        keep_out,
+        given_out,
+    )
+    products = exchanged(products, "tp_0")
+    own_columns = call(total_kernel, shape((rows, size), bf16), products)
+    every_column = lax.all_gather(own_columns, TP, axis=0)
+    mix_out = call(mix_norm_kernel, shape((rows, model), bf16), every_column, out_gain)
+
     units = w_gate.shape[2]
-    hidden = call(
+    keep, give = call(
         expert_kernel,
-        shape((slots, units), bf16),
+        (shape((groups, slots, size), bf16), shape((groups, slots, size), bf16)),
+        core,
         every_row,
         w_gate,
         w_up,
+        w_down,
+        scalars=1,
         scratch_shapes=[
             pltpu.VMEM((slots, model), bf16),
             pltpu.VMEM((model, 2 * units), bf16),
         ],
     )
-    every_hidden = lax.all_gather(hidden, TP, axis=0)
-    expert_out = call(down_kernel, shape((slots, part), bf16), every_hidden, columns)
-    returned = exchanged(expert_out, EP)
-    returned = returned.reshape(slots, part)
+    sums = call(
+        pair_kernel, shape((groups, slots, size), bf16), keep, from_partner(give)
+    )
+    sums = exchanged(sums, "tp_0")
+    expert_out = call(total_kernel, shape((slots, size), bf16), sums)
+    returned = exchanged(expert_out, EP).reshape(slots, part)
     combined = dot(turned.reshape(2 * tokens, slots), returned).reshape(2, tokens, part)
     exp_out = (combined[0] + combined[1]).astype(bf16)
-
-    every_head = lax.all_gather(attended, TP, axis=0)
-    own_columns = call(
-        mix_columns_kernel,
-        shape((tp_count // 2, rows, model // tp_count), bf16),
-        every_head,
-        columns,
-    )
-    mine = exchanged(own_columns, "tp_0")
-    mix_out = call(
-        mix_norm_kernel,
-        shape((rows, model), bf16),
-        core,
-        mine,
-        from_partner(mine),
-        out_gain,
-        scalars=1,
-    )
     return (mix_out, exp_out)
 
 

time: 215 us -> 191 us (0.89)
  blocking collectives: 90 us -> 33.9 us
  starting transfers between devices: 19 us -> 31.8 us
  waiting for transfers between devices: 57.3 us -> 66.3 us
  Pallas kernels: 30.8 us -> 37.6 us
    all_gather x1 -> x0, blocking collectives: 32.7 us -> none  [on_device(): every_head = lax.all_gather(attended, TP, axis=0)]
    all_to_all x3 -> x4, waiting for transfers between devices: 17.6 us -> 41.2 us  [exchanged(): return lax.all_to_all(value, axis, 0, 0, tiled=True)]
    all_to_all x3 -> x2, blocking collectives: 57.3 us -> 33.9 us  [exchanged(): return lax.all_to_all(value, axis, 0, 0, tiled=True)]
    all_gather x1, waiting for transfers between devices: 39.7 us -> 20.2 us  [on_device(): every_row = lax.all_gather(every_row, TP, axis=0)]
    ppermute x1 -> x3, starting transfers between devices: 2.49 us -> 10.1 us  [from_partner(): return lax.ppermute(value, 'tp_1', [(0, 1), (1, 0)])]
    pallas_call x9 -> x12, Pallas kernels: 30.8 us -> 37.6 us  [call(): return pl.pallas_call(body, out_shape=outs, in_specs=specs, **kwargs)(*args)]
    all_to_all x3 -> x4, starting transfers between devices: 16.4 us -> 21.6 us  [exchanged(): return lax.all_to_all(value, axis, 0, 0, tiled=True)]
    all_gather x1, waiting for transfers between devices: 0.02 us -> 3.71 us  [on_device(): every_column = lax.all_gather(own_columns, TP, axis=0)]
  transfers between devices with their start and end apart: 6 -> 9, of which waited for: 3 -> 6; matrix products, arithmetic and copies ran while one was open for 0% -> 0% of each run, Pallas kernels for 10% -> 17%
where the time goes in v7:
time: 191 us; the launch traced here: 189 us
  waiting for transfers between devices  66.3 us (35%)
  Pallas kernels  37.6 us (20%)
  blocking collectives  33.9 us (18%)
  starting transfers between devices  31.8 us (17%)
  between operations  14.2 us (7%)
  local copies, waits for them, and re-layouts  3.31 us (2%)
    all_to_all x4, waiting for transfers between devices, exchanged(): return lax.all_to_all(value, axis, 0, 0, tiled=True)  41.2 us
    pallas_call x12, Pallas kernels, call(): return pl.pallas_call(body, out_shape=outs, in_specs=specs, **kwargs)(*args)  37.6 us
    all_to_all x2, blocking collectives, exchanged(): return lax.all_to_all(value, axis, 0, 0, tiled=True)  33.9 us
    all_to_all x4, starting transfers between devices, exchanged(): return lax.all_to_all(value, axis, 0, 0, tiled=True)  21.6 us
    all_gather x1, waiting for transfers between devices, on_device(): every_row = lax.all_gather(every_row, TP, axis=0)  20.2 us
    ppermute x3, starting transfers between devices, from_partner(): return lax.ppermute(value, 'tp_1', [(0, 1), (1, 0)])  10.1 us
  transfers between devices with their start and end apart: 9, of which 6 were waited for; matrix products, arithmetic and copies ran while one was open for 0% of the time, Pallas kernels for 17%

profile of v7, /device:TPU:1, one launch (start us, length us, event | category | flops | bytes accessed | tf_op | source)
XLA Modules:
  0.0 188.6 jit_solution(16005389624291771111)
XLA Ops:
  7.2 3.3 %shard_map.158 = (bf16[128,128]{1,0:T(8,128)(2,1)}, bf16[4,384,128]{2,1,0:T(8,128)(2,1)}, f32[512,96]{1,0:T(8,128)}) custom-call(s32[4,96]{1,0:T(4,128)} %bitcast.19, f32[4,96]{1,0:T(4,128)} %bitcast.20, bf16[96,128]{1,0:T(8,128)(2,1)} %rows.1, bf16[256,2048]{1,0:T(8,128)(2,1)} %mix_rows.1, bf16[2048]{0:T(1024)(128)(2,1)} %gain.2, bf16[64,2048]{1,0:T(8,128)(2,1)} %w_query.1, ...), custom_call_target="tpu_custom_call" | custom-call | tf_op jit(solution)/shard_map/pallas_call | solution.py:292
  10.5 11.2 %all_to_all.37.payload = bf16[4,384,128]{2,1,0:T(8,128)(2,1)} all-to-all(bf16[4,384,128]{2,1,0:T(8,128)(2,1)} %get-tuple-element.9), channel_id=1, replica_groups=mesh['ep_0'=8,'ep_1'=4,'tp_0'=8,'tp_1'=2] {'ep_1'}, dimensions={0} | all-to-all | bytes 786432 | tf_op jit(solution)/shard_map/all_to_all | solution.py:296
  21.7 1.8 shard_map.159
  23.5 22.8 %all_to_all.38.asked = bf16[8,192,128]{2,1,0:T(8,128)(2,1)S(1)} all-to-all(bf16[8,192,128]{2,1,0:T(8,128)(2,1)} %shard_map.159), channel_id=1, replica_groups=mesh['ep_0'=8,'ep_1'=4,'tp_0'=8,'tp_1'=2] {'ep_0'}, dimensions={0} | all-to-all | bytes 786432 | tf_op jit(solution)/shard_map/all_to_all | solution.py:296
  47.1 8.6 %shard_map.160 = bf16[8,160,128]{2,1,0:T(8,128)(2,1)} custom-call(s32[1]{0:T(128)} %bitcast.z_ref, s32[1]{0:T(128)} %bitcast.1.x_ref, bf16[4,384,128]{2,1,0:T(8,128)(2,1)} %all_to_all.37.payload, bf16[8,192,128]{2,1,0:T(8,128)(2,1)} %copy-done.1, f32[1,8192]{1,0:T(1,128)} %offsets.1), custom_call_target="tpu_custom_call" | custom-call | tf_op jit(solution)/shard_map/pallas_call | solution.py:292
  55.7 3.4 %all-to-all-start.2 = ((bf16[8,160,128]{2,1,0:T(8,128)(2,1)}), bf16[8,160,128]{2,1,0:T(8,128)(2,1)S(1)}, u32[]{:S(2)}, u32[]{:S(2)}) async-start(bf16[8,160,128]{2,1,0:T(8,128)(2,1)} %shard_map.160), calls=%async_computation.2 | async-start | bytes 655360 | tf_op jit(solution)/shard_map/all_to_all | solution.py:296
  59.1 1.7 shard_map.162
  60.9 5.8 %collective-permute-start.1 = (bf16[64,1024]{1,0:T(8,128)(2,1)}, bf16[64,1024]{1,0:T(8,128)(2,1)S(1)}, u32[]{:S(2)}, u32[]{:S(2)}) collective-permute-start(bf16[64,1024]{1,0:T(8,128)(2,1)} %get-tuple-element.12), channel_id=1, source_target_pairs={{0,1},{1,0},{2,3},{3,2},{4,5},{5,4},{6,7},{7,6},{8,9},{9,8},{10,11... | collective-permute-start | bytes 393224 | tf_op jit(solution)/shard_map/ppermute | solution.py:300
  66.7 20.2 %all-gather.7.cloned.1.call-done = bf16[8448,128]{1,0:T(8,128)(2,1)} async-done(((bf16[528,128]{1,0:T(8,128)(2,1)}), bf16[8448,128]{1,0:T(8,128)(2,1)}) %all-gather.7.cloned.1.call-update) | async-done | bytes 2162704 | tf_op jit(solution)/shard_map/all_gather | solution.py:365
  86.8 5.9 %shard_map.167 = (bf16[8,512,128]{2,1,0:T(8,128)(2,1)}, bf16[8,512,128]{2,1,0:T(8,128)(2,1)}) custom-call(s32[1]{0:T(128)} %bitcast.4.core_ref, bf16[16,528,128]{2,1,0:T(8,128)(2,1)} %bitcast.13, bf16[1,2048,128]{2,1,0:T(8,128)(2,1)} %w_gate.1, bf16[1,2048,128]{2,1,0:T(8,128)(2,1)} %w_up.1, bf16[1,128,2048]{2,1,0:T(8,128)(2,1)} %w_down.1), custom_call_target="tpu_custom_call" | custom-call | tf_op jit(solution)/shard_map/pallas_call | solution.py:292
  92.8 2.2 %collective-permute-start.2 = (bf16[8,512,128]{2,1,0:T(8,128)(2,1)}, bf16[8,512,128]{2,1,0:T(8,128)(2,1)S(1)}, u32[]{:S(2)}, u32[]{:S(2)}) collective-permute-start(bf16[8,512,128]{2,1,0:T(8,128)(2,1)} %get-tuple-element.15), channel_id=1, source_target_pairs={{0,1},{1,0},{2,3},{3,2},{4,5},{5,4},{6,7},{7,6},{8,9},{9,8},{10,11... | collective-permute-start | bytes 3145736 | tf_op jit(solution)/shard_map/ppermute | solution.py:300
  95.7 2.4 %shard_map.161.mine = bf16[128,128]{1,0:T(8,128)(2,1)} custom-call(bf16[8,160,128]{2,1,0:T(8,128)(2,1)} %copy-done.3), custom_call_target="tpu_custom_call" | custom-call | tf_op jit(solution)/shard_map/pallas_call | solution.py:292
  98.1 2.1 %collective-permute-start = (bf16[128,128]{1,0:T(8,128)(2,1)}, bf16[128,128]{1,0:T(8,128)(2,1)S(1)}, u32[]{:S(2)}, u32[]{:S(2)}) collective-permute-start(bf16[128,128]{1,0:T(8,128)(2,1)} %shard_map.161.mine), channel_id=1, source_target_pairs={{0,1},{1,0},{2,3},{3,2},{4,5},{5,4},{6,7},{7,6},{8,9},{9,8},{10,11... | collective-permute-start | bytes 98312 | tf_op jit(solution)/shard_map/ppermute | solution.py:300
  102.1 2.2 %shard_map.163 = bf16[8,256,128]{2,1,0:T(8,128)(2,1)} custom-call(bf16[128,128]{1,0:T(8,128)(2,1)} %shard_map.161.mine, bf16[128,128]{1,0:T(8,128)(2,1)} %copy-done.7, bf16[64,1024]{1,0:T(8,128)(2,1)} %get-tuple-element.11.keep, bf16[64,1024]{1,0:T(8,128)(2,1)} %copy-done.6), custom_call_target="tpu_custom_call" | custom-call | tf_op jit(solution)/shard_map/pallas_call | solution.py:292
  104.2 4.2 %all-to-all-start.3 = ((bf16[8,256,128]{2,1,0:T(8,128)(2,1)}), bf16[8,256,128]{2,1,0:T(8,128)(2,1)S(1)}, u32[]{:S(2)}, u32[]{:S(2)}) async-start(bf16[8,256,128]{2,1,0:T(8,128)(2,1)} %shard_map.163), calls=%async_computation.3 | async-start | bytes 1048576 | tf_op jit(solution)/shard_map/all_to_all | solution.py:296
  109.5 2.8 %shard_map.168 = bf16[8,512,128]{2,1,0:T(8,128)(2,1)} custom-call(bf16[8,512,128]{2,1,0:T(8,128)(2,1)} %get-tuple-element.14.mine, bf16[8,512,128]{2,1,0:T(8,128)(2,1)} %copy-done.4), custom_call_target="tpu_custom_call" | custom-call | tf_op jit(solution)/shard_map/pallas_call | solution.py:292
  112.2 14.2 %all-to-all-done.3.parts = bf16[8,256,128]{2,1,0:T(8,128)(2,1)S(1)} async-done(((bf16[8,256,128]{2,1,0:T(8,128)(2,1)}), bf16[8,256,128]{2,1,0:T(8,128)(2,1)S(1)}, u32[]{:S(2)}, u32[]{:S(2)}) %all-to-all-start.3) | async-done | bytes 524320 | tf_op jit(solution)/shard_map/all_to_all | solution.py:296
  126.4 3.6 %all-to-all-start.4 = ((bf16[8,512,128]{2,1,0:T(8,128)(2,1)}), bf16[8,512,128]{2,1,0:T(8,128)(2,1)S(1)}, u32[]{:S(2)}, u32[]{:S(2)}) async-start(bf16[8,512,128]{2,1,0:T(8,128)(2,1)} %shard_map.168), calls=%async_computation.4 | async-start | bytes 2097152 | tf_op jit(solution)/shard_map/all_to_all | solution.py:296
  131.8 26.4 %all-to-all-done.4.parts = bf16[8,512,128]{2,1,0:T(8,128)(2,1)S(1)} async-done(((bf16[8,512,128]{2,1,0:T(8,128)(2,1)}), bf16[8,512,128]{2,1,0:T(8,128)(2,1)S(1)}, u32[]{:S(2)}, u32[]{:S(2)}) %all-to-all-start.4) | async-done | bytes 1048608 | tf_op jit(solution)/shard_map/all_to_all | solution.py:296
  159.2 2.0 %shard_map.169 = bf16[512,128]{1,0:T(8,128)(2,1)} custom-call(bf16[8,512,128]{2,1,0:T(8,128)(2,1)} %copy-done), custom_call_target="tpu_custom_call" | custom-call | tf_op jit(solution)/shard_map/pallas_call | solution.py:292
  161.2 10.3 %all-to-all-start.5 = ((bf16[32,16,128]{2,1,0:T(8,128)(2,1)}), bf16[32,16,128]{2,1,0:T(8,128)(2,1)S(1)}, u32[]{:S(2)}, u32[]{:S(2)}) async-start(bf16[32,16,128]{2,1,0:T(8,128)(2,1)} %bitcast.16), calls=%async_computation.5 | async-start | bytes 262144 | tf_op jit(solution)/shard_map/all_to_all | solution.py:296
  171.6 2.0 %shard_map.166 = bf16[2,96,512]{2,1,0:T(8,128)(2,1)} custom-call(f32[512,96]{1,0:T(8,128)} %get-tuple-element.13.table), custom_call_target="tpu_custom_call" | custom-call | tf_op jit(solution)/shard_map/pallas_call | solution.py:292
  173.5 3.7 %all-gather.5.cloned.1.call-done = bf16[4096,128]{1,0:T(8,128)(2,1)} async-done(((bf16[256,128]{1,0:T(8,128)(2,1)}), bf16[4096,128]{1,0:T(8,128)(2,1)}) %all-gather.5.cloned.1.call-update) | async-done | bytes 1048592 | tf_op jit(solution)/shard_map/all_gather | solution.py:402
  177.2 3.1 %shard_map.165 = bf16[256,2048]{1,0:T(8,128)(2,1)} custom-call(bf16[16,256,128]{2,1,0:T(8,128)(2,1)} %bitcast.14, bf16[2048]{0:T(1024)(128)(2,1)} %gain.3), custom_call_target="tpu_custom_call" | custom-call | tf_op jit(solution)/shard_map/pallas_call | solution.py:292
  (33 shorter events, 8.4 us)
Async XLA Ops:
  7.2 79.7 %all-gather.7.cloned.1.call-start = ((), (), s32[]{:S(2)}) async-start(), calls=%async_computation.7 | async-start | bytes 2297856 | tf_op jit(solution)/shard_map/all_gather | solution.py:365
  7.2 39.1 %copy-start.8 = (bf16[128]{0:T(256)(128)(2,1)S(1)}, bf16[128]{0:T(256)(128)(2,1)}, u32[]{:S(2)}) copy-start(bf16[128]{0:T(256)(128)(2,1)} %param.24) | copy-start | bytes 772
  46.3 0.8 copy-start.1
  55.7 39.3 %all-to-all-start.2 = ((bf16[8,160,128]{2,1,0:T(8,128)(2,1)}), bf16[8,160,128]{2,1,0:T(8,128)(2,1)S(1)}, u32[]{:S(2)}, u32[]{:S(2)}) async-start(bf16[8,160,128]{2,1,0:T(8,128)(2,1)} %shard_map.160), calls=%async_computation.2 | async-start | bytes 655360 | tf_op jit(solution)/shard_map/all_to_all | solution.py:296
  60.9 39.4 %collective-permute-start.1 = (bf16[64,1024]{1,0:T(8,128)(2,1)}, bf16[64,1024]{1,0:T(8,128)(2,1)S(1)}, u32[]{:S(2)}, u32[]{:S(2)}) collective-permute-start(bf16[64,1024]{1,0:T(8,128)(2,1)} %get-tuple-element.12), channel_id=1, source_target_pairs={{0,1},{1,0},{2,3},{3,2},{4,5},{5,4},{6,7},{7,6},{8,9},{9,8},{10,11... | collective-permute-start | bytes 393224 | tf_op jit(solution)/shard_map/ppermute | solution.py:300
  92.8 15.7 %collective-permute-start.2 = (bf16[8,512,128]{2,1,0:T(8,128)(2,1)}, bf16[8,512,128]{2,1,0:T(8,128)(2,1)S(1)}, u32[]{:S(2)}, u32[]{:S(2)}) collective-permute-start(bf16[8,512,128]{2,1,0:T(8,128)(2,1)} %get-tuple-element.15), channel_id=1, source_target_pairs={{0,1},{1,0},{2,3},{3,2},{4,5},{5,4},{6,7},{7,6},{8,9},{9,8},{10,11... | collective-permute-start | bytes 3145736 | tf_op jit(solution)/shard_map/ppermute | solution.py:300
  95.0 0.7 copy-start.3
  98.1 3.3 %collective-permute-start = (bf16[128,128]{1,0:T(8,128)(2,1)}, bf16[128,128]{1,0:T(8,128)(2,1)S(1)}, u32[]{:S(2)}, u32[]{:S(2)}) collective-permute-start(bf16[128,128]{1,0:T(8,128)(2,1)} %shard_map.161.mine), channel_id=1, source_target_pairs={{0,1},{1,0},{2,3},{3,2},{4,5},{5,4},{6,7},{7,6},{8,9},{9,8},{10,11... | collective-permute-start | bytes 98312 | tf_op jit(solution)/shard_map/ppermute | solution.py:300
  100.3 1.2 copy-start.6
  101.4 0.6 copy-start.7
  104.2 22.2 %all-to-all-start.3 = ((bf16[8,256,128]{2,1,0:T(8,128)(2,1)}), bf16[8,256,128]{2,1,0:T(8,128)(2,1)S(1)}, u32[]{:S(2)}, u32[]{:S(2)}) async-start(bf16[8,256,128]{2,1,0:T(8,128)(2,1)} %shard_map.163), calls=%async_computation.3 | async-start | bytes 1048576 | tf_op jit(solution)/shard_map/all_to_all | solution.py:296
  108.5 1.0 copy-start.4
  126.4 3.6 %copy-start.2 = (bf16[8,256,128]{2,1,0:T(8,128)(2,1)}, bf16[8,256,128]{2,1,0:T(8,128)(2,1)S(1)}, u32[]{:S(2)}) copy-start(bf16[8,256,128]{2,1,0:T(8,128)(2,1)S(1)} %all-to-all-done.3.parts) | copy-start | bytes 1572868
  126.4 31.8 %all-to-all-start.4 = ((bf16[8,512,128]{2,1,0:T(8,128)(2,1)}), bf16[8,512,128]{2,1,0:T(8,128)(2,1)S(1)}, u32[]{:S(2)}, u32[]{:S(2)}) async-start(bf16[8,512,128]{2,1,0:T(8,128)(2,1)} %shard_map.168), calls=%async_computation.4 | async-start | bytes 2097152 | tf_op jit(solution)/shard_map/all_to_all | solution.py:296
  130.0 47.3 %all-gather.5.cloned.1.call-start = ((), (), s32[]{:S(2)}) async-start(), calls=%async_computation.6 | async-start | bytes 1114112 | tf_op jit(solution)/shard_map/all_gather | solution.py:402
  158.2 1.0 copy-start
  161.2 19.7 %all-to-all-start.5 = ((bf16[32,16,128]{2,1,0:T(8,128)(2,1)}), bf16[32,16,128]{2,1,0:T(8,128)(2,1)S(1)}, u32[]{:S(2)}, u32[]{:S(2)}) async-start(bf16[32,16,128]{2,1,0:T(8,128)(2,1)} %bitcast.16), calls=%async_computation.5 | async-start | bytes 262144 | tf_op jit(solution)/shard_map/all_to_all | solution.py:296
  173.5 7.4 %copy-start.5 = (bf16[2,96,512]{2,1,0:T(8,128)(2,1)S(1)}, bf16[2,96,512]{2,1,0:T(8,128)(2,1)}, u32[]{:S(2)}) copy-start(bf16[2,96,512]{2,1,0:T(8,128)(2,1)} %shard_map.166) | copy-start | bytes 589828
Sparse Core Ops, SparseCore 0:
  47.2 39.6 all-gather.6
  132.9 44.2 all-gather.4

commit v8 on v7

--- a/solution.py
+++ b/solution.py
@@ -88,13 +88,15 @@
         payload[x, :positions, :] = pairs
 
 
-def halves_kernel(core_ref, w_out, keep, give):
+def halves_kernel(core_ref, w_out, w_down, keep, give, keep_down, give_down):
     core = core_ref[0]
-    width = w_out.shape[1] // (2 * (keep.shape[1] // 128))
+    width = 128
     for k in range(keep.shape[1] // width):
-        for out, which in ((keep, core), (give, 1 - core)):
+        to = slice(k * width, (k + 1) * width)
+        for out, down, which in ((keep, keep_down, core), (give, give_down, 1 - core)):
             at = pl.ds(pl.multiple_of((2 * k + which) * width, width), width)
-            out[:, k * width : (k + 1) * width] = w_out[:, at]
+            out[:, to] = w_out[:, at]
+            down[:, to] = w_down[0, :, at]
 
 
 def turn_kernel(table, turned):
@@ -234,19 +236,6 @@
         out[k, half:, :] = low[:, k * size : (k + 1) * size]
 
 
-def total_kernel(parts, out):
-    total = parts[0].astype(jnp.float32)
-    for k in range(1, parts.shape[0]):
-        total = total + parts[k].astype(jnp.float32)
-    out[...] = total.astype(out.dtype)
-
-
-def pair_kernel(mine, theirs, out):
-    for k in range(out.shape[0]):
-        total = mine[k].astype(jnp.float32) + theirs[k].astype(jnp.float32)
-        out[k] = total.astype(out.dtype)
-
-
 def mix_norm_kernel(columns, gain, out):
     parts, rows, width = columns.shape
     total = jnp.zeros((rows, 1), jnp.float32)
@@ -261,8 +250,9 @@
         out[:, at] = numbers.astype(out.dtype)
 
 
-def expert_kernel(core_ref, arrived, w_gate, w_up, w_down, keep, give, scaled, both):
-    core = core_ref[0]
+def expert_kernel(
+    arrived, w_gate, w_up, keep_down, give_down, keep, give, scaled, both
+):
     parts, padded, width = arrived.shape
     rows = padded - PAD
     hidden = w_gate.shape[2]
@@ -280,16 +270,20 @@
     up = jnp.clip(pre[:, hidden:], -CLAMP_LIMIT, CLAMP_LIMIT)
     units = (up + 1.0) * (gate * jax.nn.sigmoid(SILU_SHARPNESS * gate))
     units = units.astype(keep.dtype)
-    for k in range(keep.shape[0]):
-        for out, which in ((keep, core), (give, 1 - core)):
-            at = pl.ds(pl.multiple_of((2 * k + which) * width, width), width)
-            out[k] = dot(units, w_down[0, :, at]).astype(out.dtype)
+    for out, down in ((give, give_down), (keep, keep_down)):
+        product = dot(units, down[...]).astype(out.dtype)
+        for k in range(out.shape[0]):
+            out[k] = product[:, k * width : (k + 1) * width]
 
 
 def call(body, outs, *args, scalars=0, **kwargs):
     spaces = [pltpu.SMEM] * scalars + [pltpu.VMEM] * (len(args) - scalars)
     specs = [pl.BlockSpec(memory_space=space) for space in spaces]
     return pl.pallas_call(body, out_shape=outs, in_specs=specs, **kwargs)(*args)
+
+
+def total(parts):
+    return jnp.sum(parts.astype(jnp.float32), axis=0).astype(parts.dtype)
 
 
 def exchanged(value, axis):
@@ -366,11 +360,14 @@
 
     groups = tp_count // 2
     size = model // tp_count
-    keep_out, give_out = call(
+    part_out = shape((head, groups * size), bf16)
+    part_down = shape((w_down.shape[1], groups * size), bf16)
+    keep_out, give_out, keep_down, give_down = call(
         halves_kernel,
-        (shape((head, groups * size), bf16), shape((head, groups * size), bf16)),
+        (part_out, part_out, part_down, part_down),
         core,
         w_out,
+        w_down,
         scalars=1,
     )
     given_out = from_partner(give_out)
@@ -398,30 +395,28 @@
         given_out,
     )
     products = exchanged(products, "tp_0")
-    own_columns = call(total_kernel, shape((rows, size), bf16), products)
-    every_column = lax.all_gather(own_columns, TP, axis=0)
-    mix_out = call(mix_norm_kernel, shape((rows, model), bf16), every_column, out_gain)
-
+    own_columns = total(products)
     units = w_gate.shape[2]
     keep, give = call(
         expert_kernel,
         (shape((groups, slots, size), bf16), shape((groups, slots, size), bf16)),
-        core,
         every_row,
         w_gate,
         w_up,
-        w_down,
-        scalars=1,
+        keep_down,
+        give_down,
         scratch_shapes=[
             pltpu.VMEM((slots, model), bf16),
             pltpu.VMEM((model, 2 * units), bf16),
         ],
     )
-    sums = call(
-        pair_kernel, shape((groups, slots, size), bf16), keep, from_partner(give)
-    )
+    sums = keep.astype(jnp.float32) + from_partner(give).astype(jnp.float32)
+    sums = sums.astype(bf16)
+    sums, own_columns = lax.optimization_barrier((sums, own_columns))
+    every_column = lax.all_gather(own_columns, TP, axis=0)
+    mix_out = call(mix_norm_kernel, shape((rows, model), bf16), every_column, out_gain)
     sums = exchanged(sums, "tp_0")
-    expert_out = call(total_kernel, shape((slots, size), bf16), sums)
+    expert_out = total(sums)
     returned = exchanged(expert_out, EP).reshape(slots, part)
     combined = dot(turned.reshape(2 * tokens, slots), returned).reshape(2, tokens, part)
     exp_out = (combined[0] + combined[1]).astype(bf16)

time: 191 us -> 190 us (level)
  blocking collectives: 33.9 us -> 56 us
  waiting for transfers between devices: 66.3 us -> 54.8 us
  Pallas kernels: 37.6 us -> 31.1 us
  starting transfers between devices: 31.8 us -> 27.6 us
  other arithmetic: 1.35 us -> 4.08 us
  local copies, waits for them, and re-layouts: 3.31 us -> 1.35 us
    all_to_all x2 -> x3, blocking collectives: 33.9 us -> 56 us  [exchanged(): return lax.all_to_all(value, axis, 0, 0, tiled=True)]
    all_to_all x4 -> x3, waiting for transfers between devices: 41.2 us -> 27.7 us  [exchanged(): return lax.all_to_all(value, axis, 0, 0, tiled=True)]
    pallas_call x12 -> x9, Pallas kernels: 37.6 us -> 31.1 us  [call(): return pl.pallas_call(body, out_shape=outs, in_specs=specs, **kwargs)(*args)]
    all_to_all x4 -> x3, starting transfers between devices: 21.6 us -> 17.3 us  [exchanged(): return lax.all_to_all(value, axis, 0, 0, tiled=True)]
    unnamed x18 -> x14, local copies, waits for them, and re-layouts: 3.29 us -> 1.34 us
  transfers between devices with their start and end apart: 9 -> 8, of which waited for: 6 -> 4; matrix products, arithmetic and copies ran while one was open for 0% -> 1% of each run, Pallas kernels for 17% -> 14%
where the time goes in v8:
time: 190 us; the launch traced here: 189 us
  blocking collectives  56 us (29%)
  waiting for transfers between devices  54.8 us (29%)
  Pallas kernels  31.1 us (16%)
  starting transfers between devices  27.6 us (15%)
  between operations  14.2 us (7%)
  other arithmetic  4.08 us (2%)
    all_to_all x3, blocking collectives, exchanged(): return lax.all_to_all(value, axis, 0, 0, tiled=True)  56 us
    pallas_call x9, Pallas kernels, call(): return pl.pallas_call(body, out_shape=outs, in_specs=specs, **kwargs)(*args)  31.1 us
    all_to_all x3, waiting for transfers between devices, exchanged(): return lax.all_to_all(value, axis, 0, 0, tiled=True)  27.7 us
    all_gather x1, waiting for transfers between devices, on_device(): every_row = lax.all_gather(every_row, TP, axis=0)  19.7 us
    all_to_all x3, starting transfers between devices, exchanged(): return lax.all_to_all(value, axis, 0, 0, tiled=True)  17.3 us
    ppermute x3, starting transfers between devices, from_partner(): return lax.ppermute(value, 'tp_1', [(0, 1), (1, 0)])  10.3 us
    all_gather x1, waiting for transfers between devices, on_device(): every_column = lax.all_gather(own_columns, TP, axis=0)  5.59 us
  transfers between devices with their start and end apart: 8, of which 4 were waited for; matrix products, arithmetic and copies ran while one was open for 1% of the time, Pallas kernels for 14%

profile of v8, /device:TPU:1, one launch (start us, length us, event | category | flops | bytes accessed | tf_op | source)
XLA Modules:
  0.0 189.4 jit_solution(6606343713374812916)
XLA Ops:
  7.2 3.3 %shard_map.158 = (bf16[128,128]{1,0:T(8,128)(2,1)}, bf16[4,384,128]{2,1,0:T(8,128)(2,1)}, f32[512,96]{1,0:T(8,128)}) custom-call(s32[4,96]{1,0:T(4,128)} %bitcast.18, f32[4,96]{1,0:T(4,128)} %bitcast.19, bf16[96,128]{1,0:T(8,128)(2,1)} %rows.1, bf16[256,2048]{1,0:T(8,128)(2,1)} %mix_rows.1, bf16[2048]{0:T(1024)(128)(2,1)} %gain.2, bf16[64,2048]{1,0:T(8,128)(2,1)} %w_query.1, ...), custom_call_target="tpu_custom_call" | custom-call | tf_op jit(solution)/shard_map/pallas_call | solution.py:282
  10.5 11.2 %all_to_all.37.payload = bf16[4,384,128]{2,1,0:T(8,128)(2,1)} all-to-all(bf16[4,384,128]{2,1,0:T(8,128)(2,1)} %get-tuple-element.13), channel_id=1, replica_groups=mesh['ep_0'=8,'ep_1'=4,'tp_0'=8,'tp_1'=2] {'ep_1'}, dimensions={0} | all-to-all | bytes 786432 | tf_op jit(solution)/shard_map/all_to_all | solution.py:290
  21.7 1.8 shard_map.159
  23.5 22.8 %all_to_all.38.asked = bf16[8,192,128]{2,1,0:T(8,128)(2,1)S(1)} all-to-all(bf16[8,192,128]{2,1,0:T(8,128)(2,1)} %shard_map.159), channel_id=1, replica_groups=mesh['ep_0'=8,'ep_1'=4,'tp_0'=8,'tp_1'=2] {'ep_0'}, dimensions={0} | all-to-all | bytes 786432 | tf_op jit(solution)/shard_map/all_to_all | solution.py:290
  47.1 8.6 %shard_map.162 = bf16[8,160,128]{2,1,0:T(8,128)(2,1)} custom-call(s32[1]{0:T(128)} %bitcast.5.z_ref, s32[1]{0:T(128)} %bitcast.6.x_ref, bf16[4,384,128]{2,1,0:T(8,128)(2,1)} %all_to_all.37.payload, bf16[8,192,128]{2,1,0:T(8,128)(2,1)} %copy-done, f32[1,8192]{1,0:T(1,128)} %offsets.1), custom_call_target="tpu_custom_call" | custom-call | tf_op jit(solution)/shard_map/pallas_call | solution.py:282
  55.7 3.4 %all-to-all-start.2 = ((bf16[8,160,128]{2,1,0:T(8,128)(2,1)}), bf16[8,160,128]{2,1,0:T(8,128)(2,1)S(1)}, u32[]{:S(2)}, u32[]{:S(2)}) async-start(bf16[8,160,128]{2,1,0:T(8,128)(2,1)} %shard_map.162), calls=%async_computation.2 | async-start | bytes 655360 | tf_op jit(solution)/shard_map/all_to_all | solution.py:290
  59.1 2.2 %shard_map.160 = (bf16[64,1024]{1,0:T(8,128)(2,1)}, bf16[64,1024]{1,0:T(8,128)(2,1)}, bf16[128,1024]{1,0:T(8,128)(2,1)}, bf16[128,1024]{1,0:T(8,128)(2,1)}) custom-call(s32[1]{0:T(128)} %bitcast.4.core_ref, bf16[64,2048]{1,0:T(8,128)(2,1)} %w_out.1, bf16[1,128,2048]{2,1,0:T(8,128)(2,1)} %w_down.1), custom_call_target="tpu_custom_call" | custom-call | tf_op jit(solution)/shard_map/pallas_call | solution.py:282
  61.4 5.8 %collective-permute-start.2 = (bf16[64,1024]{1,0:T(8,128)(2,1)}, bf16[64,1024]{1,0:T(8,128)(2,1)S(1)}, u32[]{:S(2)}, u32[]{:S(2)}) collective-permute-start(bf16[64,1024]{1,0:T(8,128)(2,1)} %get-tuple-element.20), channel_id=1, source_target_pairs={{0,1},{1,0},{2,3},{3,2},{4,5},{5,4},{6,7},{7,6},{8,9},{9,8},{10,11... | collective-permute-start | bytes 393224 | tf_op jit(solution)/shard_map/ppermute | solution.py:294
  67.2 19.7 %all-gather.5.cloned.1.call-done = bf16[8448,128]{1,0:T(8,128)(2,1)} async-done(((bf16[528,128]{1,0:T(8,128)(2,1)}), bf16[8448,128]{1,0:T(8,128)(2,1)}) %all-gather.5.cloned.1.call-update) | async-done | bytes 2162704 | tf_op jit(solution)/shard_map/all_gather | solution.py:359
  86.8 5.6 %shard_map.161 = (bf16[8,512,128]{2,1,0:T(8,128)(2,1)}, bf16[8,512,128]{2,1,0:T(8,128)(2,1)}) custom-call(bf16[16,528,128]{2,1,0:T(8,128)(2,1)} %bitcast.13, bf16[1,2048,128]{2,1,0:T(8,128)(2,1)} %w_gate.1, bf16[1,2048,128]{2,1,0:T(8,128)(2,1)} %w_up.1, bf16[128,1024]{1,0:T(8,128)(2,1)} %get-tuple-element.15.keep_down, ...), custom_call_target="tpu_custom_call" | custom-call | tf_op jit(solution)/shard_map/pallas_call | solution.py:282
  92.4 2.3 %collective-permute-start = (bf16[8,512,128]{2,1,0:T(8,128)(2,1)}, bf16[8,512,128]{2,1,0:T(8,128)(2,1)S(1)}, u32[]{:S(2)}, u32[]{:S(2)}) collective-permute-start(bf16[8,512,128]{2,1,0:T(8,128)(2,1)} %get-tuple-element.18), channel_id=1, source_target_pairs={{0,1},{1,0},{2,3},{3,2},{4,5},{5,4},{6,7},{7,6},{8,9},{9,8},{10,11... | collective-permute-start | bytes 3145736 | tf_op jit(solution)/shard_map/ppermute | solution.py:294
  95.5 2.4 %shard_map.163.mine = bf16[128,128]{1,0:T(8,128)(2,1)} custom-call(bf16[8,160,128]{2,1,0:T(8,128)(2,1)} %copy-done.1), custom_call_target="tpu_custom_call" | custom-call | tf_op jit(solution)/shard_map/pallas_call | solution.py:282
  97.9 2.1 %collective-permute-start.1 = (bf16[128,128]{1,0:T(8,128)(2,1)}, bf16[128,128]{1,0:T(8,128)(2,1)S(1)}, u32[]{:S(2)}, u32[]{:S(2)}) collective-permute-start(bf16[128,128]{1,0:T(8,128)(2,1)} %shard_map.163.mine), channel_id=1, source_target_pairs={{0,1},{1,0},{2,3},{3,2},{4,5},{5,4},{6,7},{7,6},{8,9},{9,8},{10,11... | collective-permute-start | bytes 98312 | tf_op jit(solution)/shard_map/ppermute | solution.py:294
  100.0 1.1 collective-permute-done.1.theirs
  101.8 2.1 %shard_map.164 = bf16[8,256,128]{2,1,0:T(8,128)(2,1)} custom-call(bf16[128,128]{1,0:T(8,128)(2,1)} %shard_map.163.mine, bf16[128,128]{1,0:T(8,128)(2,1)} %copy-done.5, bf16[64,1024]{1,0:T(8,128)(2,1)} %get-tuple-element.19.keep, bf16[64,1024]{1,0:T(8,128)(2,1)} %copy-done.4), custom_call_target="tpu_custom_call" | custom-call | tf_op jit(solution)/shard_map/pallas_call | solution.py:282
  103.9 22.1 %all_to_all.39 = bf16[8,256,128]{2,1,0:T(8,128)(2,1)S(1)} all-to-all(bf16[8,256,128]{2,1,0:T(8,128)(2,1)} %shard_map.164), channel_id=1, replica_groups=mesh['ep_0'=8,'ep_1'=4,'tp_0'=8,'tp_1'=2] {'tp_0'}, dimensions={0} | all-to-all | bytes 1048576 | tf_op jit(solution)/shard_map/all_to_all | solution.py:290
  126.7 1.2 add_convert_fusion
  127.9 3.6 %all-to-all-start.4 = ((bf16[8,512,128]{2,1,0:T(8,128)(2,1)}), bf16[8,512,128]{2,1,0:T(8,128)(2,1)S(1)}, u32[]{:S(2)}, u32[]{:S(2)}) async-start(bf16[8,512,128]{2,1,0:T(8,128)(2,1)} %add_convert_fusion), calls=%async_computation.4 | async-start | bytes 2097152 | tf_op jit(solution)/shard_map/all_to_all | solution.py:290
  132.2 27.7 %all-to-all-done.4 = bf16[8,512,128]{2,1,0:T(8,128)(2,1)S(1)} async-done(((bf16[8,512,128]{2,1,0:T(8,128)(2,1)}), bf16[8,512,128]{2,1,0:T(8,128)(2,1)S(1)}, u32[]{:S(2)}, u32[]{:S(2)}) %all-to-all-start.4) | async-done | bytes 1048608 | tf_op jit(solution)/shard_map/all_to_all | solution.py:290
  160.0 0.8 reduce_sum.25
  160.8 10.3 %all-to-all-start.5 = ((bf16[32,16,128]{2,1,0:T(8,128)(2,1)}), bf16[32,16,128]{2,1,0:T(8,128)(2,1)S(1)}, u32[]{:S(2)}, u32[]{:S(2)}) async-start(bf16[32,16,128]{2,1,0:T(8,128)(2,1)} %bitcast.9), calls=%async_computation.5 | async-start | bytes 262144 | tf_op jit(solution)/shard_map/all_to_all | solution.py:290
  171.0 2.0 %shard_map.166 = bf16[2,96,512]{2,1,0:T(8,128)(2,1)} custom-call(f32[512,96]{1,0:T(8,128)} %get-tuple-element.22.table), custom_call_target="tpu_custom_call" | custom-call | tf_op jit(solution)/shard_map/pallas_call | solution.py:282
  173.0 5.6 %all-gather.7.cloned.1.call-done = bf16[4096,128]{1,0:T(8,128)(2,1)} async-done(((bf16[256,128]{1,0:T(8,128)(2,1)}), bf16[4096,128]{1,0:T(8,128)(2,1)}) %all-gather.7.cloned.1.call-update) | async-done | bytes 1048592 | tf_op jit(solution)/shard_map/all_gather | solution.py:416
  178.6 3.1 %shard_map.165 = bf16[256,2048]{1,0:T(8,128)(2,1)} custom-call(bf16[16,256,128]{2,1,0:T(8,128)(2,1)} %bitcast.14, bf16[2048]{0:T(1024)(128)(2,1)} %gain.3), custom_call_target="tpu_custom_call" | custom-call | tf_op jit(solution)/shard_map/pallas_call | solution.py:282
  (28 shorter events, 4.4 us)
Async XLA Ops:
  7.2 79.7 %all-gather.5.cloned.1.call-start = ((), (), s32[]{:S(2)}) async-start(), calls=%async_computation.6 | async-start | bytes 2297856 | tf_op jit(solution)/shard_map/all_gather | solution.py:359
  7.2 39.1 %copy-start.6 = (bf16[128]{0:T(256)(128)(2,1)S(1)}, bf16[128]{0:T(256)(128)(2,1)}, u32[]{:S(2)}) copy-start(bf16[128]{0:T(256)(128)(2,1)} %param.24) | copy-start | bytes 772
  46.3 0.8 copy-start
  55.7 39.0 %all-to-all-start.2 = ((bf16[8,160,128]{2,1,0:T(8,128)(2,1)}), bf16[8,160,128]{2,1,0:T(8,128)(2,1)S(1)}, u32[]{:S(2)}, u32[]{:S(2)}) async-start(bf16[8,160,128]{2,1,0:T(8,128)(2,1)} %shard_map.162), calls=%async_computation.2 | async-start | bytes 655360 | tf_op jit(solution)/shard_map/all_to_all | solution.py:290
  61.4 38.7 %collective-permute-start.2 = (bf16[64,1024]{1,0:T(8,128)(2,1)}, bf16[64,1024]{1,0:T(8,128)(2,1)S(1)}, u32[]{:S(2)}, u32[]{:S(2)}) collective-permute-start(bf16[64,1024]{1,0:T(8,128)(2,1)} %get-tuple-element.20), channel_id=1, source_target_pairs={{0,1},{1,0},{2,3},{3,2},{4,5},{5,4},{6,7},{7,6},{8,9},{9,8},{10,11... | collective-permute-start | bytes 393224 | tf_op jit(solution)/shard_map/ppermute | solution.py:294
  92.4 34.3 %copy-start.2 = (bf16[8,512,128]{2,1,0:T(8,128)(2,1)S(1)}, bf16[8,512,128]{2,1,0:T(8,128)(2,1)}, u32[]{:S(2)}) copy-start(bf16[8,512,128]{2,1,0:T(8,128)(2,1)} %get-tuple-element.17) | copy-start | bytes 3145732
  92.4 34.3 %collective-permute-start = (bf16[8,512,128]{2,1,0:T(8,128)(2,1)}, bf16[8,512,128]{2,1,0:T(8,128)(2,1)S(1)}, u32[]{:S(2)}, u32[]{:S(2)}) collective-permute-start(bf16[8,512,128]{2,1,0:T(8,128)(2,1)} %get-tuple-element.18), channel_id=1, source_target_pairs={{0,1},{1,0},{2,3},{3,2},{4,5},{5,4},{6,7},{7,6},{8,9},{9,8},{10,11... | collective-permute-start | bytes 3145736 | tf_op jit(solution)/shard_map/ppermute | solution.py:294
  94.7 0.7 copy-start.1
  97.9 3.3 %collective-permute-start.1 = (bf16[128,128]{1,0:T(8,128)(2,1)}, bf16[128,128]{1,0:T(8,128)(2,1)S(1)}, u32[]{:S(2)}, u32[]{:S(2)}) collective-permute-start(bf16[128,128]{1,0:T(8,128)(2,1)} %shard_map.163.mine), channel_id=1, source_target_pairs={{0,1},{1,0},{2,3},{3,2},{4,5},{5,4},{6,7},{7,6},{8,9},{9,8},{10,11... | collective-permute-start | bytes 98312 | tf_op jit(solution)/shard_map/ppermute | solution.py:294
  100.0 1.2 copy-start.4
  101.2 0.6 copy-start.5
  127.9 32.0 %all-to-all-start.4 = ((bf16[8,512,128]{2,1,0:T(8,128)(2,1)}), bf16[8,512,128]{2,1,0:T(8,128)(2,1)S(1)}, u32[]{:S(2)}, u32[]{:S(2)}) async-start(bf16[8,512,128]{2,1,0:T(8,128)(2,1)} %add_convert_fusion), calls=%async_computation.4 | async-start | bytes 2097152 | tf_op jit(solution)/shard_map/all_to_all | solution.py:290
  131.5 47.1 %all-gather.7.cloned.1.call-start = ((), (), s32[]{:S(2)}) async-start(), calls=%async_computation.7 | async-start | bytes 1114112 | tf_op jit(solution)/shard_map/all_gather | solution.py:416
  160.8 20.9 %all-to-all-start.5 = ((bf16[32,16,128]{2,1,0:T(8,128)(2,1)}), bf16[32,16,128]{2,1,0:T(8,128)(2,1)S(1)}, u32[]{:S(2)}, u32[]{:S(2)}) async-start(bf16[32,16,128]{2,1,0:T(8,128)(2,1)} %bitcast.9), calls=%async_computation.5 | async-start | bytes 262144 | tf_op jit(solution)/shard_map/all_to_all | solution.py:290
  173.0 8.7 %copy-start.3 = (bf16[2,96,512]{2,1,0:T(8,128)(2,1)S(1)}, bf16[2,96,512]{2,1,0:T(8,128)(2,1)}, u32[]{:S(2)}) copy-start(bf16[2,96,512]{2,1,0:T(8,128)(2,1)} %shard_map.166) | copy-start | bytes 589828
Sparse Core Ops, SparseCore 0:
  47.2 39.6 all-gather.4
  134.4 44.1 all-gather.6
